TPU v7x, 512 devices: a whole 4x8x8 slice. The times are simulated.
512 devices in a mesh: fs: 64 (over z, y), tp: 8 (over x, core).
Axes of the slice: x: 4, y: 8, z: 8, core: 2. Of those that a mesh axis runs over, the one named last changes fastest.
Arguments:
- x_late: bfloat16 [12288, 2048], P(('fs', 'tp')), may hold values from -6 to 6
- x_early: bfloat16 [12288, 2048], P(('fs', 'tp')), may hold values from -6 to 6
- cotangent: bfloat16 [12288, 2048], P(('fs', 'tp')), may hold values from -1.25 to 1.25
- norm_gain: bfloat16 [2048], replicated, may hold values from 0.099609375 to 1.8984375
- gate_weight: bfloat16 [2048, 2816], P('fs', 'tp'), may hold values from -0.125 to 0.125
- up_weight: bfloat16 [2048, 2816], P('fs', 'tp'), may hold values from -0.125 to 0.125
- down_weight: bfloat16 [2048, 2816], P('fs', 'tp'), may hold values from -0.109375 to 0.109375
- gate_sum: float32 [2048, 2816], P('fs', 'tp'), may hold values from -6 to 6
- up_sum: float32 [2048, 2816], P('fs', 'tp'), may hold values from -6 to 6
- down_sum: float32 [2048, 2816], P('fs', 'tp'), may hold values from -6 to 6
Outputs:
- out_late: bfloat16 [12288, 2048], P(('fs', 'tp'))
- grad_early: bfloat16 [12288, 2048], P(('fs', 'tp'))
- gate_sum_out: float32 [2048, 2816], P('fs', 'tp')
- up_sum_out: float32 [2048, 2816], P('fs', 'tp')
- down_sum_out: float32 [2048, 2816], P('fs', 'tp')
All inputs are finite; a program needn't handle non-finite values.
Results may differ from a plain program's by a relative error of at most 0.0095.
Values may be sent and summed in bfloat16 or wider, within the bound.
No kernel may reach another device: no remote copies, remote signals or barrier semaphores. Data moves between devices by JAX's collectives and lax.ppermute only.
A program may use at most 64 MiB of HBM per device.

v0:
```python
import functools

import jax
import jax.numpy as jnp
from jax import lax
from jax.experimental import pallas as pl
from jax.experimental.pallas import tpu as pltpu
from jax.sharding import Mesh
from jax.sharding import PartitionSpec as P


eps = 1e-06
f32 = jnp.float32
bf16 = jnp.bfloat16

AXES = ("z", "yq", "ys", "x", "c")
NZ, NY, NX, NC = 8, 8, 4, 2
ROWS = 32
HALF = 176
MAIN = 128
TAIL = 48
LANES = 640


def call(body, out_shape, *args, mib=16, **kw):
    return pl.pallas_call(
        body,
        out_shape=out_shape,
        compiler_params=pltpu.CompilerParams(vmem_limit_bytes=mib * 1024 * 1024),
        **kw,
    )(*args)


def exchange(x, axis, size, phase):
    pairs = []
    for i in range(size):
        for c in range(NC):
            j = (i + 1) % size if (i + c + phase) % 2 == 0 else (i - 1) % size
            pairs.append((i * NC + c, j * NC + c))
    return lax.ppermute(x, (axis, "c"), pairs)


def swapped(x, axis):
    return lax.ppermute(x, axis, [(0, 1), (1, 0)])


def over_y(x):
    return lax.all_to_all(x, ("yq", "ys"), split_axis=0, concat_axis=0, tiled=True)


def dot_tt(left, right):
    return lax.dot_general(left, right, (((1,), (1,)), ((), ())), preferred_element_type=f32)


def dot_nn(left, right):
    return lax.dot_general(left, right, (((1,), (0,)), ((), ())), preferred_element_type=f32)


def lanes_below(n):
    return lax.broadcasted_iota(jnp.int32, (ROWS, 128), 1) < n


def fetch(pairs, sem):
    copies = [pltpu.make_async_copy(a, b, sem.at[i]) for i, (a, b) in enumerate(pairs)]
    for copy in copies:
        copy.start()
    for copy in copies:
        copy.wait()


def pack_weights(g_hbm, u_hbm, d_hbm, o_ref, g_ref, u_ref, d_ref, sem):
    fetch(((g_hbm, g_ref), (u_hbm, u_ref), (d_hbm, d_ref)), sem)
    last = []
    for r in (g_ref, u_ref, d_ref):
        r = r[...].astype(f32)
        last.append(jnp.concatenate([r[:, 256:352], jnp.zeros((ROWS, 32), f32)], axis=1))
    g, u, d = last
    for h in range(2):
        if h == 0:
            t3 = jnp.where(lanes_below(48), g, pltpu.roll(u, 48, 1))
            t4 = d
        else:
            t3 = jnp.where(lanes_below(48), pltpu.roll(g, 80, 1), u)
            t4 = pltpu.roll(d, 80, 1)
        t3 = jnp.where(lanes_below(96), t3, 0.0).astype(bf16)
        t4 = jnp.where(lanes_below(48), t4, 0.0).astype(bf16)
        for q in range(4):
            for i, r in enumerate((g_ref, u_ref, d_ref)):
                o_ref[2 * q + h, :, MAIN * i : MAIN * (i + 1)] = r[:, h * MAIN : (h + 1) * MAIN]
            o_ref[2 * q + h, :, 384:512] = t3
            o_ref[2 * q + h, :, 512:640] = t4


def normalize(x, gain):
    inv = lax.rsqrt(jnp.mean(x * x, axis=-1, keepdims=True) + eps)
    return inv, x * inv * gain


def prepare_tokens(e_hbm, c_hbm, l_hbm, g_hbm, o_ref, e_ref, c_ref, l_ref, g_ref, sem):
    fetch(((e_hbm, e_ref), (c_hbm, c_ref), (l_hbm, l_ref), (g_hbm, g_ref)), sem)
    gain = g_ref[...].astype(f32)
    o_ref[0] = normalize(e_ref[...].astype(f32), gain)[1].astype(bf16)
    o_ref[1] = (0.5 * c_ref[...].astype(f32)).astype(bf16)
    o_ref[2] = normalize(l_ref[...].astype(f32), gain)[1].astype(bf16)


def turn_block(r_ref, o_ref):
    t = r_ref[...].reshape(NY * ROWS, LANES).T
    for i, at in enumerate((384, 432, 512)):
        o_ref[HALF * i : HALF * i + MAIN] = t[MAIN * i : MAIN * (i + 1)]
        o_ref[HALF * i + MAIN : HALF * (i + 1)] = t[at : at + TAIL]


def join(a_ref, b_ref, o_ref):
    o_ref[0] = a_ref[...]
    o_ref[1] = b_ref[...]


def turned(f):
    zero = jnp.zeros((32, 256), f.dtype)
    return jnp.concatenate(
        [f[HALF * i : HALF * i + MAIN] for i in range(3)]
        + [f[HALF * i + MAIN : HALF * (i + 1)] for i in range(2)]
        + [zero, f[2 * HALF + MAIN : 3 * HALF], zero, zero, zero[:16]],
        axis=0,
    ).T


def forward_part(b_ref, ta, tb, p0, p1, p2, te, th, tl, acc, w):
    for q, piece in enumerate((ta, tb)):
        for n in range(2):
            rows = pl.ds((q * 2 + n) * 48, 48)
            for k in range(8):
                cols = pl.ds(pl.multiple_of(b_ref[k] * 256, 256), 256)
                out = pl.ds(k * 256, 256)
                te[rows, out] = piece[n, 0, :, cols]
                th[rows, out] = piece[n, 1, :, cols]
                tl[rows, out] = piece[n, 2, :, cols]
    for q, pair in enumerate((p0, p1, p2)):
        for n in range(2):
            w[:, pl.ds((2 * q + n) * 256, 256)] = pair[n]
    k = 6 * 256
    g, u, d = w[0:HALF], w[HALF : 2 * HALF], w[2 * HALF : 3 * HALF]
    acc[0] = dot_tt(te[:, :k], g)
    acc[1] = dot_tt(te[:, :k], u)
    acc[2] = dot_tt(th[:, :k], d)


def grad_block(at_ref, te, th, k, o, n, add=None):
    cols = pl.ds(k * 256, 256)
    for rows, t in ((slice(0, 2 * HALF), te), (slice(2 * HALF, 3 * HALF), th)):
        sums = dot_nn(at_ref[0, rows], t[0][:, cols]) + dot_nn(at_ref[1, rows], t[1][:, cols])
        if add is not None:
            sums = sums + add[rows].astype(f32)
        o[n, rows] = sums.astype(o.dtype)


def early_rest(acc0, acc1, te0, te1, th0, th1, p3, dg_ref, du_ref, at_ref, s_ref, w):
    for n in range(2):
        w[:, pl.ds(n * 256, 256)] = p3[n]
    k = 6 * 256
    for h, (acc, te, th) in enumerate(((acc0, te0, th0), (acc1, te1, th1))):
        gate = acc[0] + dot_tt(te[:, k:], w[0:HALF])
        up = acc[1] + dot_tt(te[:, k:], w[HALF : 2 * HALF])
        dh = acc[2] + dot_tt(th[:, k:], w[2 * HALF : 3 * HALF])
        sig = jax.nn.sigmoid(gate)
        silu = gate * sig
        hidden = (silu * up).astype(bf16)
        dg = (dh * up * sig * (1.0 + gate * (1.0 - sig))).astype(bf16)
        du = (dh * silu).astype(bf16)
        dg_ref[h] = dg
        du_ref[h] = du
        at_ref[h, 0:HALF] = dg.T
        at_ref[h, HALF : 2 * HALF] = du.T
        at_ref[h, 2 * HALF : 3 * HALF] = hidden.T
    for n in range(2):
        grad_block(at_ref, (te0, te1), (th0, th1), 6 + n, s_ref, n)


def add_pair(k, at_ref, te0, te1, th0, th1, r_ref, o_ref):
    for n in range(2):
        grad_block(at_ref, (te0, te1), (th0, th1), k + n, o_ref, n, r_ref[n])


def add_second(at_ref, te0, te1, th0, th1, r_ref, o_ref):
    grad_block(at_ref, (te0, te1), (th0, th1), 1, o_ref, 0, r_ref[1])


def own_block(at_ref, te0, te1, th0, th1, r_ref, o_ref, f):
    grad_block(at_ref, (te0, te1), (th0, th1), 0, f, 0, r_ref[0])
    o_ref[...] = turned(f[0])


def last_block(f_ref, r_ref, o_ref):
    t = f_ref[...] + turned(r_ref[0]).astype(f32)
    o_ref[...] = t.reshape(NY, ROWS, LANES).astype(bf16)


def token_parts(b_ref, dg_ref, du_ref, tl0, tl1, p0, p1, p2, p3, near, far, w):
    pairs = (p0, p1, p2, p3)
    for q, pair in enumerate(pairs):
        for n in range(2):
            w[:, pl.ds((2 * q + n) * 256, 256)] = pair[n, 0 : 2 * HALF]
    for h, (tl, o) in enumerate(((tl0, near), (tl1, far))):
        gl = dot_tt(tl[...], w[0:HALF])
        ul = dot_tt(tl[...], w[HALF : 2 * HALF])
        hl = (gl * jax.nn.sigmoid(gl) * ul).astype(bf16)
        dg, du = dg_ref[h], du_ref[h]
        for q, pair in enumerate(pairs):
            for n in range(2):
                cols = pl.ds(pl.multiple_of(b_ref[2 * q + n] * 256, 256), 256)
                late = dot_nn(hl, pair[n, 2 * HALF : 3 * HALF])
                early = dot_nn(dg, pair[n, 0:HALF]) + dot_nn(du, pair[n, HALF : 2 * HALF])
                o[0, :, cols] = late.astype(o.dtype)
                o[1, :, cols] = early.astype(o.dtype)


def fold(n_ref, r_ref, keep, send):
    rows = keep.shape[1]
    for i in range(2):
        keep[i] = n_ref[i, :rows] + r_ref[i, :rows].astype(f32)
        send[i] = (n_ref[i, rows:] + r_ref[i, rows:].astype(f32)).astype(bf16)


def finish_tokens(n_ref, r_ref, e_ref, c_ref, l_ref, g_ref, late, early):
    gain = g_ref[...].astype(f32)
    branch = n_ref[0] + r_ref[0].astype(f32)
    late[...] = (l_ref[...].astype(f32) + 0.5 * branch).astype(bf16)
    d_normed = n_ref[1] + r_ref[1].astype(f32)
    x = e_ref[...].astype(f32)
    inv, _ = normalize(x, gain)
    scaled = d_normed * gain
    d_input = inv * scaled - x * inv**3 * jnp.mean(scaled * x, axis=-1, keepdims=True)
    early[...] = (c_ref[...].astype(f32) + d_input).astype(bf16)


def finish_weights(r_ref, gs, us, ds, go, uo, do):
    total = []
    for h in range(2):
        t = r_ref[h].astype(f32)
        for q in range(1, 4):
            t = t + r_ref[2 * q + h].astype(f32)
        total.append(t)
    t3 = [t[:, 384:512] for t in total]
    t4 = [t[:, 512:640] for t in total]
    low = lanes_below(48)
    g2 = jnp.where(low, t3[0], pltpu.roll(t3[1], 48, 1))
    u2 = jnp.where(low, pltpu.roll(t3[0], 80, 1), t3[1])
    d2 = jnp.where(low, t4[0], pltpu.roll(t4[1], 48, 1))
    for i, (s, o, t2) in enumerate(((gs, go, g2), (us, uo, u2), (ds, do, d2))):
        for h in range(2):
            cols = slice(h * MAIN, (h + 1) * MAIN)
            o[:, cols] = s[:, cols] + total[h][:, i * MAIN : (i + 1) * MAIN]
        o[:, 256:352] = s[:, 256:352] + t2[:, :96]


def shape(dims, dtype=bf16):
    return jax.ShapeDtypeStruct(dims, dtype)


VM = pl.BlockSpec(memory_space=pltpu.VMEM)
HB = pl.BlockSpec(memory_space=pltpu.MemorySpace.HBM)
SM = pl.BlockSpec(memory_space=pltpu.SMEM)


def on_device(
    x_late,
    x_early,
    cotangent,
    norm_gain,
    gate_weight,
    up_weight,
    down_weight,
    gate_sum,
    up_sum,
    down_sum,
):
    gain = norm_gain.reshape(1, -1)
    z, c = lax.axis_index("z"), lax.axis_index("c")
    step = 1 - 2 * lax.rem(z + c, 2)
    order = jnp.array([0, 1, -1, -2, 2, 3, -3, -4], jnp.int32)
    blocks = lax.rem(z + order * step + 8, 8).astype(jnp.int32)

    sent = call(
        pack_weights,
        shape((NY, ROWS, LANES)),
        *(pltpu.with_memory_space_constraint(w, pltpu.HBM) for w in (gate_weight, up_weight, down_weight)),
        in_specs=[HB] * 3,
        scratch_shapes=[pltpu.VMEM((ROWS, 352), bf16)] * 3 + [pltpu.SemaphoreType.DMA((3,))],
    )
    own = call(turn_block, shape((3 * HALF, 256)), over_y(sent))
    p0 = call(join, shape((2, 3 * HALF, 256)), own, exchange(own, "z", NZ, 0))
    p1 = exchange(p0, "z", NZ, 1)
    p2 = exchange(p1, "z", NZ, 0)
    p3 = exchange(p2, "z", NZ, 1)

    tok = call(
        prepare_tokens,
        shape((3, 24, 2048)),
        *(pltpu.with_memory_space_constraint(x, pltpu.HBM) for x in (x_early, cotangent, x_late, gain)),
        in_specs=[HB] * 4,
        scratch_shapes=[pltpu.VMEM((24, 2048), bf16)] * 3
        + [pltpu.VMEM((1, 2048), bf16), pltpu.SemaphoreType.DMA((4,))],
    )
    t0 = jnp.concatenate([tok, swapped(tok, "ys")], axis=1)
    ta = jnp.stack([t0, exchange(t0, "x", NX, 0)])
    tb = exchange(ta, "x", NX, 1)
    tc = swapped(ta, "c")
    td = swapped(tb, "c")

    def most(first, second):
        return call(
            forward_part,
            (shape((192, 2048)),) * 3 + (shape((3, 192, HALF), f32),),
            blocks, first, second, p0, p1, p2,
            in_specs=[SM] + [VM] * 5,
            scratch_shapes=[pltpu.VMEM((3 * HALF, 6 * 256), bf16)],
        )

    te0, th0, tl0, acc0 = most(ta, tb)
    te1, th1, tl1, acc1 = most(tc, td)
    pair = shape((2, 3 * HALF, 256))
    dg, du, at, s3 = call(
        early_rest,
        (shape((2, 192, HALF)), shape((2, 192, HALF)), shape((2, 3 * HALF, 192)), pair),
        acc0, acc1, te0, te1, th0, th1, p3,
        scratch_shapes=[pltpu.VMEM((3 * HALF, 512), bf16)],
    )
    tokens = (at, te0, te1, th0, th1)
    r3 = exchange(s3, "z", NZ, 1)
    near, far = call(
        token_parts,
        (shape((2, 192, 2048), f32), shape((2, 192, 2048))),
        blocks, dg, du, tl0, tl1, p0, p1, p2, p3,
        in_specs=[SM] + [VM] * 8,
        scratch_shapes=[pltpu.VMEM((2 * HALF, 2048), bf16)],
    )
    s2 = call(functools.partial(add_pair, 4), pair, *tokens, r3)
    r2 = exchange(s2, "z", NZ, 0)
    s1 = call(functools.partial(add_pair, 2), pair, *tokens, r2)
    r1 = exchange(s1, "z", NZ, 1)
    s0 = call(add_second, shape((1, 3 * HALF, 256)), *tokens, r1)
    r0 = exchange(s0, "z", NZ, 0)
    block = call(
        own_block,
        shape((256, LANES), f32),
        *tokens, r1,
        scratch_shapes=[pltpu.VMEM((1, 3 * HALF, 256), f32)],
    )
    back = call(last_block, shape((NY, ROWS, LANES)), block, r0)
    sums = call(
        finish_weights,
        (shape((ROWS, 352), f32),) * 3,
        over_y(back), gate_sum, up_sum, down_sum,
    )

    def folded(near, far):
        dims = (2, near.shape[1] // 2, 2048)
        return call(fold, (shape(dims, f32), shape(dims)), near, far)

    near, far = folded(near, swapped(far, "c"))
    near, far = folded(near, exchange(far, "x", NX, 1))
    near, far = folded(near, exchange(far, "x", NX, 0))
    late, early = call(
        finish_tokens,
        (shape((24, 2048)),) * 2,
        near, swapped(far, "ys"), x_early, cotangent, x_late, gain,
    )
    return (late, early, *sums)


def solution(mesh):
    fine = Mesh(mesh.devices.reshape(NZ, 4, 2, NX, NC), AXES)
    token = P(AXES, None)
    weight = P(("z", "yq", "ys"), ("x", "c"))
    return jax.shard_map(
        on_device,
        mesh=fine,
        in_specs=(token, token, token, P()) + (weight,) * 6,
        out_specs=(token, token) + (weight,) * 3,
        check_vma=False,
    )
```

profile of v0, /device:TPU:2, one launch (start us, length us, event | category | flops | bytes accessed | tf_op | source)
XLA Modules:
  0.0 162.4 jit_solution(11410196505540437989)
XLA Ops:
  3.1 3.5 %collective-permute-start = (bf16[3,24,2048]{2,1,0:T(8,128)(2,1)S(1)}, bf16[3,24,2048]{2,1,0:T(8,128)(2,1)S(1)}, u32[]{:S(2)}, u32[]{:S(2)}) collective-permute-start(bf16[3,24,2048]{2,1,0:T(8,128)(2,1)S(1)} %shard_map.146), channel_id=1, source_target_pairs={{0,8},{8,0},{1,9},{9,1},{2,10},{10,2},{3,11},{11,3},{4,12},{12,4},... | collective-permute-start | bytes 884744 | tf_op jit(solution)/shard_map/ppermute | solution.py:44
  6.6 7.1 %collective-permute-done = bf16[3,24,2048]{2,1,0:T(8,128)(2,1)S(1)} collective-permute-done((bf16[3,24,2048]{2,1,0:T(8,128)(2,1)S(1)}, bf16[3,24,2048]{2,1,0:T(8,128)(2,1)S(1)}, u32[]{:S(2)}, u32[]{:S(2)}) %collective-permute-start) | collective-permute-done | bytes 294944 | tf_op jit(solution)/shard_map/ppermute | solution.py:44
  13.9 5.8 %collective-permute-start.1 = (bf16[3,48,2048]{2,1,0:T(8,128)(2,1)S(1)}, bf16[3,48,2048]{2,1,0:T(8,128)(2,1)S(1)}, u32[]{:S(2)}, u32[]{:S(2)}) collective-permute-start(bf16[3,48,2048]{2,1,0:T(8,128)(2,1)S(1)} %get-tuple-element.56), channel_id=1, source_target_pairs={{0,2},{1,7},{2,0},{3,5},{4,6},{5,3},{6,4},{7,1},{8,10},{9,15},{10,... | collective-permute-start | bytes 1769480 | tf_op jit(solution)/shard_map/ppermute | solution.py:40
  21.3 3.8 %all-to-all-start = ((bf16[8,32,640]{2,1,0:T(8,128)(2,1)}), bf16[8,32,640]{2,1,0:T(8,128)(2,1)S(1)}, u32[]{:S(2)}, u32[]{:S(2)}) async-start(bf16[8,32,640]{2,1,0:T(8,128)(2,1)} %shard_map.147), calls=%async_computation | async-start | bytes 655360 | tf_op jit(solution)/shard_map/all_to_all | solution.py:48
  25.1 2.4 %collective-permute-done.1 = bf16[3,48,2048]{2,1,0:T(8,128)(2,1)S(1)} collective-permute-done((bf16[3,48,2048]{2,1,0:T(8,128)(2,1)S(1)}, bf16[3,48,2048]{2,1,0:T(8,128)(2,1)S(1)}, u32[]{:S(2)}, u32[]{:S(2)}) %collective-permute-start.1) | collective-permute-done | bytes 589856 | tf_op jit(solution)/shard_map/ppermute | solution.py:40
  27.6 1.9 %collective-permute-start.2 = (bf16[2,3,48,2048]{3,2,1,0:T(8,128)(2,1)S(1)}, bf16[2,3,48,2048]{3,2,1,0:T(8,128)(2,1)}, u32[]{:S(2)}, u32[]{:S(2)}) collective-permute-start(bf16[2,3,48,2048]{3,2,1,0:T(8,128)(2,1)S(1)} %pad_maximum_fusion.ta), channel_id=1, source_target_pairs={{0,6},{1,3},{2,4},{3,1},{4,2},{5,7},{6,0},{7,5},{8,14},{9,11},{10,... | collective-permute-start | bytes 3538952 | tf_op jit(solution)/shard_map/ppermute | solution.py:40
  29.6 8.6 %all-to-all-done.r_ref = bf16[8,32,640]{2,1,0:T(8,128)(2,1)S(1)} async-done(((bf16[8,32,640]{2,1,0:T(8,128)(2,1)}), bf16[8,32,640]{2,1,0:T(8,128)(2,1)S(1)}, u32[]{:S(2)}, u32[]{:S(2)}) %all-to-all-start) | async-done | bytes 327712 | tf_op jit(solution)/shard_map/all_to_all | solution.py:48
  38.3 4.3 %collective-permute-start.3 = (bf16[528,256]{1,0:T(8,128)(2,1)S(1)}, bf16[528,256]{1,0:T(8,128)(2,1)S(1)}, u32[]{:S(2)}, u32[]{:S(2)}) collective-permute-start(bf16[528,256]{1,0:T(8,128)(2,1)S(1)} %shard_map.148.a_ref), channel_id=1, source_target_pairs={{0,64},{1,449},{64,0},{65,129},{128,192},{129,65},{192,128},{193,2... | collective-permute-start | bytes 811016 | tf_op jit(solution)/shard_map/ppermute | solution.py:40
  42.6 4.4 %collective-permute-done.3.b_ref = bf16[528,256]{1,0:T(8,128)(2,1)S(1)} collective-permute-done((bf16[528,256]{1,0:T(8,128)(2,1)S(1)}, bf16[528,256]{1,0:T(8,128)(2,1)S(1)}, u32[]{:S(2)}, u32[]{:S(2)}) %collective-permute-start.3) | collective-permute-done | bytes 270368 | tf_op jit(solution)/shard_map/ppermute | solution.py:40
  47.1 10.6 %collective-permute-start.4 = (bf16[2,528,256]{2,1,0:T(8,128)(2,1)S(1)}, bf16[2,528,256]{2,1,0:T(8,128)(2,1)S(1)}, u32[]{:S(2)}, u32[]{:S(2)}) collective-permute-start(bf16[2,528,256]{2,1,0:T(8,128)(2,1)S(1)} %shard_map.149.p0), channel_id=1, source_target_pairs={{0,448},{1,65},{64,128},{65,1},{128,64},{129,193},{192,256},{193,1... | collective-permute-start | bytes 1622024 | tf_op jit(solution)/shard_map/ppermute | solution.py:40
  57.6 1.9 %collective-permute-start.6 = (bf16[2,3,48,2048]{3,2,1,0:T(8,128)(2,1)S(1)}, bf16[2,3,48,2048]{3,2,1,0:T(8,128)(2,1)}, u32[]{:S(2)}, u32[]{:S(2)}) collective-permute-start(bf16[2,3,48,2048]{3,2,1,0:T(8,128)(2,1)S(1)} %pad_maximum_fusion.ta), channel_id=1, source_target_pairs={{0,1},{1,0},{2,3},{3,2},{4,5},{5,4},{6,7},{7,6},{8,9},{9,8},{10,11... | collective-permute-start | bytes 3538952 | tf_op jit(solution)/shard_map/ppermute | solution.py:44
  59.6 2.4 %collective-permute-start.7 = (bf16[2,3,48,2048]{3,2,1,0:T(8,128)(2,1)}, bf16[2,3,48,2048]{3,2,1,0:T(8,128)(2,1)}, u32[]{:S(2)}, u32[]{:S(2)}) collective-permute-start(bf16[2,3,48,2048]{3,2,1,0:T(8,128)(2,1)} %collective-permute-done.2.tb), channel_id=1, source_target_pairs={{0,1},{1,0},{2,3},{3,2},{4,5},{5,4},{6,7},{7,6},{8,9},{9,8},{10,11... | collective-permute-start | bytes 3538952 | tf_op jit(solution)/shard_map/ppermute | solution.py:44
  62.0 3.0 %collective-permute-done.4.p1 = bf16[2,528,256]{2,1,0:T(8,128)(2,1)S(1)} collective-permute-done((bf16[2,528,256]{2,1,0:T(8,128)(2,1)S(1)}, bf16[2,528,256]{2,1,0:T(8,128)(2,1)S(1)}, u32[]{:S(2)}, u32[]{:S(2)}) %collective-permute-start.4) | collective-permute-done | bytes 540704 | tf_op jit(solution)/shard_map/ppermute | solution.py:40
  66.9 9.3 %collective-permute-done.5.p2 = bf16[2,528,256]{2,1,0:T(8,128)(2,1)S(1)} collective-permute-done((bf16[2,528,256]{2,1,0:T(8,128)(2,1)S(1)}, bf16[2,528,256]{2,1,0:T(8,128)(2,1)S(1)}, u32[]{:S(2)}, u32[]{:S(2)}) %collective-permute-start.5) | collective-permute-done | bytes 540704 | tf_op jit(solution)/shard_map/ppermute | solution.py:40
  76.2 5.1 %collective-permute-start.8 = (bf16[2,528,256]{2,1,0:T(8,128)(2,1)S(1)}, bf16[2,528,256]{2,1,0:T(8,128)(2,1)S(1)}, u32[]{:S(2)}, u32[]{:S(2)}) collective-permute-start(bf16[2,528,256]{2,1,0:T(8,128)(2,1)S(1)} %collective-permute-done.5.p2), channel_id=1, source_target_pairs={{0,448},{1,65},{64,128},{65,1},{128,64},{129,193},{192,256},{193,1... | collective-permute-start | bytes 1622024 | tf_op jit(solution)/shard_map/ppermute | solution.py:40
  81.4 2.1 %shard_map.150 = (bf16[192,2048]{1,0:T(8,128)(2,1)S(1)}, bf16[192,2048]{1,0:T(8,128)(2,1)S(1)}, bf16[192,2048]{1,0:T(8,128)(2,1)S(1)}, f32[3,192,176]{2,1,0:T(8,128)S(1)}) custom-call(s32[8]{0:T(128)S(1)} %compare_select_fusion.b_ref, bf16[2,3,48,2048]{3,2,1,0:T(8,128)(2,1)S(1)} %pad_maximum_fusion.ta, bf16[2,3,48,2048]{3,2,1,0:T(8,128)(2,1)} %collective-permute-done.2.tb, ...), custom_call_target="tpu_custom_call" | custom-call | tf_op jit(solution)/shard_map/pallas_call | solution.py:26
  83.5 2.4 %shard_map.151 = (bf16[192,2048]{1,0:T(8,128)(2,1)S(1)}, bf16[192,2048]{1,0:T(8,128)(2,1)S(1)}, bf16[192,2048]{1,0:T(8,128)(2,1)S(1)}, f32[3,192,176]{2,1,0:T(8,128)S(1)}) custom-call(s32[8]{0:T(128)S(1)} %compare_select_fusion.b_ref, bf16[2,3,48,2048]{3,2,1,0:T(8,128)(2,1)} %collective-permute-done.6.ta, ...), custom_call_target="tpu_custom_call" | custom-call | tf_op jit(solution)/shard_map/pallas_call | solution.py:26
  85.9 2.8 %collective-permute-done.8.p3 = bf16[2,528,256]{2,1,0:T(8,128)(2,1)S(1)} collective-permute-done((bf16[2,528,256]{2,1,0:T(8,128)(2,1)S(1)}, bf16[2,528,256]{2,1,0:T(8,128)(2,1)S(1)}, u32[]{:S(2)}, u32[]{:S(2)}) %collective-permute-start.8) | collective-permute-done | bytes 540704 | tf_op jit(solution)/shard_map/ppermute | solution.py:40
  89.8 3.3 %shard_map.153 = (f32[2,192,2048]{2,1,0:T(8,128)S(1)}, bf16[2,192,2048]{2,1,0:T(8,128)(2,1)S(1)}) custom-call(s32[8]{0:T(128)S(1)} %compare_select_fusion.b_ref, bf16[2,192,176]{2,1,0:T(8,128)(2,1)S(1)} %get-tuple-element.36.dg_ref, bf16[2,192,176]{2,1,0:T(8,128)(2,1)S(1)} %get-tuple-element.37.du_ref, bf16[192,2048]{1,0:T(8,128)(2,1)S(1)} %get-tuple-element.38.tl0, ...), custom_call_target="tpu_custom_call" | custom-call | tf_op jit(solution)/shard_map/pallas_call | solution.py:26
  93.0 1.9 %collective-permute-start.9 = (bf16[2,192,2048]{2,1,0:T(8,128)(2,1)S(1)}, bf16[2,192,2048]{2,1,0:T(8,128)(2,1)S(1)}, u32[]{:S(2)}, u32[]{:S(2)}) collective-permute-start(bf16[2,192,2048]{2,1,0:T(8,128)(2,1)S(1)} %get-tuple-element.41), channel_id=1, source_target_pairs={{0,1},{1,0},{2,3},{3,2},{4,5},{5,4},{6,7},{7,6},{8,9},{9,8},{10,11... | collective-permute-start | bytes 4718600 | tf_op jit(solution)/shard_map/ppermute | solution.py:44
  95.0 5.1 %collective-permute-start.13 = (bf16[2,528,256]{2,1,0:T(8,128)(2,1)S(1)}, bf16[2,528,256]{2,1,0:T(8,128)(2,1)S(1)}, u32[]{:S(2)}, u32[]{:S(2)}) collective-permute-start(bf16[2,528,256]{2,1,0:T(8,128)(2,1)S(1)} %get-tuple-element.51), channel_id=1, source_target_pairs={{0,448},{1,65},{64,128},{65,1},{128,64},{129,193},{192,256},{193,1... | collective-permute-start | bytes 1622024 | tf_op jit(solution)/shard_map/ppermute | solution.py:40
  100.1 7.3 %collective-permute-done.13.r_ref = bf16[2,528,256]{2,1,0:T(8,128)(2,1)S(1)} collective-permute-done((bf16[2,528,256]{2,1,0:T(8,128)(2,1)S(1)}, bf16[2,528,256]{2,1,0:T(8,128)(2,1)S(1)}, u32[]{:S(2)}, u32[]{:S(2)}) %collective-permute-start.13) | collective-permute-done | bytes 540704 | tf_op jit(solution)/shard_map/ppermute | solution.py:40
  107.9 1.9 %collective-permute-start.14 = (bf16[2,528,256]{2,1,0:T(8,128)(2,1)S(1)}, bf16[2,528,256]{2,1,0:T(8,128)(2,1)S(1)}, u32[]{:S(2)}, u32[]{:S(2)}) collective-permute-start(bf16[2,528,256]{2,1,0:T(8,128)(2,1)S(1)} %shard_map.158), channel_id=1, source_target_pairs={{0,64},{1,449},{64,0},{65,129},{128,192},{129,65},{192,128},{193,2... | collective-permute-start | bytes 1622024 | tf_op jit(solution)/shard_map/ppermute | solution.py:40
  109.8 9.3 %collective-permute-done.14.r_ref = bf16[2,528,256]{2,1,0:T(8,128)(2,1)S(1)} collective-permute-done((bf16[2,528,256]{2,1,0:T(8,128)(2,1)S(1)}, bf16[2,528,256]{2,1,0:T(8,128)(2,1)S(1)}, u32[]{:S(2)}, u32[]{:S(2)}) %collective-permute-start.14) | collective-permute-done | bytes 540704 | tf_op jit(solution)/shard_map/ppermute | solution.py:40
  119.6 5.1 %collective-permute-start.15 = (bf16[2,528,256]{2,1,0:T(8,128)(2,1)S(1)}, bf16[2,528,256]{2,1,0:T(8,128)(2,1)S(1)}, u32[]{:S(2)}, u32[]{:S(2)}) collective-permute-start(bf16[2,528,256]{2,1,0:T(8,128)(2,1)S(1)} %shard_map.159), channel_id=1, source_target_pairs={{0,448},{1,65},{64,128},{65,1},{128,64},{129,193},{192,256},{193,1... | collective-permute-start | bytes 1622024 | tf_op jit(solution)/shard_map/ppermute | solution.py:40
  125.1 3.4 %collective-permute-start.10 = (bf16[2,96,2048]{2,1,0:T(8,128)(2,1)S(1)}, bf16[2,96,2048]{2,1,0:T(8,128)(2,1)S(1)}, u32[]{:S(2)}, u32[]{:S(2)}) collective-permute-start(bf16[2,96,2048]{2,1,0:T(8,128)(2,1)S(1)} %get-tuple-element.43), channel_id=1, source_target_pairs={{0,6},{1,3},{2,4},{3,1},{4,2},{5,7},{6,0},{7,5},{8,14},{9,11},{10,... | collective-permute-start | bytes 2359304 | tf_op jit(solution)/shard_map/ppermute | solution.py:40
  128.5 3.5 %collective-permute-done.15.r_ref = bf16[2,528,256]{2,1,0:T(8,128)(2,1)S(1)} collective-permute-done((bf16[2,528,256]{2,1,0:T(8,128)(2,1)S(1)}, bf16[2,528,256]{2,1,0:T(8,128)(2,1)S(1)}, u32[]{:S(2)}, u32[]{:S(2)}) %collective-permute-start.15) | collective-permute-done | bytes 540704 | tf_op jit(solution)/shard_map/ppermute | solution.py:40
  134.3 5.3 %collective-permute-done.10.r_ref = bf16[2,96,2048]{2,1,0:T(8,128)(2,1)S(1)} collective-permute-done((bf16[2,96,2048]{2,1,0:T(8,128)(2,1)S(1)}, bf16[2,96,2048]{2,1,0:T(8,128)(2,1)S(1)}, u32[]{:S(2)}, u32[]{:S(2)}) %collective-permute-start.10) | collective-permute-done | bytes 786464 | tf_op jit(solution)/shard_map/ppermute | solution.py:40
  139.7 5.0 %collective-permute-start.11 = (bf16[2,48,2048]{2,1,0:T(8,128)(2,1)S(1)}, bf16[2,48,2048]{2,1,0:T(8,128)(2,1)S(1)}, u32[]{:S(2)}, u32[]{:S(2)}) collective-permute-start(bf16[2,48,2048]{2,1,0:T(8,128)(2,1)S(1)} %get-tuple-element.45), channel_id=1, source_target_pairs={{0,2},{1,7},{2,0},{3,5},{4,6},{5,3},{6,4},{7,1},{8,10},{9,15},{10,... | collective-permute-start | bytes 1179656 | tf_op jit(solution)/shard_map/ppermute | solution.py:40
  146.1 3.6 %all-to-all-start.1 = ((bf16[8,32,640]{2,1,0:T(8,128)(2,1)}), bf16[8,32,640]{2,1,0:T(8,128)(2,1)S(1)}, u32[]{:S(2)}, u32[]{:S(2)}) async-start(bf16[8,32,640]{2,1,0:T(8,128)(2,1)} %shard_map.162), calls=%async_computation.1 | async-start | bytes 655360 | tf_op jit(solution)/shard_map/all_to_all | solution.py:48
  150.5 3.1 %collective-permute-start.12 = (bf16[2,24,2048]{2,1,0:T(8,128)(2,1)S(1)}, bf16[2,24,2048]{2,1,0:T(8,128)(2,1)S(1)}, u32[]{:S(2)}, u32[]{:S(2)}) collective-permute-start(bf16[2,24,2048]{2,1,0:T(8,128)(2,1)S(1)} %get-tuple-element.47), channel_id=1, source_target_pairs={{0,8},{8,0},{1,9},{9,1},{2,10},{10,2},{3,11},{11,3},{4,12},{12,4},... | collective-permute-start | bytes 589832 | tf_op jit(solution)/shard_map/ppermute | solution.py:44
  153.6 7.3 %all-to-all-done.1.r_ref = bf16[8,32,640]{2,1,0:T(8,128)(2,1)S(1)} async-done(((bf16[8,32,640]{2,1,0:T(8,128)(2,1)}), bf16[8,32,640]{2,1,0:T(8,128)(2,1)S(1)}, u32[]{:S(2)}, u32[]{:S(2)}) %all-to-all-start.1) | async-done | bytes 327712 | tf_op jit(solution)/shard_map/all_to_all | solution.py:48
  (44 shorter events, 14.8 us)
Async XLA Ops:
  3.1 10.6 %collective-permute-start = (bf16[3,24,2048]{2,1,0:T(8,128)(2,1)S(1)}, bf16[3,24,2048]{2,1,0:T(8,128)(2,1)S(1)}, u32[]{:S(2)}, u32[]{:S(2)}) collective-permute-start(bf16[3,24,2048]{2,1,0:T(8,128)(2,1)S(1)} %shard_map.146), channel_id=1, source_target_pairs={{0,8},{8,0},{1,9},{9,1},{2,10},{10,2},{3,11},{11,3},{4,12},{12,4},... | collective-permute-start | bytes 884744 | tf_op jit(solution)/shard_map/ppermute | solution.py:44
  13.9 13.6 %collective-permute-start.1 = (bf16[3,48,2048]{2,1,0:T(8,128)(2,1)S(1)}, bf16[3,48,2048]{2,1,0:T(8,128)(2,1)S(1)}, u32[]{:S(2)}, u32[]{:S(2)}) collective-permute-start(bf16[3,48,2048]{2,1,0:T(8,128)(2,1)S(1)} %get-tuple-element.56), channel_id=1, source_target_pairs={{0,2},{1,7},{2,0},{3,5},{4,6},{5,3},{6,4},{7,1},{8,10},{9,15},{10,... | collective-permute-start | bytes 1769480 | tf_op jit(solution)/shard_map/ppermute | solution.py:40
  21.3 16.9 %all-to-all-start = ((bf16[8,32,640]{2,1,0:T(8,128)(2,1)}), bf16[8,32,640]{2,1,0:T(8,128)(2,1)S(1)}, u32[]{:S(2)}, u32[]{:S(2)}) async-start(bf16[8,32,640]{2,1,0:T(8,128)(2,1)} %shard_map.147), calls=%async_computation | async-start | bytes 655360 | tf_op jit(solution)/shard_map/all_to_all | solution.py:48
  27.6 53.7 %copy-start.7 = (s32[8]{0:T(128)S(1)}, s32[8]{0:T(128)}, u32[]{:S(2)}) copy-start(s32[8]{0:T(128)} %constant.24.clone) | copy-start | bytes 100
  27.6 32.0 %collective-permute-start.2 = (bf16[2,3,48,2048]{3,2,1,0:T(8,128)(2,1)S(1)}, bf16[2,3,48,2048]{3,2,1,0:T(8,128)(2,1)}, u32[]{:S(2)}, u32[]{:S(2)}) collective-permute-start(bf16[2,3,48,2048]{3,2,1,0:T(8,128)(2,1)S(1)} %pad_maximum_fusion.ta), channel_id=1, source_target_pairs={{0,6},{1,3},{2,4},{3,1},{4,2},{5,7},{6,0},{7,5},{8,14},{9,11},{10,... | collective-permute-start | bytes 3538952 | tf_op jit(solution)/shard_map/ppermute | solution.py:40
  38.3 8.7 %collective-permute-start.3 = (bf16[528,256]{1,0:T(8,128)(2,1)S(1)}, bf16[528,256]{1,0:T(8,128)(2,1)S(1)}, u32[]{:S(2)}, u32[]{:S(2)}) collective-permute-start(bf16[528,256]{1,0:T(8,128)(2,1)S(1)} %shard_map.148.a_ref), channel_id=1, source_target_pairs={{0,64},{1,449},{64,0},{65,129},{128,192},{129,65},{192,128},{193,2... | collective-permute-start | bytes 811016 | tf_op jit(solution)/shard_map/ppermute | solution.py:40
  47.1 17.9 %collective-permute-start.4 = (bf16[2,528,256]{2,1,0:T(8,128)(2,1)S(1)}, bf16[2,528,256]{2,1,0:T(8,128)(2,1)S(1)}, u32[]{:S(2)}, u32[]{:S(2)}) collective-permute-start(bf16[2,528,256]{2,1,0:T(8,128)(2,1)S(1)} %shard_map.149.p0), channel_id=1, source_target_pairs={{0,448},{1,65},{64,128},{65,1},{128,64},{129,193},{192,256},{193,1... | collective-permute-start | bytes 1622024 | tf_op jit(solution)/shard_map/ppermute | solution.py:40
  57.6 25.8 %collective-permute-start.6 = (bf16[2,3,48,2048]{3,2,1,0:T(8,128)(2,1)S(1)}, bf16[2,3,48,2048]{3,2,1,0:T(8,128)(2,1)}, u32[]{:S(2)}, u32[]{:S(2)}) collective-permute-start(bf16[2,3,48,2048]{3,2,1,0:T(8,128)(2,1)S(1)} %pad_maximum_fusion.ta), channel_id=1, source_target_pairs={{0,1},{1,0},{2,3},{3,2},{4,5},{5,4},{6,7},{7,6},{8,9},{9,8},{10,11... | collective-permute-start | bytes 3538952 | tf_op jit(solution)/shard_map/ppermute | solution.py:44
  59.6 23.9 %collective-permute-start.7 = (bf16[2,3,48,2048]{3,2,1,0:T(8,128)(2,1)}, bf16[2,3,48,2048]{3,2,1,0:T(8,128)(2,1)}, u32[]{:S(2)}, u32[]{:S(2)}) collective-permute-start(bf16[2,3,48,2048]{3,2,1,0:T(8,128)(2,1)} %collective-permute-done.2.tb), channel_id=1, source_target_pairs={{0,1},{1,0},{2,3},{3,2},{4,5},{5,4},{6,7},{7,6},{8,9},{9,8},{10,11... | collective-permute-start | bytes 3538952 | tf_op jit(solution)/shard_map/ppermute | solution.py:44
  65.0 11.2 %collective-permute-start.5 = (bf16[2,528,256]{2,1,0:T(8,128)(2,1)S(1)}, bf16[2,528,256]{2,1,0:T(8,128)(2,1)S(1)}, u32[]{:S(2)}, u32[]{:S(2)}) collective-permute-start(bf16[2,528,256]{2,1,0:T(8,128)(2,1)S(1)} %collective-permute-done.4.p1), channel_id=1, source_target_pairs={{0,64},{1,449},{64,0},{65,129},{128,192},{129,65},{192,128},{193,2... | collective-permute-start | bytes 1622024 | tf_op jit(solution)/shard_map/ppermute | solution.py:40
  76.2 12.4 %collective-permute-start.8 = (bf16[2,528,256]{2,1,0:T(8,128)(2,1)S(1)}, bf16[2,528,256]{2,1,0:T(8,128)(2,1)S(1)}, u32[]{:S(2)}, u32[]{:S(2)}) collective-permute-start(bf16[2,528,256]{2,1,0:T(8,128)(2,1)S(1)} %collective-permute-done.5.p2), channel_id=1, source_target_pairs={{0,448},{1,65},{64,128},{65,1},{128,64},{129,193},{192,256},{193,1... | collective-permute-start | bytes 1622024 | tf_op jit(solution)/shard_map/ppermute | solution.py:40
  93.0 31.7 %collective-permute-start.9 = (bf16[2,192,2048]{2,1,0:T(8,128)(2,1)S(1)}, bf16[2,192,2048]{2,1,0:T(8,128)(2,1)S(1)}, u32[]{:S(2)}, u32[]{:S(2)}) collective-permute-start(bf16[2,192,2048]{2,1,0:T(8,128)(2,1)S(1)} %get-tuple-element.41), channel_id=1, source_target_pairs={{0,1},{1,0},{2,3},{3,2},{4,5},{5,4},{6,7},{7,6},{8,9},{9,8},{10,11... | collective-permute-start | bytes 4718600 | tf_op jit(solution)/shard_map/ppermute | solution.py:44
  95.0 12.5 %collective-permute-start.13 = (bf16[2,528,256]{2,1,0:T(8,128)(2,1)S(1)}, bf16[2,528,256]{2,1,0:T(8,128)(2,1)S(1)}, u32[]{:S(2)}, u32[]{:S(2)}) collective-permute-start(bf16[2,528,256]{2,1,0:T(8,128)(2,1)S(1)} %get-tuple-element.51), channel_id=1, source_target_pairs={{0,448},{1,65},{64,128},{65,1},{128,64},{129,193},{192,256},{193,1... | collective-permute-start | bytes 1622024 | tf_op jit(solution)/shard_map/ppermute | solution.py:40
  107.9 11.3 %collective-permute-start.14 = (bf16[2,528,256]{2,1,0:T(8,128)(2,1)S(1)}, bf16[2,528,256]{2,1,0:T(8,128)(2,1)S(1)}, u32[]{:S(2)}, u32[]{:S(2)}) collective-permute-start(bf16[2,528,256]{2,1,0:T(8,128)(2,1)S(1)} %shard_map.158), channel_id=1, source_target_pairs={{0,64},{1,449},{64,0},{65,129},{128,192},{129,65},{192,128},{193,2... | collective-permute-start | bytes 1622024 | tf_op jit(solution)/shard_map/ppermute | solution.py:40
  119.6 12.5 %collective-permute-start.15 = (bf16[2,528,256]{2,1,0:T(8,128)(2,1)S(1)}, bf16[2,528,256]{2,1,0:T(8,128)(2,1)S(1)}, u32[]{:S(2)}, u32[]{:S(2)}) collective-permute-start(bf16[2,528,256]{2,1,0:T(8,128)(2,1)S(1)} %shard_map.159), channel_id=1, source_target_pairs={{0,448},{1,65},{64,128},{65,1},{128,64},{129,193},{192,256},{193,1... | collective-permute-start | bytes 1622024 | tf_op jit(solution)/shard_map/ppermute | solution.py:40
  125.1 14.5 %collective-permute-start.10 = (bf16[2,96,2048]{2,1,0:T(8,128)(2,1)S(1)}, bf16[2,96,2048]{2,1,0:T(8,128)(2,1)S(1)}, u32[]{:S(2)}, u32[]{:S(2)}) collective-permute-start(bf16[2,96,2048]{2,1,0:T(8,128)(2,1)S(1)} %get-tuple-element.43), channel_id=1, source_target_pairs={{0,6},{1,3},{2,4},{3,1},{4,2},{5,7},{6,0},{7,5},{8,14},{9,11},{10,... | collective-permute-start | bytes 2359304 | tf_op jit(solution)/shard_map/ppermute | solution.py:40
  132.3 12.8 %collective-permute-start.16 = (bf16[1,528,256]{2,1,0:T(8,128)(2,1)S(1)}, bf16[1,528,256]{2,1,0:T(8,128)(2,1)S(1)}, u32[]{:S(2)}, u32[]{:S(2)}) collective-permute-start(bf16[1,528,256]{2,1,0:T(8,128)(2,1)S(1)} %shard_map.161), channel_id=1, source_target_pairs={{0,64},{1,449},{64,0},{65,129},{128,192},{129,65},{192,128},{193,2... | collective-permute-start | bytes 811016 | tf_op jit(solution)/shard_map/ppermute | solution.py:40
  139.7 10.7 %collective-permute-start.11 = (bf16[2,48,2048]{2,1,0:T(8,128)(2,1)S(1)}, bf16[2,48,2048]{2,1,0:T(8,128)(2,1)S(1)}, u32[]{:S(2)}, u32[]{:S(2)}) collective-permute-start(bf16[2,48,2048]{2,1,0:T(8,128)(2,1)S(1)} %get-tuple-element.45), channel_id=1, source_target_pairs={{0,2},{1,7},{2,0},{3,5},{4,6},{5,3},{6,4},{7,1},{8,10},{9,15},{10,... | collective-permute-start | bytes 1179656 | tf_op jit(solution)/shard_map/ppermute | solution.py:40
  146.0 14.8 %copy-start.4 = (f32[32,352]{1,0:T(8,128)S(1)}, f32[32,352]{1,0:T(8,128)}, u32[]{:S(2)}) copy-start(f32[32,352]{1,0:T(8,128)} %gs.1) | copy-start | bytes 135172
  146.0 14.8 %copy-start.5 = (f32[32,352]{1,0:T(8,128)S(1)}, f32[32,352]{1,0:T(8,128)}, u32[]{:S(2)}) copy-start(f32[32,352]{1,0:T(8,128)} %us.1) | copy-start | bytes 135172
  146.0 14.8 %copy-start.6 = (f32[32,352]{1,0:T(8,128)S(1)}, f32[32,352]{1,0:T(8,128)}, u32[]{:S(2)}) copy-start(f32[32,352]{1,0:T(8,128)} %ds.1) | copy-start | bytes 135172
  146.0 15.6 %copy-start = (bf16[24,2048]{1,0:T(8,128)(2,1)S(1)}, bf16[24,2048]{1,0:T(8,128)(2,1)}, u32[]{:S(2)}) copy-start(bf16[24,2048]{1,0:T(8,128)(2,1)} %e_ref.1) | copy-start | bytes 294916
  146.0 15.6 %copy-start.1 = (bf16[24,2048]{1,0:T(8,128)(2,1)S(1)}, bf16[24,2048]{1,0:T(8,128)(2,1)}, u32[]{:S(2)}) copy-start(bf16[24,2048]{1,0:T(8,128)(2,1)} %c_ref.1) | copy-start | bytes 294916
  146.0 15.6 %copy-start.2 = (bf16[24,2048]{1,0:T(8,128)(2,1)S(1)}, bf16[24,2048]{1,0:T(8,128)(2,1)}, u32[]{:S(2)}) copy-start(bf16[24,2048]{1,0:T(8,128)(2,1)} %l_ref.1) | copy-start | bytes 294916
  146.0 15.6 %copy-start.3 = (bf16[1,2048]{1,0:T(2,128)(2,1)S(1)}, bf16[1,2048]{1,0:T(2,128)(2,1)}, u32[]{:S(2)}) copy-start(bf16[1,2048]{1,0:T(2,128)(2,1)} %reshape.13.g_hbm.g_ref) | copy-start | bytes 12292
  146.1 14.8 %all-to-all-start.1 = ((bf16[8,32,640]{2,1,0:T(8,128)(2,1)}), bf16[8,32,640]{2,1,0:T(8,128)(2,1)S(1)}, u32[]{:S(2)}, u32[]{:S(2)}) async-start(bf16[8,32,640]{2,1,0:T(8,128)(2,1)} %shard_map.162), calls=%async_computation.1 | async-start | bytes 655360 | tf_op jit(solution)/shard_map/all_to_all | solution.py:48
  150.5 11.1 %collective-permute-start.12 = (bf16[2,24,2048]{2,1,0:T(8,128)(2,1)S(1)}, bf16[2,24,2048]{2,1,0:T(8,128)(2,1)S(1)}, u32[]{:S(2)}, u32[]{:S(2)}) collective-permute-start(bf16[2,24,2048]{2,1,0:T(8,128)(2,1)S(1)} %get-tuple-element.47), channel_id=1, source_target_pairs={{0,8},{8,0},{1,9},{9,1},{2,10},{10,2},{3,11},{11,3},{4,12},{12,4},... | collective-permute-start | bytes 589832 | tf_op jit(solution)/shard_map/ppermute | solution.py:44
where the time goes:
time: 163 us; the launch traced here: 162 us
  starting transfers between devices  72.3 us (44%)
  waiting for transfers between devices  71.2 us (44%)
  Pallas kernels  16.3 us (10%)
    ppermute x12, starting transfers between devices, exchange(): return lax.ppermute(x, (axis, 'c'), pairs)  52.1 us
    ppermute x12, waiting for transfers between devices, exchange(): return lax.ppermute(x, (axis, 'c'), pairs)  48.2 us
    pallas_call x18, Pallas kernels, call(): pl.pallas_call(body, out_shape=out_shape, compiler_params=pltpu.CompilerP...  16.3 us
    all_to_all x2, waiting for transfers between devices, over_y(): lax.all_to_all(x, ('yq', 'ys'), split_axis=0, concat_axis=0, tiled=True)  15.9 us
    ppermute x5, starting transfers between devices, swapped(): return lax.ppermute(x, axis, [(0, 1), (1, 0)])  12.8 us
    all_to_all x2, starting transfers between devices, over_y(): lax.all_to_all(x, ('yq', 'ys'), split_axis=0, concat_axis=0, tiled=True)  7.37 us
    ppermute x5, waiting for transfers between devices, swapped(): return lax.ppermute(x, axis, [(0, 1), (1, 0)])  7.16 us
  transfers between devices with their start and end apart: 19, of which 13 were waited for; matrix products, arithmetic and copies ran while one was open for 0% of the time, Pallas kernels for 6%

commit v1 on v0

--- a/solution.py
+++ b/solution.py
@@ -19,7 +19,7 @@
 HALF = 176
 MAIN = 128
 TAIL = 48
-LANES = 640
+PACK = 136
 
 
 def call(body, out_shape, *args, mib=16, **kw):
@@ -40,6 +40,15 @@
     return lax.ppermute(x, (axis, "c"), pairs)
 
 
+def hop_two(x):
+    pairs = []
+    for i in range(NZ):
+        for c in range(NC):
+            j = (i - 2) % NZ if (i + c) % 2 == 0 else (i + 2) % NZ
+            pairs.append((i * NC + c, j * NC + c))
+    return lax.ppermute(x, ("z", "c"), pairs)
+
+
 def swapped(x, axis):
     return lax.ppermute(x, axis, [(0, 1), (1, 0)])
 
@@ -56,8 +65,26 @@
     return lax.dot_general(left, right, (((1,), (0,)), ((), ())), preferred_element_type=f32)
 
 
-def lanes_below(n):
-    return lax.broadcasted_iota(jnp.int32, (ROWS, 128), 1) < n
+def pick(*parts):
+    out = parts[-1][1]
+    lane = lax.broadcasted_iota(jnp.int32, out.shape, out.ndim - 1)
+    for bound, part in reversed(parts[:-1]):
+        out = jnp.where(lane < bound, part, out)
+    return out
+
+
+def shift(x, by):
+    return pltpu.roll(x, by % 128, x.ndim - 1)
+
+
+def fold_rows(x, start, axis):
+    rows = [lax.slice_in_dim(x, 8 * j, 8 * j + 8, axis=axis) for j in range(4)]
+    rows = [(16 * j + 16, shift(r, 16 * j - start)) for j, r in enumerate(rows)]
+    return pick(*rows, (128, jnp.zeros_like(rows[0][1])))
+
+
+def unfold_rows(x, axis):
+    return jnp.concatenate([shift(x, -16 * j) for j in range(4)], axis=axis)
 
 
 def fetch(pairs, sem):
@@ -68,47 +95,48 @@
         copy.wait()
 
 
-def pack_weights(g_hbm, u_hbm, d_hbm, o_ref, g_ref, u_ref, d_ref, sem):
-    fetch(((g_hbm, g_ref), (u_hbm, u_ref), (d_hbm, d_ref)), sem)
-    last = []
-    for r in (g_ref, u_ref, d_ref):
-        r = r[...].astype(f32)
-        last.append(jnp.concatenate([r[:, 256:352], jnp.zeros((ROWS, 32), f32)], axis=1))
-    g, u, d = last
-    for h in range(2):
-        if h == 0:
-            t3 = jnp.where(lanes_below(48), g, pltpu.roll(u, 48, 1))
-            t4 = d
-        else:
-            t3 = jnp.where(lanes_below(48), pltpu.roll(g, 80, 1), u)
-            t4 = pltpu.roll(d, 80, 1)
-        t3 = jnp.where(lanes_below(96), t3, 0.0).astype(bf16)
-        t4 = jnp.where(lanes_below(48), t4, 0.0).astype(bf16)
-        for q in range(4):
-            for i, r in enumerate((g_ref, u_ref, d_ref)):
-                o_ref[2 * q + h, :, MAIN * i : MAIN * (i + 1)] = r[:, h * MAIN : (h + 1) * MAIN]
-            o_ref[2 * q + h, :, 384:512] = t3
-            o_ref[2 * q + h, :, 512:640] = t4
-
-
 def normalize(x, gain):
     inv = lax.rsqrt(jnp.mean(x * x, axis=-1, keepdims=True) + eps)
     return inv, x * inv * gain
 
 
-def prepare_tokens(e_hbm, c_hbm, l_hbm, g_hbm, o_ref, e_ref, c_ref, l_ref, g_ref, sem):
-    fetch(((e_hbm, e_ref), (c_hbm, c_ref), (l_hbm, l_ref), (g_hbm, g_ref)), sem)
-    gain = g_ref[...].astype(f32)
-    o_ref[0] = normalize(e_ref[...].astype(f32), gain)[1].astype(bf16)
-    o_ref[1] = (0.5 * c_ref[...].astype(f32)).astype(bf16)
-    o_ref[2] = normalize(l_ref[...].astype(f32), gain)[1].astype(bf16)
+def pack_weights(g_hbm, u_hbm, d_hbm, o_ref, g_ref, u_ref, d_ref, sem):
+    fetch(((g_hbm, g_ref), (u_hbm, u_ref), (d_hbm, d_ref)), sem)
+    weights = (g_ref, u_ref, d_ref)
+    tails = []
+    for r in weights:
+        tail = r[:, 256:352].astype(f32)
+        tails.append(jnp.concatenate([tail, jnp.zeros((ROWS, 32), f32)], axis=1))
+    g, u, d = tails
+    for h in range(2):
+        at = h * TAIL
+        tail = pick((48, shift(g, -at)), (96, shift(u, 48 - at)), (128, shift(d, 96 - at)))
+        rest = fold_rows(d, at + 32, 0)
+        for q in range(4):
+            for i, r in enumerate(weights):
+                o_ref[2 * q + h, ROWS * i : ROWS * (i + 1)] = r[:, h * MAIN : (h + 1) * MAIN]
+            o_ref[2 * q + h, 96:128] = tail.astype(bf16)
+            o_ref[2 * q + h, 128:136] = rest.astype(bf16)
+
+
+def prepare_tokens(e_hbm, c_hbm, l_hbm, g_hbm, o_ref, early, cot, late, gain, sem):
+    fetch(((e_hbm, early), (c_hbm, cot), (l_hbm, late), (g_hbm, gain)), sem)
+    gain = gain[...].astype(f32).reshape(1, 2048)
+    o_ref[0] = normalize(early[...].astype(f32), gain)[1].astype(bf16)
+    o_ref[1] = (0.5 * cot[...].astype(f32)).astype(bf16)
+    o_ref[2] = normalize(late[...].astype(f32), gain)[1].astype(bf16)
 
 
 def turn_block(r_ref, o_ref):
-    t = r_ref[...].reshape(NY * ROWS, LANES).T
-    for i, at in enumerate((384, 432, 512)):
-        o_ref[HALF * i : HALF * i + MAIN] = t[MAIN * i : MAIN * (i + 1)]
-        o_ref[HALF * i + MAIN : HALF * (i + 1)] = t[at : at + TAIL]
+    tiles = [r_ref[:, 32 * i : 32 * (i + 1)].reshape(NY * ROWS, 128).T for i in range(4)]
+    rest = unfold_rows(r_ref[:, 128:136].astype(f32), 1).reshape(NY * ROWS, 128).T
+    for i in range(3):
+        o_ref[HALF * i : HALF * i + MAIN] = tiles[i]
+    tail = tiles[3]
+    o_ref[128:176] = tail[0:48]
+    o_ref[304:352] = tail[48:96]
+    o_ref[480:512] = tail[96:128]
+    o_ref[512:528] = rest[0:16].astype(bf16)
 
 
 def join(a_ref, b_ref, o_ref):
@@ -117,13 +145,11 @@
 
 
 def turned(f):
-    zero = jnp.zeros((32, 256), f.dtype)
-    return jnp.concatenate(
-        [f[HALF * i : HALF * i + MAIN] for i in range(3)]
-        + [f[HALF * i + MAIN : HALF * (i + 1)] for i in range(2)]
-        + [zero, f[2 * HALF + MAIN : 3 * HALF], zero, zero, zero[:16]],
-        axis=0,
-    ).T
+    parts = [f[HALF * i : HALF * i + MAIN] for i in range(3)]
+    parts.append(jnp.concatenate([f[128:176], f[304:352], f[480:512]], axis=0))
+    parts.append(jnp.concatenate([f[512:528], jnp.zeros((112, 256), f.dtype)], axis=0))
+    parts = [p.T.reshape(NY, ROWS, 128).astype(f32) for p in parts]
+    return jnp.concatenate([*parts[:4], fold_rows(parts[4], 0, 1)], axis=1)
 
 
 def forward_part(b_ref, ta, tb, p0, p1, p2, te, th, tl, acc, w):
@@ -182,18 +208,23 @@
         grad_block(at_ref, (te0, te1), (th0, th1), k + n, o_ref, n, r_ref[n])
 
 
-def add_second(at_ref, te0, te1, th0, th1, r_ref, o_ref):
-    grad_block(at_ref, (te0, te1), (th0, th1), 1, o_ref, 0, r_ref[1])
-
-
-def own_block(at_ref, te0, te1, th0, th1, r_ref, o_ref, f):
-    grad_block(at_ref, (te0, te1), (th0, th1), 0, f, 0, r_ref[0])
+def add_each(at_ref, te0, te1, th0, th1, r_ref, o_ref, p_ref):
+    for n, o in enumerate((o_ref, p_ref)):
+        grad_block(at_ref, (te0, te1), (th0, th1), 2 + n, o, 0, r_ref[n])
+
+
+def neighbour_share(at_ref, te0, te1, th0, th1, o_ref):
+    grad_block(at_ref, (te0, te1), (th0, th1), 1, o_ref, 0)
+
+
+def own_block(at_ref, te0, te1, th0, th1, r_ref, q_ref, o_ref, f):
+    both = r_ref[0].astype(f32) + q_ref[0].astype(f32)
+    grad_block(at_ref, (te0, te1), (th0, th1), 0, f, 0, both)
     o_ref[...] = turned(f[0])
 
 
 def last_block(f_ref, r_ref, o_ref):
-    t = f_ref[...] + turned(r_ref[0]).astype(f32)
-    o_ref[...] = t.reshape(NY, ROWS, LANES).astype(bf16)
+    o_ref[...] = (f_ref[...] + turned(r_ref[0])).astype(bf16)
 
 
 def token_parts(b_ref, dg_ref, du_ref, tl0, tl1, p0, p1, p2, p3, near, far, w):
@@ -241,16 +272,15 @@
         for q in range(1, 4):
             t = t + r_ref[2 * q + h].astype(f32)
         total.append(t)
-    t3 = [t[:, 384:512] for t in total]
-    t4 = [t[:, 512:640] for t in total]
-    low = lanes_below(48)
-    g2 = jnp.where(low, t3[0], pltpu.roll(t3[1], 48, 1))
-    u2 = jnp.where(low, pltpu.roll(t3[0], 80, 1), t3[1])
-    d2 = jnp.where(low, t4[0], pltpu.roll(t4[1], 48, 1))
+    t = [t[96:128] for t in total]
+    r = [unfold_rows(t[128:136], 0) for t in total]
+    g2 = pick((48, t[0]), (128, shift(t[1], 48)))
+    u2 = pick((48, shift(t[0], -48)), (128, t[1]))
+    d2 = pick((32, shift(t[0], 32)), (48, shift(r[0], 32)), (80, shift(t[1], 80)), (128, shift(r[1], 80)))
     for i, (s, o, t2) in enumerate(((gs, go, g2), (us, uo, u2), (ds, do, d2))):
         for h in range(2):
             cols = slice(h * MAIN, (h + 1) * MAIN)
-            o[:, cols] = s[:, cols] + total[h][:, i * MAIN : (i + 1) * MAIN]
+            o[:, cols] = s[:, cols] + total[h][ROWS * i : ROWS * (i + 1)]
         o[:, 256:352] = s[:, 256:352] + t2[:, :96]
 
 
@@ -281,29 +311,27 @@
     order = jnp.array([0, 1, -1, -2, 2, 3, -3, -4], jnp.int32)
     blocks = lax.rem(z + order * step + 8, 8).astype(jnp.int32)
 
-    sent = call(
-        pack_weights,
-        shape((NY, ROWS, LANES)),
-        *(pltpu.with_memory_space_constraint(w, pltpu.HBM) for w in (gate_weight, up_weight, down_weight)),
-        in_specs=[HB] * 3,
-        scratch_shapes=[pltpu.VMEM((ROWS, 352), bf16)] * 3 + [pltpu.SemaphoreType.DMA((3,))],
-    )
+    def staged(body, dims, *given):
+        n = len(given)
+        return call(
+            body,
+            shape(dims),
+            *(pltpu.with_memory_space_constraint(a, pltpu.HBM) for a in given),
+            in_specs=[HB] * n,
+            scratch_shapes=[pltpu.VMEM(a.shape, bf16) for a in given]
+            + [pltpu.SemaphoreType.DMA((n,))],
+        )
+
+    sent = staged(pack_weights, (NY, PACK, 128), gate_weight, up_weight, down_weight)
+    tok = staged(prepare_tokens, (3, 24, 2048), x_early, cotangent, x_late, norm_gain)
     own = call(turn_block, shape((3 * HALF, 256)), over_y(sent))
     p0 = call(join, shape((2, 3 * HALF, 256)), own, exchange(own, "z", NZ, 0))
     p1 = exchange(p0, "z", NZ, 1)
     p2 = exchange(p1, "z", NZ, 0)
     p3 = exchange(p2, "z", NZ, 1)
 
-    tok = call(
-        prepare_tokens,
-        shape((3, 24, 2048)),
-        *(pltpu.with_memory_space_constraint(x, pltpu.HBM) for x in (x_early, cotangent, x_late, gain)),
-        in_specs=[HB] * 4,
-        scratch_shapes=[pltpu.VMEM((24, 2048), bf16)] * 3
-        + [pltpu.VMEM((1, 2048), bf16), pltpu.SemaphoreType.DMA((4,))],
-    )
-    t0 = jnp.concatenate([tok, swapped(tok, "ys")], axis=1)
-    ta = jnp.stack([t0, exchange(t0, "x", NX, 0)])
+    t0 = jnp.concatenate([tok, exchange(tok, "x", NX, 0)], axis=1)
+    ta = jnp.stack([t0, swapped(t0, "ys")])
     tb = exchange(ta, "x", NX, 1)
     tc = swapped(ta, "c")
     td = swapped(tb, "c")
@@ -337,17 +365,18 @@
     )
     s2 = call(functools.partial(add_pair, 4), pair, *tokens, r3)
     r2 = exchange(s2, "z", NZ, 0)
-    s1 = call(functools.partial(add_pair, 2), pair, *tokens, r2)
+    one = shape((1, 3 * HALF, 256))
+    mine = exchange(call(neighbour_share, one, *tokens), "z", NZ, 0)
+    s1, s0 = call(add_each, (one, one), *tokens, r2)
+    r0 = hop_two(s0)
     r1 = exchange(s1, "z", NZ, 1)
-    s0 = call(add_second, shape((1, 3 * HALF, 256)), *tokens, r1)
-    r0 = exchange(s0, "z", NZ, 0)
     block = call(
         own_block,
-        shape((256, LANES), f32),
-        *tokens, r1,
+        shape((NY, PACK, 128), f32),
+        *tokens, mine, r1,
         scratch_shapes=[pltpu.VMEM((1, 3 * HALF, 256), f32)],
     )
-    back = call(last_block, shape((NY, ROWS, LANES)), block, r0)
+    back = call(last_block, shape((NY, PACK, 128)), block, r0)
     sums = call(
         finish_weights,
         (shape((ROWS, 352), f32),) * 3,
@@ -360,11 +389,11 @@
 
     near, far = folded(near, swapped(far, "c"))
     near, far = folded(near, exchange(far, "x", NX, 1))
-    near, far = folded(near, exchange(far, "x", NX, 0))
+    near, far = folded(near, swapped(far, "ys"))
     late, early = call(
         finish_tokens,
         (shape((24, 2048)),) * 2,
-        near, swapped(far, "ys"), x_early, cotangent, x_late, gain,
+        near, exchange(far, "x", NX, 0), x_early, cotangent, x_late, gain,
     )
     return (late, early, *sums)
 

time: 163 us -> 152 us (0.933)
  the two profiles are of different devices: /device:TPU:2 before, /device:TPU:64 now
where the time goes in v1:
time: 152 us; the launch traced here: 151 us
  starting transfers between devices  74.3 us (49%)
  waiting for transfers between devices  59.2 us (39%)
  Pallas kernels  16.6 us (11%)
    ppermute x12, starting transfers between devices, exchange(): return lax.ppermute(x, (axis, 'c'), pairs)  44.4 us
    ppermute x12, waiting for transfers between devices, exchange(): return lax.ppermute(x, (axis, 'c'), pairs)  34.4 us
    pallas_call x18, Pallas kernels, call(): pl.pallas_call(body, out_shape=out_shape, compiler_params=pltpu.CompilerP...  16.6 us
    ppermute x5, starting transfers between devices, swapped(): return lax.ppermute(x, axis, [(0, 1), (1, 0)])  13 us
    all_to_all x2, starting transfers between devices, over_y(): lax.all_to_all(x, ('yq', 'ys'), split_axis=0, concat_axis=0, tiled=True)  10.7 us
    all_to_all x2, waiting for transfers between devices, over_y(): lax.all_to_all(x, ('yq', 'ys'), split_axis=0, concat_axis=0, tiled=True)  9.92 us
    ppermute x5, waiting for transfers between devices, swapped(): return lax.ppermute(x, axis, [(0, 1), (1, 0)])  9.88 us
    ppermute x1, starting transfers between devices, hop_two(): return lax.ppermute(x, ('z', 'c'), pairs)  6.18 us
  transfers between devices with their start and end apart: 20, of which 14 were waited for; matrix products, arithmetic and copies ran while one was open for 0% of the time, Pallas kernels for 7%

profile of v1, /device:TPU:64, one launch (start us, length us, event | category | flops | bytes accessed | tf_op | source)
XLA Modules:
  0.0 151.3 jit_solution(6826275237399016460)
XLA Ops:
  1.8 3.4 %collective-permute-start = (bf16[3,24,2048]{2,1,0:T(8,128)(2,1)S(1)}, bf16[3,24,2048]{2,1,0:T(8,128)(2,1)S(1)}, u32[]{:S(2)}, u32[]{:S(2)}) collective-permute-start(bf16[3,24,2048]{2,1,0:T(8,128)(2,1)S(1)} %shard_map.146), channel_id=1, source_target_pairs={{0,2},{1,7},{2,0},{3,5},{4,6},{5,3},{6,4},{7,1},{8,10},{9,15},{10,... | collective-permute-start | bytes 884744 | tf_op jit(solution)/shard_map/ppermute | solution.py:40
  5.2 5.2 %collective-permute-done = bf16[3,24,2048]{2,1,0:T(8,128)(2,1)S(1)} collective-permute-done((bf16[3,24,2048]{2,1,0:T(8,128)(2,1)S(1)}, bf16[3,24,2048]{2,1,0:T(8,128)(2,1)S(1)}, u32[]{:S(2)}, u32[]{:S(2)}) %collective-permute-start) | collective-permute-done | bytes 294944 | tf_op jit(solution)/shard_map/ppermute | solution.py:40
  10.6 3.5 %collective-permute-start.1 = (bf16[3,48,2048]{2,1,0:T(8,128)(2,1)S(1)}, bf16[3,48,2048]{2,1,0:T(8,128)(2,1)S(1)}, u32[]{:S(2)}, u32[]{:S(2)}) collective-permute-start(bf16[3,48,2048]{2,1,0:T(8,128)(2,1)S(1)} %get-tuple-element.60), channel_id=1, source_target_pairs={{0,8},{8,0},{1,9},{9,1},{2,10},{10,2},{3,11},{11,3},{4,12},{12,4},... | collective-permute-start | bytes 1769480 | tf_op jit(solution)/shard_map/ppermute | solution.py:53
  15.7 6.2 %all-to-all-start = ((bf16[8,136,128]{2,1,0:T(8,128)(2,1)}), bf16[8,136,128]{2,1,0:T(8,128)(2,1)S(1)}, u32[]{:S(2)}, u32[]{:S(2)}) async-start(bf16[8,136,128]{2,1,0:T(8,128)(2,1)} %shard_map.147), calls=%async_computation | async-start | bytes 557056 | tf_op jit(solution)/shard_map/all_to_all | solution.py:57
  21.9 8.3 %collective-permute-done.1 = bf16[3,48,2048]{2,1,0:T(8,128)(2,1)S(1)} collective-permute-done((bf16[3,48,2048]{2,1,0:T(8,128)(2,1)S(1)}, bf16[3,48,2048]{2,1,0:T(8,128)(2,1)S(1)}, u32[]{:S(2)}, u32[]{:S(2)}) %collective-permute-start.1) | collective-permute-done | bytes 589856 | tf_op jit(solution)/shard_map/ppermute | solution.py:53
  30.3 4.7 %collective-permute-start.2 = (bf16[2,3,48,2048]{3,2,1,0:T(8,128)(2,1)S(1)}, bf16[2,3,48,2048]{3,2,1,0:T(8,128)(2,1)}, u32[]{:S(2)}, u32[]{:S(2)}) collective-permute-start(bf16[2,3,48,2048]{3,2,1,0:T(8,128)(2,1)S(1)} %pad_maximum_fusion.ta), channel_id=1, source_target_pairs={{0,6},{1,3},{2,4},{3,1},{4,2},{5,7},{6,0},{7,5},{8,14},{9,11},{10,... | collective-permute-start | bytes 3538952 | tf_op jit(solution)/shard_map/ppermute | solution.py:40
  34.9 2.7 %all-to-all-done.r_ref = bf16[8,136,128]{2,1,0:T(8,128)(2,1)S(1)} async-done(((bf16[8,136,128]{2,1,0:T(8,128)(2,1)}), bf16[8,136,128]{2,1,0:T(8,128)(2,1)S(1)}, u32[]{:S(2)}, u32[]{:S(2)}) %all-to-all-start) | async-done | bytes 278560 | tf_op jit(solution)/shard_map/all_to_all | solution.py:57
  37.8 1.9 %collective-permute-start.3 = (bf16[528,256]{1,0:T(8,128)(2,1)S(1)}, bf16[528,256]{1,0:T(8,128)(2,1)S(1)}, u32[]{:S(2)}, u32[]{:S(2)}) collective-permute-start(bf16[528,256]{1,0:T(8,128)(2,1)S(1)} %shard_map.148.a_ref), channel_id=1, source_target_pairs={{0,64},{1,449},{64,0},{65,129},{128,192},{129,65},{192,128},{193,2... | collective-permute-start | bytes 811016 | tf_op jit(solution)/shard_map/ppermute | solution.py:40
  39.8 6.4 %collective-permute-done.3.b_ref = bf16[528,256]{1,0:T(8,128)(2,1)S(1)} collective-permute-done((bf16[528,256]{1,0:T(8,128)(2,1)S(1)}, bf16[528,256]{1,0:T(8,128)(2,1)S(1)}, u32[]{:S(2)}, u32[]{:S(2)}) %collective-permute-start.3) | collective-permute-done | bytes 270368 | tf_op jit(solution)/shard_map/ppermute | solution.py:40
  46.2 4.6 %collective-permute-start.4 = (bf16[2,528,256]{2,1,0:T(8,128)(2,1)S(1)}, bf16[2,528,256]{2,1,0:T(8,128)(2,1)S(1)}, u32[]{:S(2)}, u32[]{:S(2)}) collective-permute-start(bf16[2,528,256]{2,1,0:T(8,128)(2,1)S(1)} %shard_map.149.p0), channel_id=1, source_target_pairs={{0,448},{1,65},{64,128},{65,1},{128,64},{129,193},{192,256},{193,1... | collective-permute-start | bytes 1622024 | tf_op jit(solution)/shard_map/ppermute | solution.py:40
  50.9 2.8 %collective-permute-start.6 = (bf16[2,3,48,2048]{3,2,1,0:T(8,128)(2,1)S(1)}, bf16[2,3,48,2048]{3,2,1,0:T(8,128)(2,1)}, u32[]{:S(2)}, u32[]{:S(2)}) collective-permute-start(bf16[2,3,48,2048]{3,2,1,0:T(8,128)(2,1)S(1)} %pad_maximum_fusion.ta), channel_id=1, source_target_pairs={{0,1},{1,0},{2,3},{3,2},{4,5},{5,4},{6,7},{7,6},{8,9},{9,8},{10,11... | collective-permute-start | bytes 3538952 | tf_op jit(solution)/shard_map/ppermute | solution.py:53
  53.7 1.9 %collective-permute-start.7 = (bf16[2,3,48,2048]{3,2,1,0:T(8,128)(2,1)}, bf16[2,3,48,2048]{3,2,1,0:T(8,128)(2,1)}, u32[]{:S(2)}, u32[]{:S(2)}) collective-permute-start(bf16[2,3,48,2048]{3,2,1,0:T(8,128)(2,1)} %collective-permute-done.2.tb), channel_id=1, source_target_pairs={{0,1},{1,0},{2,3},{3,2},{4,5},{5,4},{6,7},{7,6},{8,9},{9,8},{10,11... | collective-permute-start | bytes 3538952 | tf_op jit(solution)/shard_map/ppermute | solution.py:53
  55.6 2.6 %collective-permute-done.4.p1 = bf16[2,528,256]{2,1,0:T(8,128)(2,1)S(1)} collective-permute-done((bf16[2,528,256]{2,1,0:T(8,128)(2,1)S(1)}, bf16[2,528,256]{2,1,0:T(8,128)(2,1)S(1)}, u32[]{:S(2)}, u32[]{:S(2)}) %collective-permute-start.4) | collective-permute-done | bytes 540704 | tf_op jit(solution)/shard_map/ppermute | solution.py:40
  58.2 7.9 %collective-permute-start.5 = (bf16[2,528,256]{2,1,0:T(8,128)(2,1)S(1)}, bf16[2,528,256]{2,1,0:T(8,128)(2,1)S(1)}, u32[]{:S(2)}, u32[]{:S(2)}) collective-permute-start(bf16[2,528,256]{2,1,0:T(8,128)(2,1)S(1)} %collective-permute-done.4.p1), channel_id=1, source_target_pairs={{0,64},{1,449},{64,0},{65,129},{128,192},{129,65},{192,128},{193,2... | collective-permute-start | bytes 1622024 | tf_op jit(solution)/shard_map/ppermute | solution.py:40
  66.1 7.3 %collective-permute-done.5.p2 = bf16[2,528,256]{2,1,0:T(8,128)(2,1)S(1)} collective-permute-done((bf16[2,528,256]{2,1,0:T(8,128)(2,1)S(1)}, bf16[2,528,256]{2,1,0:T(8,128)(2,1)S(1)}, u32[]{:S(2)}, u32[]{:S(2)}) %collective-permute-start.5) | collective-permute-done | bytes 540704 | tf_op jit(solution)/shard_map/ppermute | solution.py:40
  75.3 2.1 %shard_map.150 = (bf16[192,2048]{1,0:T(8,128)(2,1)S(1)}, bf16[192,2048]{1,0:T(8,128)(2,1)S(1)}, bf16[192,2048]{1,0:T(8,128)(2,1)S(1)}, f32[3,192,176]{2,1,0:T(8,128)S(1)}) custom-call(s32[8]{0:T(128)S(1)} %compare_select_fusion.b_ref, bf16[2,3,48,2048]{3,2,1,0:T(8,128)(2,1)S(1)} %pad_maximum_fusion.ta, bf16[2,3,48,2048]{3,2,1,0:T(8,128)(2,1)} %collective-permute-done.2.tb, ...), custom_call_target="tpu_custom_call" | custom-call | tf_op jit(solution)/shard_map/pallas_call | solution.py:26
  77.4 2.4 %shard_map.151 = (bf16[192,2048]{1,0:T(8,128)(2,1)S(1)}, bf16[192,2048]{1,0:T(8,128)(2,1)S(1)}, bf16[192,2048]{1,0:T(8,128)(2,1)S(1)}, f32[3,192,176]{2,1,0:T(8,128)S(1)}) custom-call(s32[8]{0:T(128)S(1)} %compare_select_fusion.b_ref, bf16[2,3,48,2048]{3,2,1,0:T(8,128)(2,1)} %collective-permute-done.6.ta, ...), custom_call_target="tpu_custom_call" | custom-call | tf_op jit(solution)/shard_map/pallas_call | solution.py:26
  79.9 4.8 %collective-permute-done.8.p3 = bf16[2,528,256]{2,1,0:T(8,128)(2,1)S(1)} collective-permute-done((bf16[2,528,256]{2,1,0:T(8,128)(2,1)S(1)}, bf16[2,528,256]{2,1,0:T(8,128)(2,1)S(1)}, u32[]{:S(2)}, u32[]{:S(2)}) %collective-permute-start.8) | collective-permute-done | bytes 540704 | tf_op jit(solution)/shard_map/ppermute | solution.py:40
  85.7 3.3 %shard_map.153 = (f32[2,192,2048]{2,1,0:T(8,128)S(1)}, bf16[2,192,2048]{2,1,0:T(8,128)(2,1)S(1)}) custom-call(s32[8]{0:T(128)S(1)} %compare_select_fusion.b_ref, bf16[2,192,176]{2,1,0:T(8,128)(2,1)S(1)} %get-tuple-element.38.dg_ref, bf16[2,192,176]{2,1,0:T(8,128)(2,1)S(1)} %get-tuple-element.39.du_ref, bf16[192,2048]{1,0:T(8,128)(2,1)S(1)} %get-tuple-element.40.tl0, ...), custom_call_target="tpu_custom_call" | custom-call | tf_op jit(solution)/shard_map/pallas_call | solution.py:26
  89.0 1.9 %collective-permute-start.9 = (bf16[2,192,2048]{2,1,0:T(8,128)(2,1)S(1)}, bf16[2,192,2048]{2,1,0:T(8,128)(2,1)S(1)}, u32[]{:S(2)}, u32[]{:S(2)}) collective-permute-start(bf16[2,192,2048]{2,1,0:T(8,128)(2,1)S(1)} %get-tuple-element.43), channel_id=1, source_target_pairs={{0,1},{1,0},{2,3},{3,2},{4,5},{5,4},{6,7},{7,6},{8,9},{9,8},{10,11... | collective-permute-start | bytes 4718600 | tf_op jit(solution)/shard_map/ppermute | solution.py:53
  94.7 4.7 %collective-permute-start.10 = (bf16[2,96,2048]{2,1,0:T(8,128)(2,1)S(1)}, bf16[2,96,2048]{2,1,0:T(8,128)(2,1)S(1)}, u32[]{:S(2)}, u32[]{:S(2)}) collective-permute-start(bf16[2,96,2048]{2,1,0:T(8,128)(2,1)S(1)} %get-tuple-element.45), channel_id=1, source_target_pairs={{0,6},{1,3},{2,4},{3,1},{4,2},{5,7},{6,0},{7,5},{8,14},{9,11},{10,... | collective-permute-start | bytes 2359304 | tf_op jit(solution)/shard_map/ppermute | solution.py:40
  99.3 2.8 %collective-permute-done.14.r_ref = bf16[2,528,256]{2,1,0:T(8,128)(2,1)S(1)} collective-permute-done((bf16[2,528,256]{2,1,0:T(8,128)(2,1)S(1)}, bf16[2,528,256]{2,1,0:T(8,128)(2,1)S(1)}, u32[]{:S(2)}, u32[]{:S(2)}) %collective-permute-start.14) | collective-permute-done | bytes 540704 | tf_op jit(solution)/shard_map/ppermute | solution.py:40
  102.6 6.4 %collective-permute-start.15 = (bf16[2,528,256]{2,1,0:T(8,128)(2,1)S(1)}, bf16[2,528,256]{2,1,0:T(8,128)(2,1)S(1)}, u32[]{:S(2)}, u32[]{:S(2)}) collective-permute-start(bf16[2,528,256]{2,1,0:T(8,128)(2,1)S(1)} %shard_map.159), channel_id=1, source_target_pairs={{0,64},{1,449},{64,0},{65,129},{128,192},{129,65},{192,128},{193,2... | collective-permute-start | bytes 1622024 | tf_op jit(solution)/shard_map/ppermute | solution.py:40
  109.3 1.9 %collective-permute-start.13 = (bf16[1,528,256]{2,1,0:T(8,128)(2,1)S(1)}, bf16[1,528,256]{2,1,0:T(8,128)(2,1)S(1)}, u32[]{:S(2)}, u32[]{:S(2)}) collective-permute-start(bf16[1,528,256]{2,1,0:T(8,128)(2,1)S(1)} %shard_map.158), channel_id=1, source_target_pairs={{0,64},{1,449},{64,0},{65,129},{128,192},{129,65},{192,128},{193,2... | collective-permute-start | bytes 811016 | tf_op jit(solution)/shard_map/ppermute | solution.py:40
  111.2 5.1 %collective-permute-done.15.r_ref = bf16[2,528,256]{2,1,0:T(8,128)(2,1)S(1)} collective-permute-done((bf16[2,528,256]{2,1,0:T(8,128)(2,1)S(1)}, bf16[2,528,256]{2,1,0:T(8,128)(2,1)S(1)}, u32[]{:S(2)}, u32[]{:S(2)}) %collective-permute-start.15) | collective-permute-done | bytes 540704 | tf_op jit(solution)/shard_map/ppermute | solution.py:40
  116.8 1.9 %collective-permute-start.16 = (bf16[1,528,256]{2,1,0:T(8,128)(2,1)S(1)}, bf16[1,528,256]{2,1,0:T(8,128)(2,1)S(1)}, u32[]{:S(2)}, u32[]{:S(2)}) collective-permute-start(bf16[1,528,256]{2,1,0:T(8,128)(2,1)S(1)} %get-tuple-element.54), channel_id=1, source_target_pairs={{0,448},{1,65},{64,128},{65,1},{128,64},{129,193},{192,256},{193,1... | collective-permute-start | bytes 811016 | tf_op jit(solution)/shard_map/ppermute | solution.py:40
  118.7 6.2 %collective-permute-start.17 = (bf16[1,528,256]{2,1,0:T(8,128)(2,1)S(1)}, bf16[1,528,256]{2,1,0:T(8,128)(2,1)S(1)}, u32[]{:S(2)}, u32[]{:S(2)}) collective-permute-start(bf16[1,528,256]{2,1,0:T(8,128)(2,1)S(1)} %get-tuple-element.55), channel_id=1, source_target_pairs={{0,384},{1,129},{64,192},{65,449},{128,0},{129,257},{192,320},{193... | collective-permute-start | bytes 811016 | tf_op jit(solution)/shard_map/ppermute | solution.py:49
  125.1 2.9 %collective-permute-start.11 = (bf16[2,48,2048]{2,1,0:T(8,128)(2,1)S(1)}, bf16[2,48,2048]{2,1,0:T(8,128)(2,1)S(1)}, u32[]{:S(2)}, u32[]{:S(2)}) collective-permute-start(bf16[2,48,2048]{2,1,0:T(8,128)(2,1)S(1)} %get-tuple-element.47), channel_id=1, source_target_pairs={{0,8},{8,0},{1,9},{9,1},{2,10},{10,2},{3,11},{11,3},{4,12},{12,4},... | collective-permute-start | bytes 1179656 | tf_op jit(solution)/shard_map/ppermute | solution.py:53
  128.6 5.0 %collective-permute-done.17.r_ref = bf16[1,528,256]{2,1,0:T(8,128)(2,1)S(1)} collective-permute-done((bf16[1,528,256]{2,1,0:T(8,128)(2,1)S(1)}, bf16[1,528,256]{2,1,0:T(8,128)(2,1)S(1)}, u32[]{:S(2)}, u32[]{:S(2)}) %collective-permute-start.17) | collective-permute-done | bytes 270368 | tf_op jit(solution)/shard_map/ppermute | solution.py:49
  134.5 4.5 %all-to-all-start.1 = ((bf16[8,136,128]{2,1,0:T(8,128)(2,1)}), bf16[8,136,128]{2,1,0:T(8,128)(2,1)S(1)}, u32[]{:S(2)}, u32[]{:S(2)}) async-start(bf16[8,136,128]{2,1,0:T(8,128)(2,1)} %shard_map.162), calls=%async_computation.1 | async-start | bytes 557056 | tf_op jit(solution)/shard_map/all_to_all | solution.py:57
  139.3 3.2 %collective-permute-start.12 = (bf16[2,24,2048]{2,1,0:T(8,128)(2,1)S(1)}, bf16[2,24,2048]{2,1,0:T(8,128)(2,1)S(1)}, u32[]{:S(2)}, u32[]{:S(2)}) collective-permute-start(bf16[2,24,2048]{2,1,0:T(8,128)(2,1)S(1)} %get-tuple-element.49), channel_id=1, source_target_pairs={{0,2},{1,7},{2,0},{3,5},{4,6},{5,3},{6,4},{7,1},{8,10},{9,15},{10,... | collective-permute-start | bytes 589832 | tf_op jit(solution)/shard_map/ppermute | solution.py:40
  142.5 7.2 %all-to-all-done.1.r_ref = bf16[8,136,128]{2,1,0:T(8,128)(2,1)S(1)} async-done(((bf16[8,136,128]{2,1,0:T(8,128)(2,1)}), bf16[8,136,128]{2,1,0:T(8,128)(2,1)S(1)}, u32[]{:S(2)}, u32[]{:S(2)}) %all-to-all-start.1) | async-done | bytes 278560 | tf_op jit(solution)/shard_map/all_to_all | solution.py:57
  (46 shorter events, 14.7 us)
Async XLA Ops:
  1.8 8.6 %collective-permute-start = (bf16[3,24,2048]{2,1,0:T(8,128)(2,1)S(1)}, bf16[3,24,2048]{2,1,0:T(8,128)(2,1)S(1)}, u32[]{:S(2)}, u32[]{:S(2)}) collective-permute-start(bf16[3,24,2048]{2,1,0:T(8,128)(2,1)S(1)} %shard_map.146), channel_id=1, source_target_pairs={{0,2},{1,7},{2,0},{3,5},{4,6},{5,3},{6,4},{7,1},{8,10},{9,15},{10,... | collective-permute-start | bytes 884744 | tf_op jit(solution)/shard_map/ppermute | solution.py:40
  10.6 19.6 %collective-permute-start.1 = (bf16[3,48,2048]{2,1,0:T(8,128)(2,1)S(1)}, bf16[3,48,2048]{2,1,0:T(8,128)(2,1)S(1)}, u32[]{:S(2)}, u32[]{:S(2)}) collective-permute-start(bf16[3,48,2048]{2,1,0:T(8,128)(2,1)S(1)} %get-tuple-element.60), channel_id=1, source_target_pairs={{0,8},{8,0},{1,9},{9,1},{2,10},{10,2},{3,11},{11,3},{4,12},{12,4},... | collective-permute-start | bytes 1769480 | tf_op jit(solution)/shard_map/ppermute | solution.py:53
  15.7 22.0 %all-to-all-start = ((bf16[8,136,128]{2,1,0:T(8,128)(2,1)}), bf16[8,136,128]{2,1,0:T(8,128)(2,1)S(1)}, u32[]{:S(2)}, u32[]{:S(2)}) async-start(bf16[8,136,128]{2,1,0:T(8,128)(2,1)} %shard_map.147), calls=%async_computation | async-start | bytes 557056 | tf_op jit(solution)/shard_map/all_to_all | solution.py:57
  30.3 45.1 %copy-start.7 = (s32[8]{0:T(128)S(1)}, s32[8]{0:T(128)}, u32[]{:S(2)}) copy-start(s32[8]{0:T(128)} %constant.24.clone) | copy-start | bytes 100
  30.3 23.4 %collective-permute-start.2 = (bf16[2,3,48,2048]{3,2,1,0:T(8,128)(2,1)S(1)}, bf16[2,3,48,2048]{3,2,1,0:T(8,128)(2,1)}, u32[]{:S(2)}, u32[]{:S(2)}) collective-permute-start(bf16[2,3,48,2048]{3,2,1,0:T(8,128)(2,1)S(1)} %pad_maximum_fusion.ta), channel_id=1, source_target_pairs={{0,6},{1,3},{2,4},{3,1},{4,2},{5,7},{6,0},{7,5},{8,14},{9,11},{10,... | collective-permute-start | bytes 3538952 | tf_op jit(solution)/shard_map/ppermute | solution.py:40
  37.8 8.4 %collective-permute-start.3 = (bf16[528,256]{1,0:T(8,128)(2,1)S(1)}, bf16[528,256]{1,0:T(8,128)(2,1)S(1)}, u32[]{:S(2)}, u32[]{:S(2)}) collective-permute-start(bf16[528,256]{1,0:T(8,128)(2,1)S(1)} %shard_map.148.a_ref), channel_id=1, source_target_pairs={{0,64},{1,449},{64,0},{65,129},{128,192},{129,65},{192,128},{193,2... | collective-permute-start | bytes 811016 | tf_op jit(solution)/shard_map/ppermute | solution.py:40
  46.2 12.0 %collective-permute-start.4 = (bf16[2,528,256]{2,1,0:T(8,128)(2,1)S(1)}, bf16[2,528,256]{2,1,0:T(8,128)(2,1)S(1)}, u32[]{:S(2)}, u32[]{:S(2)}) collective-permute-start(bf16[2,528,256]{2,1,0:T(8,128)(2,1)S(1)} %shard_map.149.p0), channel_id=1, source_target_pairs={{0,448},{1,65},{64,128},{65,1},{128,64},{129,193},{192,256},{193,1... | collective-permute-start | bytes 1622024 | tf_op jit(solution)/shard_map/ppermute | solution.py:40
  50.9 26.5 %collective-permute-start.6 = (bf16[2,3,48,2048]{3,2,1,0:T(8,128)(2,1)S(1)}, bf16[2,3,48,2048]{3,2,1,0:T(8,128)(2,1)}, u32[]{:S(2)}, u32[]{:S(2)}) collective-permute-start(bf16[2,3,48,2048]{3,2,1,0:T(8,128)(2,1)S(1)} %pad_maximum_fusion.ta), channel_id=1, source_target_pairs={{0,1},{1,0},{2,3},{3,2},{4,5},{5,4},{6,7},{7,6},{8,9},{9,8},{10,11... | collective-permute-start | bytes 3538952 | tf_op jit(solution)/shard_map/ppermute | solution.py:53
  53.7 23.8 %collective-permute-start.7 = (bf16[2,3,48,2048]{3,2,1,0:T(8,128)(2,1)}, bf16[2,3,48,2048]{3,2,1,0:T(8,128)(2,1)}, u32[]{:S(2)}, u32[]{:S(2)}) collective-permute-start(bf16[2,3,48,2048]{3,2,1,0:T(8,128)(2,1)} %collective-permute-done.2.tb), channel_id=1, source_target_pairs={{0,1},{1,0},{2,3},{3,2},{4,5},{5,4},{6,7},{7,6},{8,9},{9,8},{10,11... | collective-permute-start | bytes 3538952 | tf_op jit(solution)/shard_map/ppermute | solution.py:53
  58.2 15.2 %collective-permute-start.5 = (bf16[2,528,256]{2,1,0:T(8,128)(2,1)S(1)}, bf16[2,528,256]{2,1,0:T(8,128)(2,1)S(1)}, u32[]{:S(2)}, u32[]{:S(2)}) collective-permute-start(bf16[2,528,256]{2,1,0:T(8,128)(2,1)S(1)} %collective-permute-done.4.p1), channel_id=1, source_target_pairs={{0,64},{1,449},{64,0},{65,129},{128,192},{129,65},{192,128},{193,2... | collective-permute-start | bytes 1622024 | tf_op jit(solution)/shard_map/ppermute | solution.py:40
  73.4 11.2 %collective-permute-start.8 = (bf16[2,528,256]{2,1,0:T(8,128)(2,1)S(1)}, bf16[2,528,256]{2,1,0:T(8,128)(2,1)S(1)}, u32[]{:S(2)}, u32[]{:S(2)}) collective-permute-start(bf16[2,528,256]{2,1,0:T(8,128)(2,1)S(1)} %collective-permute-done.5.p2), channel_id=1, source_target_pairs={{0,448},{1,65},{64,128},{65,1},{128,64},{129,193},{192,256},{193,1... | collective-permute-start | bytes 1622024 | tf_op jit(solution)/shard_map/ppermute | solution.py:40
  89.0 5.3 %collective-permute-start.9 = (bf16[2,192,2048]{2,1,0:T(8,128)(2,1)S(1)}, bf16[2,192,2048]{2,1,0:T(8,128)(2,1)S(1)}, u32[]{:S(2)}, u32[]{:S(2)}) collective-permute-start(bf16[2,192,2048]{2,1,0:T(8,128)(2,1)S(1)} %get-tuple-element.43), channel_id=1, source_target_pairs={{0,1},{1,0},{2,3},{3,2},{4,5},{5,4},{6,7},{7,6},{8,9},{9,8},{10,11... | collective-permute-start | bytes 4718600 | tf_op jit(solution)/shard_map/ppermute | solution.py:53
  90.9 11.3 %collective-permute-start.14 = (bf16[2,528,256]{2,1,0:T(8,128)(2,1)S(1)}, bf16[2,528,256]{2,1,0:T(8,128)(2,1)S(1)}, u32[]{:S(2)}, u32[]{:S(2)}) collective-permute-start(bf16[2,528,256]{2,1,0:T(8,128)(2,1)S(1)} %get-tuple-element.53), channel_id=1, source_target_pairs={{0,448},{1,65},{64,128},{65,1},{128,64},{129,193},{192,256},{193,1... | collective-permute-start | bytes 1622024 | tf_op jit(solution)/shard_map/ppermute | solution.py:40
  94.7 30.3 %collective-permute-start.10 = (bf16[2,96,2048]{2,1,0:T(8,128)(2,1)S(1)}, bf16[2,96,2048]{2,1,0:T(8,128)(2,1)S(1)}, u32[]{:S(2)}, u32[]{:S(2)}) collective-permute-start(bf16[2,96,2048]{2,1,0:T(8,128)(2,1)S(1)} %get-tuple-element.45), channel_id=1, source_target_pairs={{0,6},{1,3},{2,4},{3,1},{4,2},{5,7},{6,0},{7,5},{8,14},{9,11},{10,... | collective-permute-start | bytes 2359304 | tf_op jit(solution)/shard_map/ppermute | solution.py:40
  102.6 13.7 %collective-permute-start.15 = (bf16[2,528,256]{2,1,0:T(8,128)(2,1)S(1)}, bf16[2,528,256]{2,1,0:T(8,128)(2,1)S(1)}, u32[]{:S(2)}, u32[]{:S(2)}) collective-permute-start(bf16[2,528,256]{2,1,0:T(8,128)(2,1)S(1)} %shard_map.159), channel_id=1, source_target_pairs={{0,64},{1,449},{64,0},{65,129},{128,192},{129,65},{192,128},{193,2... | collective-permute-start | bytes 1622024 | tf_op jit(solution)/shard_map/ppermute | solution.py:40
  109.3 18.6 %collective-permute-start.13 = (bf16[1,528,256]{2,1,0:T(8,128)(2,1)S(1)}, bf16[1,528,256]{2,1,0:T(8,128)(2,1)S(1)}, u32[]{:S(2)}, u32[]{:S(2)}) collective-permute-start(bf16[1,528,256]{2,1,0:T(8,128)(2,1)S(1)} %shard_map.158), channel_id=1, source_target_pairs={{0,64},{1,449},{64,0},{65,129},{128,192},{129,65},{192,128},{193,2... | collective-permute-start | bytes 811016 | tf_op jit(solution)/shard_map/ppermute | solution.py:40
  116.8 11.3 %collective-permute-start.16 = (bf16[1,528,256]{2,1,0:T(8,128)(2,1)S(1)}, bf16[1,528,256]{2,1,0:T(8,128)(2,1)S(1)}, u32[]{:S(2)}, u32[]{:S(2)}) collective-permute-start(bf16[1,528,256]{2,1,0:T(8,128)(2,1)S(1)} %get-tuple-element.54), channel_id=1, source_target_pairs={{0,448},{1,65},{64,128},{65,1},{128,64},{129,193},{192,256},{193,1... | collective-permute-start | bytes 811016 | tf_op jit(solution)/shard_map/ppermute | solution.py:40
  118.7 14.9 %collective-permute-start.17 = (bf16[1,528,256]{2,1,0:T(8,128)(2,1)S(1)}, bf16[1,528,256]{2,1,0:T(8,128)(2,1)S(1)}, u32[]{:S(2)}, u32[]{:S(2)}) collective-permute-start(bf16[1,528,256]{2,1,0:T(8,128)(2,1)S(1)} %get-tuple-element.55), channel_id=1, source_target_pairs={{0,384},{1,129},{64,192},{65,449},{128,0},{129,257},{192,320},{193... | collective-permute-start | bytes 811016 | tf_op jit(solution)/shard_map/ppermute | solution.py:49
  125.1 14.2 %collective-permute-start.11 = (bf16[2,48,2048]{2,1,0:T(8,128)(2,1)S(1)}, bf16[2,48,2048]{2,1,0:T(8,128)(2,1)S(1)}, u32[]{:S(2)}, u32[]{:S(2)}) collective-permute-start(bf16[2,48,2048]{2,1,0:T(8,128)(2,1)S(1)} %get-tuple-element.47), channel_id=1, source_target_pairs={{0,8},{8,0},{1,9},{9,1},{2,10},{10,2},{3,11},{11,3},{4,12},{12,4},... | collective-permute-start | bytes 1179656 | tf_op jit(solution)/shard_map/ppermute | solution.py:53
  128.5 14.0 %copy-start.6 = (bf16[2048]{0:T(1024)(128)(2,1)S(1)}, bf16[2048]{0:T(1024)(128)(2,1)}, u32[]{:S(2)}) copy-start(bf16[2048]{0:T(1024)(128)(2,1)} %g_hbm.2) | copy-start | bytes 12292
  128.5 21.2 %copy-start.3 = (f32[32,352]{1,0:T(8,128)S(1)}, f32[32,352]{1,0:T(8,128)}, u32[]{:S(2)}) copy-start(f32[32,352]{1,0:T(8,128)} %gs.1) | copy-start | bytes 135172
  128.6 21.2 %copy-start.4 = (f32[32,352]{1,0:T(8,128)S(1)}, f32[32,352]{1,0:T(8,128)}, u32[]{:S(2)}) copy-start(f32[32,352]{1,0:T(8,128)} %us.1) | copy-start | bytes 135172
  128.6 21.2 %copy-start.5 = (f32[32,352]{1,0:T(8,128)S(1)}, f32[32,352]{1,0:T(8,128)}, u32[]{:S(2)}) copy-start(f32[32,352]{1,0:T(8,128)} %ds.1) | copy-start | bytes 135172
  134.5 16.0 %copy-start = (bf16[24,2048]{1,0:T(8,128)(2,1)S(1)}, bf16[24,2048]{1,0:T(8,128)(2,1)}, u32[]{:S(2)}) copy-start(bf16[24,2048]{1,0:T(8,128)(2,1)} %e_ref.1) | copy-start | bytes 294916
  134.5 16.0 %copy-start.1 = (bf16[24,2048]{1,0:T(8,128)(2,1)S(1)}, bf16[24,2048]{1,0:T(8,128)(2,1)}, u32[]{:S(2)}) copy-start(bf16[24,2048]{1,0:T(8,128)(2,1)} %c_ref.1) | copy-start | bytes 294916
  134.5 16.0 %copy-start.2 = (bf16[24,2048]{1,0:T(8,128)(2,1)S(1)}, bf16[24,2048]{1,0:T(8,128)(2,1)}, u32[]{:S(2)}) copy-start(bf16[24,2048]{1,0:T(8,128)(2,1)} %l_ref.1) | copy-start | bytes 294916
  134.5 15.2 %all-to-all-start.1 = ((bf16[8,136,128]{2,1,0:T(8,128)(2,1)}), bf16[8,136,128]{2,1,0:T(8,128)(2,1)S(1)}, u32[]{:S(2)}, u32[]{:S(2)}) async-start(bf16[8,136,128]{2,1,0:T(8,128)(2,1)} %shard_map.162), calls=%async_computation.1 | async-start | bytes 557056 | tf_op jit(solution)/shard_map/all_to_all | solution.py:57
  139.3 11.2 %collective-permute-start.12 = (bf16[2,24,2048]{2,1,0:T(8,128)(2,1)S(1)}, bf16[2,24,2048]{2,1,0:T(8,128)(2,1)S(1)}, u32[]{:S(2)}, u32[]{:S(2)}) collective-permute-start(bf16[2,24,2048]{2,1,0:T(8,128)(2,1)S(1)} %get-tuple-element.49), channel_id=1, source_target_pairs={{0,2},{1,7},{2,0},{3,5},{4,6},{5,3},{6,4},{7,1},{8,10},{9,15},{10,... | collective-permute-start | bytes 589832 | tf_op jit(solution)/shard_map/ppermute | solution.py:40

commit v2 on v1

--- a/solution.py
+++ b/solution.py
@@ -15,6 +15,7 @@
 
 AXES = ("z", "yq", "ys", "x", "c")
 NZ, NY, NX, NC = 8, 8, 4, 2
+FLIP = {"z": 0, "x": 1}
 ROWS = 32
 HALF = 176
 MAIN = 128
@@ -35,16 +36,16 @@
     pairs = []
     for i in range(size):
         for c in range(NC):
-            j = (i + 1) % size if (i + c + phase) % 2 == 0 else (i - 1) % size
+            j = (i + 1) % size if (i + c + phase + FLIP[axis]) % 2 == 0 else (i - 1) % size
             pairs.append((i * NC + c, j * NC + c))
     return lax.ppermute(x, (axis, "c"), pairs)
 
 
-def hop_two(x):
+def hop_two(x, way):
     pairs = []
     for i in range(NZ):
         for c in range(NC):
-            j = (i - 2) % NZ if (i + c) % 2 == 0 else (i + 2) % NZ
+            j = (i + 2 * way) % NZ if (i + c + FLIP["z"]) % 2 == 0 else (i - 2 * way) % NZ
             pairs.append((i * NC + c, j * NC + c))
     return lax.ppermute(x, ("z", "c"), pairs)
 
@@ -152,7 +153,7 @@
     return jnp.concatenate([*parts[:4], fold_rows(parts[4], 0, 1)], axis=1)
 
 
-def forward_part(b_ref, ta, tb, p0, p1, p2, te, th, tl, acc, w):
+def forward_part(b_ref, ta, tb, own, got, p1, p2, te, th, tl, acc, w):
     for q, piece in enumerate((ta, tb)):
         for n in range(2):
             rows = pl.ds((q * 2 + n) * 48, 48)
@@ -162,9 +163,8 @@
                 te[rows, out] = piece[n, 0, :, cols]
                 th[rows, out] = piece[n, 1, :, cols]
                 tl[rows, out] = piece[n, 2, :, cols]
-    for q, pair in enumerate((p0, p1, p2)):
-        for n in range(2):
-            w[:, pl.ds((2 * q + n) * 256, 256)] = pair[n]
+    for n, block in enumerate((own, got, p1.at[0], p1.at[1], p2.at[0], p2.at[1])):
+        w[:, pl.ds(n * 256, 256)] = block[...]
     k = 6 * 256
     g, u, d = w[0:HALF], w[HALF : 2 * HALF], w[2 * HALF : 3 * HALF]
     acc[0] = dot_tt(te[:, :k], g)
@@ -227,23 +227,21 @@
     o_ref[...] = (f_ref[...] + turned(r_ref[0])).astype(bf16)
 
 
-def token_parts(b_ref, dg_ref, du_ref, tl0, tl1, p0, p1, p2, p3, near, far, w):
-    pairs = (p0, p1, p2, p3)
-    for q, pair in enumerate(pairs):
-        for n in range(2):
-            w[:, pl.ds((2 * q + n) * 256, 256)] = pair[n, 0 : 2 * HALF]
+def token_parts(b_ref, dg_ref, du_ref, tl0, tl1, own, got, p1, p2, p3, near, far, w):
+    blocks = (own, got) + tuple(p.at[n] for p in (p1, p2, p3) for n in range(2))
+    for n, block in enumerate(blocks):
+        w[:, pl.ds(n * 256, 256)] = block[0 : 2 * HALF]
     for h, (tl, o) in enumerate(((tl0, near), (tl1, far))):
         gl = dot_tt(tl[...], w[0:HALF])
         ul = dot_tt(tl[...], w[HALF : 2 * HALF])
         hl = (gl * jax.nn.sigmoid(gl) * ul).astype(bf16)
         dg, du = dg_ref[h], du_ref[h]
-        for q, pair in enumerate(pairs):
-            for n in range(2):
-                cols = pl.ds(pl.multiple_of(b_ref[2 * q + n] * 256, 256), 256)
-                late = dot_nn(hl, pair[n, 2 * HALF : 3 * HALF])
-                early = dot_nn(dg, pair[n, 0:HALF]) + dot_nn(du, pair[n, HALF : 2 * HALF])
-                o[0, :, cols] = late.astype(o.dtype)
-                o[1, :, cols] = early.astype(o.dtype)
+        for n, block in enumerate(blocks):
+            cols = pl.ds(pl.multiple_of(b_ref[n] * 256, 256), 256)
+            late = dot_nn(hl, block[2 * HALF : 3 * HALF])
+            early = dot_nn(dg, block[0:HALF]) + dot_nn(du, block[HALF : 2 * HALF])
+            o[0, :, cols] = late.astype(o.dtype)
+            o[1, :, cols] = early.astype(o.dtype)
 
 
 def fold(n_ref, r_ref, keep, send):
@@ -251,6 +249,13 @@
     for i in range(2):
         keep[i] = n_ref[i, :rows] + r_ref[i, :rows].astype(f32)
         send[i] = (n_ref[i, rows:] + r_ref[i, rows:].astype(f32)).astype(bf16)
+
+
+def fold_mate(n_ref, r_ref, keep, send):
+    for i in range(2):
+        sums = n_ref[i] + r_ref[i].astype(f32)
+        keep[i] = jnp.concatenate([sums[0:24], sums[48:72]], axis=0)
+        send[i] = jnp.concatenate([sums[24:48], sums[72:96]], axis=0).astype(bf16)
 
 
 def finish_tokens(n_ref, r_ref, e_ref, c_ref, l_ref, g_ref, late, early):
@@ -307,7 +312,7 @@
 ):
     gain = norm_gain.reshape(1, -1)
     z, c = lax.axis_index("z"), lax.axis_index("c")
-    step = 1 - 2 * lax.rem(z + c, 2)
+    step = 1 - 2 * lax.rem(z + c + FLIP["z"], 2)
     order = jnp.array([0, 1, -1, -2, 2, 3, -3, -4], jnp.int32)
     blocks = lax.rem(z + order * step + 8, 8).astype(jnp.int32)
 
@@ -325,13 +330,14 @@
     sent = staged(pack_weights, (NY, PACK, 128), gate_weight, up_weight, down_weight)
     tok = staged(prepare_tokens, (3, 24, 2048), x_early, cotangent, x_late, norm_gain)
     own = call(turn_block, shape((3 * HALF, 256)), over_y(sent))
-    p0 = call(join, shape((2, 3 * HALF, 256)), own, exchange(own, "z", NZ, 0))
-    p1 = exchange(p0, "z", NZ, 1)
+    got = exchange(own, "z", NZ, 0)
+    far = hop_two(own, 1)
+    p1 = call(join, shape((2, 3 * HALF, 256)), exchange(own, "z", NZ, 1), far)
     p2 = exchange(p1, "z", NZ, 0)
     p3 = exchange(p2, "z", NZ, 1)
 
-    t0 = jnp.concatenate([tok, exchange(tok, "x", NX, 0)], axis=1)
-    ta = jnp.stack([t0, swapped(t0, "ys")])
+    t0 = jnp.concatenate([tok, swapped(tok, "ys")], axis=1)
+    ta = call(join, shape((2, 3, 48, 2048)), t0, exchange(t0, "x", NX, 0))
     tb = exchange(ta, "x", NX, 1)
     tc = swapped(ta, "c")
     td = swapped(tb, "c")
@@ -340,8 +346,8 @@
         return call(
             forward_part,
             (shape((192, 2048)),) * 3 + (shape((3, 192, HALF), f32),),
-            blocks, first, second, p0, p1, p2,
-            in_specs=[SM] + [VM] * 5,
+            blocks, first, second, own, got, p1, p2,
+            in_specs=[SM] + [VM] * 6,
             scratch_shapes=[pltpu.VMEM((3 * HALF, 6 * 256), bf16)],
         )
 
@@ -359,8 +365,8 @@
     near, far = call(
         token_parts,
         (shape((2, 192, 2048), f32), shape((2, 192, 2048))),
-        blocks, dg, du, tl0, tl1, p0, p1, p2, p3,
-        in_specs=[SM] + [VM] * 8,
+        blocks, dg, du, tl0, tl1, own, got, p1, p2, p3,
+        in_specs=[SM] + [VM] * 9,
         scratch_shapes=[pltpu.VMEM((2 * HALF, 2048), bf16)],
     )
     s2 = call(functools.partial(add_pair, 4), pair, *tokens, r3)
@@ -368,7 +374,7 @@
     one = shape((1, 3 * HALF, 256))
     mine = exchange(call(neighbour_share, one, *tokens), "z", NZ, 0)
     s1, s0 = call(add_each, (one, one), *tokens, r2)
-    r0 = hop_two(s0)
+    r0 = hop_two(s0, -1)
     r1 = exchange(s1, "z", NZ, 1)
     block = call(
         own_block,
@@ -383,12 +389,12 @@
         over_y(back), gate_sum, up_sum, down_sum,
     )
 
-    def folded(near, far):
+    def folded(near, far, body=fold):
         dims = (2, near.shape[1] // 2, 2048)
-        return call(fold, (shape(dims, f32), shape(dims)), near, far)
+        return call(body, (shape(dims, f32), shape(dims)), near, far)
 
     near, far = folded(near, swapped(far, "c"))
-    near, far = folded(near, exchange(far, "x", NX, 1))
+    near, far = folded(near, exchange(far, "x", NX, 1), fold_mate)
     near, far = folded(near, swapped(far, "ys"))
     late, early = call(
         finish_tokens,

time: 152 us -> 160 us (1.053)
  blocking collectives: 0 us -> 18.4 us
  starting transfers between devices: 74.3 us -> 69 us
  waiting for transfers between devices: 59.2 us -> 54.9 us
    all_to_all x0 -> x1, blocking collectives: none -> 18.4 us  [over_y(): lax.all_to_all(x, ('yq', 'ys'), split_axis=0, concat_axis=0, tiled=True)]
    ppermute x1 -> x2, starting transfers between devices: 6.18 us -> 14 us  [hop_two(): return lax.ppermute(x, ('z', 'c'), pairs)]
    all_to_all x2 -> x1, starting transfers between devices: 10.7 us -> 3.55 us  [over_y(): lax.all_to_all(x, ('yq', 'ys'), split_axis=0, concat_axis=0, tiled=True)]
    ppermute x12, starting transfers between devices: 44.4 us -> 39.7 us  [exchange(): return lax.ppermute(x, (axis, 'c'), pairs)]
    ppermute x12, waiting for transfers between devices: 34.4 us -> 31.6 us  [exchange(): return lax.ppermute(x, (axis, 'c'), pairs)]
    all_to_all x2 -> x1, waiting for transfers between devices: 9.92 us -> 7.99 us  [over_y(): lax.all_to_all(x, ('yq', 'ys'), split_axis=0, concat_axis=0, tiled=True)]
    ppermute x1 -> x2, waiting for transfers between devices: 5.01 us -> 6.14 us  [hop_two(): return lax.ppermute(x, ('z', 'c'), pairs)]
    pallas_call x18 -> x19, Pallas kernels: 16.6 us -> 16 us  [call(): pl.pallas_call(body, out_shape=out_shape, compiler_params=pltpu.CompilerP...]
  transfers between devices with their start and end apart: 20 -> 20, of which waited for: 14 -> 12; matrix products, arithmetic and copies ran while one was open for 0% -> 0% of each run, Pallas kernels for 7% -> 6%
where the time goes in v2:
time: 160 us; the launch traced here: 159 us
  starting transfers between devices  69 us (43%)
  waiting for transfers between devices  54.9 us (34%)
  blocking collectives  18.4 us (11%)
  Pallas kernels  16 us (10%)
    ppermute x12, starting transfers between devices, exchange(): return lax.ppermute(x, (axis, 'c'), pairs)  39.7 us
    ppermute x12, waiting for transfers between devices, exchange(): return lax.ppermute(x, (axis, 'c'), pairs)  31.6 us
    all_to_all x1, blocking collectives, over_y(): lax.all_to_all(x, ('yq', 'ys'), split_axis=0, concat_axis=0, tiled=True)  18.4 us
    pallas_call x19, Pallas kernels, call(): pl.pallas_call(body, out_shape=out_shape, compiler_params=pltpu.CompilerP...  16 us
    ppermute x2, starting transfers between devices, hop_two(): return lax.ppermute(x, ('z', 'c'), pairs)  14 us
    ppermute x5, starting transfers between devices, swapped(): return lax.ppermute(x, axis, [(0, 1), (1, 0)])  11.7 us
    ppermute x5, waiting for transfers between devices, swapped(): return lax.ppermute(x, axis, [(0, 1), (1, 0)])  9.13 us
    all_to_all x1, waiting for transfers between devices, over_y(): lax.all_to_all(x, ('yq', 'ys'), split_axis=0, concat_axis=0, tiled=True)  7.99 us
  transfers between devices with their start and end apart: 20, of which 12 were waited for; matrix products, arithmetic and copies ran while one was open for 0% of the time, Pallas kernels for 6%

profile of v2, /device:TPU:64, one launch (start us, length us, event | category | flops | bytes accessed | tf_op | source)
XLA Modules:
  0.0 159.3 jit_solution(7013704895520082152)
XLA Ops:
  1.8 3.5 %collective-permute-start = (bf16[3,24,2048]{2,1,0:T(8,128)(2,1)S(1)}, bf16[3,24,2048]{2,1,0:T(8,128)(2,1)S(1)}, u32[]{:S(2)}, u32[]{:S(2)}) collective-permute-start(bf16[3,24,2048]{2,1,0:T(8,128)(2,1)S(1)} %shard_map.146), channel_id=1, source_target_pairs={{0,8},{8,0},{1,9},{9,1},{2,10},{10,2},{3,11},{11,3},{4,12},{12,4},... | collective-permute-start | bytes 884744 | tf_op jit(solution)/shard_map/ppermute | solution.py:54
  5.3 7.1 %collective-permute-done = bf16[3,24,2048]{2,1,0:T(8,128)(2,1)S(1)} collective-permute-done((bf16[3,24,2048]{2,1,0:T(8,128)(2,1)S(1)}, bf16[3,24,2048]{2,1,0:T(8,128)(2,1)S(1)}, u32[]{:S(2)}, u32[]{:S(2)}) %collective-permute-start) | collective-permute-done | bytes 294944 | tf_op jit(solution)/shard_map/ppermute | solution.py:54
  12.5 4.7 %collective-permute-start.1 = (bf16[3,48,2048]{2,1,0:T(8,128)(2,1)S(1)}, bf16[3,48,2048]{2,1,0:T(8,128)(2,1)S(1)}, u32[]{:S(2)}, u32[]{:S(2)}) collective-permute-start(bf16[3,48,2048]{2,1,0:T(8,128)(2,1)S(1)} %pad_maximum_fusion.a_ref), channel_id=1, source_target_pairs={{0,6},{1,3},{2,4},{3,1},{4,2},{5,7},{6,0},{7,5},{8,14},{9,11},{10,... | collective-permute-start | bytes 1769480 | tf_op jit(solution)/shard_map/ppermute | solution.py:41
  17.2 8.3 %collective-permute-done.1.b_ref = bf16[3,48,2048]{2,1,0:T(8,128)(2,1)S(1)} collective-permute-done((bf16[3,48,2048]{2,1,0:T(8,128)(2,1)S(1)}, bf16[3,48,2048]{2,1,0:T(8,128)(2,1)S(1)}, u32[]{:S(2)}, u32[]{:S(2)}) %collective-permute-start.1) | collective-permute-done | bytes 589856 | tf_op jit(solution)/shard_map/ppermute | solution.py:41
  25.6 2.2 %collective-permute-start.2 = (bf16[2,3,48,2048]{3,2,1,0:T(8,128)(2,1)S(1)}, bf16[2,3,48,2048]{3,2,1,0:T(8,128)(2,1)}, u32[]{:S(2)}, u32[]{:S(2)}) collective-permute-start(bf16[2,3,48,2048]{3,2,1,0:T(8,128)(2,1)S(1)} %shard_map.147.ta), channel_id=1, source_target_pairs={{0,2},{1,7},{2,0},{3,5},{4,6},{5,3},{6,4},{7,1},{8,10},{9,15},{10,... | collective-permute-start | bytes 3538952 | tf_op jit(solution)/shard_map/ppermute | solution.py:41
  28.7 18.4 %all_to_all.10.r_ref = bf16[8,136,128]{2,1,0:T(8,128)(2,1)S(1)} all-to-all(bf16[8,136,128]{2,1,0:T(8,128)(2,1)S(1)} %shard_map.148), channel_id=1, replica_groups=mesh['z'=8,'yq'=4,'ys'=2,'x'=4,'c'=2] {'yq','ys'}, dimensions={0} | all-to-all | bytes 557056 | tf_op jit(solution)/shard_map/all_to_all | solution.py:58
  47.3 4.3 %collective-permute-start.4 = (bf16[528,256]{1,0:T(8,128)(2,1)S(1)}, bf16[528,256]{1,0:T(8,128)(2,1)S(1)}, u32[]{:S(2)}, u32[]{:S(2)}) collective-permute-start(bf16[528,256]{1,0:T(8,128)(2,1)S(1)} %shard_map.149.own), channel_id=1, source_target_pairs={{0,448},{1,65},{64,128},{65,1},{128,64},{129,193},{192,256},{193,1... | collective-permute-start | bytes 811016 | tf_op jit(solution)/shard_map/ppermute | solution.py:41
  51.6 7.7 %collective-permute-start.5 = (bf16[528,256]{1,0:T(8,128)(2,1)S(1)}, bf16[528,256]{1,0:T(8,128)(2,1)S(1)}, u32[]{:S(2)}, u32[]{:S(2)}) collective-permute-start(bf16[528,256]{1,0:T(8,128)(2,1)S(1)} %shard_map.149.own), channel_id=1, source_target_pairs={{0,128},{1,385},{64,448},{65,193},{128,256},{129,1},{192,64},{193,... | collective-permute-start | bytes 811016 | tf_op jit(solution)/shard_map/ppermute | solution.py:50
  59.3 1.9 %collective-permute-start.7 = (bf16[2,3,48,2048]{3,2,1,0:T(8,128)(2,1)S(1)}, bf16[2,3,48,2048]{3,2,1,0:T(8,128)(2,1)}, u32[]{:S(2)}, u32[]{:S(2)}) collective-permute-start(bf16[2,3,48,2048]{3,2,1,0:T(8,128)(2,1)S(1)} %shard_map.147.ta), channel_id=1, source_target_pairs={{0,1},{1,0},{2,3},{3,2},{4,5},{5,4},{6,7},{7,6},{8,9},{9,8},{10,11... | collective-permute-start | bytes 3538952 | tf_op jit(solution)/shard_map/ppermute | solution.py:54
  61.2 2.4 %collective-permute-start.8 = (bf16[2,3,48,2048]{3,2,1,0:T(8,128)(2,1)}, bf16[2,3,48,2048]{3,2,1,0:T(8,128)(2,1)}, u32[]{:S(2)}, u32[]{:S(2)}) collective-permute-start(bf16[2,3,48,2048]{3,2,1,0:T(8,128)(2,1)} %collective-permute-done.2.tb), channel_id=1, source_target_pairs={{0,1},{1,0},{2,3},{3,2},{4,5},{5,4},{6,7},{7,6},{8,9},{9,8},{10,11... | collective-permute-start | bytes 3538952 | tf_op jit(solution)/shard_map/ppermute | solution.py:54
  64.8 6.0 %collective-permute-start.6 = (bf16[2,528,256]{2,1,0:T(8,128)(2,1)S(1)}, bf16[2,528,256]{2,1,0:T(8,128)(2,1)S(1)}, u32[]{:S(2)}, u32[]{:S(2)}) collective-permute-start(bf16[2,528,256]{2,1,0:T(8,128)(2,1)S(1)} %shard_map.150.p1), channel_id=1, source_target_pairs={{0,64},{1,449},{64,0},{65,129},{128,192},{129,65},{192,128},{193,2... | collective-permute-start | bytes 1622024 | tf_op jit(solution)/shard_map/ppermute | solution.py:41
  70.8 7.3 %collective-permute-done.6.p2 = bf16[2,528,256]{2,1,0:T(8,128)(2,1)S(1)} collective-permute-done((bf16[2,528,256]{2,1,0:T(8,128)(2,1)S(1)}, bf16[2,528,256]{2,1,0:T(8,128)(2,1)S(1)}, u32[]{:S(2)}, u32[]{:S(2)}) %collective-permute-start.6) | collective-permute-done | bytes 540704 | tf_op jit(solution)/shard_map/ppermute | solution.py:41
  78.1 1.9 %collective-permute-start.9 = (bf16[2,528,256]{2,1,0:T(8,128)(2,1)S(1)}, bf16[2,528,256]{2,1,0:T(8,128)(2,1)S(1)}, u32[]{:S(2)}, u32[]{:S(2)}) collective-permute-start(bf16[2,528,256]{2,1,0:T(8,128)(2,1)S(1)} %collective-permute-done.6.p2), channel_id=1, source_target_pairs={{0,448},{1,65},{64,128},{65,1},{128,64},{129,193},{192,256},{193,1... | collective-permute-start | bytes 1622024 | tf_op jit(solution)/shard_map/ppermute | solution.py:41
  80.1 5.9 %collective-permute-start.3 = (bf16[528,256]{1,0:T(8,128)(2,1)S(1)}, bf16[528,256]{1,0:T(8,128)(2,1)S(1)}, u32[]{:S(2)}, u32[]{:S(2)}) collective-permute-start(bf16[528,256]{1,0:T(8,128)(2,1)S(1)} %shard_map.149.own), channel_id=1, source_target_pairs={{0,64},{1,449},{64,0},{65,129},{128,192},{129,65},{192,128},{193,2... | collective-permute-start | bytes 811016 | tf_op jit(solution)/shard_map/ppermute | solution.py:41
  86.0 4.4 %collective-permute-done.3.got = bf16[528,256]{1,0:T(8,128)(2,1)S(1)} collective-permute-done((bf16[528,256]{1,0:T(8,128)(2,1)S(1)}, bf16[528,256]{1,0:T(8,128)(2,1)S(1)}, u32[]{:S(2)}, u32[]{:S(2)}) %collective-permute-start.3) | collective-permute-done | bytes 270368 | tf_op jit(solution)/shard_map/ppermute | solution.py:41
  90.4 2.1 %shard_map.151 = (bf16[192,2048]{1,0:T(8,128)(2,1)S(1)}, bf16[192,2048]{1,0:T(8,128)(2,1)S(1)}, bf16[192,2048]{1,0:T(8,128)(2,1)S(1)}, f32[3,192,176]{2,1,0:T(8,128)S(1)}) custom-call(s32[8]{0:T(128)S(1)} %compare_select_fusion.b_ref, bf16[2,3,48,2048]{3,2,1,0:T(8,128)(2,1)S(1)} %shard_map.147.ta, bf16[2,3,48,2048]{3,2,1,0:T(8,128)(2,1)} %collective-permute-done.2.tb, ...), custom_call_target="tpu_custom_call" | custom-call | tf_op jit(solution)/shard_map/pallas_call | solution.py:27
  92.5 2.4 %shard_map.152 = (bf16[192,2048]{1,0:T(8,128)(2,1)S(1)}, bf16[192,2048]{1,0:T(8,128)(2,1)S(1)}, bf16[192,2048]{1,0:T(8,128)(2,1)S(1)}, f32[3,192,176]{2,1,0:T(8,128)S(1)}) custom-call(s32[8]{0:T(128)S(1)} %compare_select_fusion.b_ref, bf16[2,3,48,2048]{3,2,1,0:T(8,128)(2,1)} %collective-permute-done.7.ta, ...), custom_call_target="tpu_custom_call" | custom-call | tf_op jit(solution)/shard_map/pallas_call | solution.py:27
  96.0 3.3 %shard_map.154 = (f32[2,192,2048]{2,1,0:T(8,128)S(1)}, bf16[2,192,2048]{2,1,0:T(8,128)(2,1)S(1)}) custom-call(s32[8]{0:T(128)S(1)} %compare_select_fusion.b_ref, bf16[2,192,176]{2,1,0:T(8,128)(2,1)S(1)} %get-tuple-element.38.dg_ref, bf16[2,192,176]{2,1,0:T(8,128)(2,1)S(1)} %get-tuple-element.39.du_ref, bf16[192,2048]{1,0:T(8,128)(2,1)S(1)} %get-tuple-element.40.tl0, ...), custom_call_target="tpu_custom_call" | custom-call | tf_op jit(solution)/shard_map/pallas_call | solution.py:27
  99.3 1.9 %collective-permute-start.10 = (bf16[2,192,2048]{2,1,0:T(8,128)(2,1)S(1)}, bf16[2,192,2048]{2,1,0:T(8,128)(2,1)S(1)}, u32[]{:S(2)}, u32[]{:S(2)}) collective-permute-start(bf16[2,192,2048]{2,1,0:T(8,128)(2,1)S(1)} %get-tuple-element.43), channel_id=1, source_target_pairs={{0,1},{1,0},{2,3},{3,2},{4,5},{5,4},{6,7},{7,6},{8,9},{9,8},{10,11... | collective-permute-start | bytes 4718600 | tf_op jit(solution)/shard_map/ppermute | solution.py:54
  101.2 1.9 %collective-permute-start.15 = (bf16[2,528,256]{2,1,0:T(8,128)(2,1)S(1)}, bf16[2,528,256]{2,1,0:T(8,128)(2,1)S(1)}, u32[]{:S(2)}, u32[]{:S(2)}) collective-permute-start(bf16[2,528,256]{2,1,0:T(8,128)(2,1)S(1)} %get-tuple-element.53), channel_id=1, source_target_pairs={{0,448},{1,65},{64,128},{65,1},{128,64},{129,193},{192,256},{193,1... | collective-permute-start | bytes 1622024 | tf_op jit(solution)/shard_map/ppermute | solution.py:41
  104.9 1.9 %collective-permute-start.11 = (bf16[2,96,2048]{2,1,0:T(8,128)(2,1)S(1)}, bf16[2,96,2048]{2,1,0:T(8,128)(2,1)S(1)}, u32[]{:S(2)}, u32[]{:S(2)}) collective-permute-start(bf16[2,96,2048]{2,1,0:T(8,128)(2,1)S(1)} %get-tuple-element.45), channel_id=1, source_target_pairs={{0,2},{1,7},{2,0},{3,5},{4,6},{5,3},{6,4},{7,1},{8,10},{9,15},{10,... | collective-permute-start | bytes 2359304 | tf_op jit(solution)/shard_map/ppermute | solution.py:41
  106.9 5.6 %collective-permute-done.15.r_ref = bf16[2,528,256]{2,1,0:T(8,128)(2,1)S(1)} collective-permute-done((bf16[2,528,256]{2,1,0:T(8,128)(2,1)S(1)}, bf16[2,528,256]{2,1,0:T(8,128)(2,1)S(1)}, u32[]{:S(2)}, u32[]{:S(2)}) %collective-permute-start.15) | collective-permute-done | bytes 540704 | tf_op jit(solution)/shard_map/ppermute | solution.py:41
  112.9 5.1 %collective-permute-start.16 = (bf16[2,528,256]{2,1,0:T(8,128)(2,1)S(1)}, bf16[2,528,256]{2,1,0:T(8,128)(2,1)S(1)}, u32[]{:S(2)}, u32[]{:S(2)}) collective-permute-start(bf16[2,528,256]{2,1,0:T(8,128)(2,1)S(1)} %shard_map.160), channel_id=1, source_target_pairs={{0,64},{1,449},{64,0},{65,129},{128,192},{129,65},{192,128},{193,2... | collective-permute-start | bytes 1622024 | tf_op jit(solution)/shard_map/ppermute | solution.py:41
  118.4 1.9 %collective-permute-start.14 = (bf16[1,528,256]{2,1,0:T(8,128)(2,1)S(1)}, bf16[1,528,256]{2,1,0:T(8,128)(2,1)S(1)}, u32[]{:S(2)}, u32[]{:S(2)}) collective-permute-start(bf16[1,528,256]{2,1,0:T(8,128)(2,1)S(1)} %shard_map.159), channel_id=1, source_target_pairs={{0,64},{1,449},{64,0},{65,129},{128,192},{129,65},{192,128},{193,2... | collective-permute-start | bytes 811016 | tf_op jit(solution)/shard_map/ppermute | solution.py:41
  120.3 5.1 %collective-permute-done.16.r_ref = bf16[2,528,256]{2,1,0:T(8,128)(2,1)S(1)} collective-permute-done((bf16[2,528,256]{2,1,0:T(8,128)(2,1)S(1)}, bf16[2,528,256]{2,1,0:T(8,128)(2,1)S(1)}, u32[]{:S(2)}, u32[]{:S(2)}) %collective-permute-start.16) | collective-permute-done | bytes 540704 | tf_op jit(solution)/shard_map/ppermute | solution.py:41
  125.8 1.9 %collective-permute-start.17 = (bf16[1,528,256]{2,1,0:T(8,128)(2,1)S(1)}, bf16[1,528,256]{2,1,0:T(8,128)(2,1)S(1)}, u32[]{:S(2)}, u32[]{:S(2)}) collective-permute-start(bf16[1,528,256]{2,1,0:T(8,128)(2,1)S(1)} %get-tuple-element.54), channel_id=1, source_target_pairs={{0,448},{1,65},{64,128},{65,1},{128,64},{129,193},{192,256},{193,1... | collective-permute-start | bytes 811016 | tf_op jit(solution)/shard_map/ppermute | solution.py:41
  127.8 6.3 %collective-permute-start.18 = (bf16[1,528,256]{2,1,0:T(8,128)(2,1)S(1)}, bf16[1,528,256]{2,1,0:T(8,128)(2,1)S(1)}, u32[]{:S(2)}, u32[]{:S(2)}) collective-permute-start(bf16[1,528,256]{2,1,0:T(8,128)(2,1)S(1)} %get-tuple-element.55), channel_id=1, source_target_pairs={{0,384},{1,129},{64,192},{65,449},{128,0},{129,257},{192,320},{193... | collective-permute-start | bytes 811016 | tf_op jit(solution)/shard_map/ppermute | solution.py:50
  134.3 2.0 %collective-permute-start.12 = (bf16[2,48,2048]{2,1,0:T(8,128)(2,1)S(1)}, bf16[2,48,2048]{2,1,0:T(8,128)(2,1)S(1)}, u32[]{:S(2)}, u32[]{:S(2)}) collective-permute-start(bf16[2,48,2048]{2,1,0:T(8,128)(2,1)S(1)} %get-tuple-element.47), channel_id=1, source_target_pairs={{0,8},{8,0},{1,9},{9,1},{2,10},{10,2},{3,11},{11,3},{4,12},{12,4},... | collective-permute-start | bytes 1179656 | tf_op jit(solution)/shard_map/ppermute | solution.py:54
  137.6 5.0 %collective-permute-done.18.r_ref = bf16[1,528,256]{2,1,0:T(8,128)(2,1)S(1)} collective-permute-done((bf16[1,528,256]{2,1,0:T(8,128)(2,1)S(1)}, bf16[1,528,256]{2,1,0:T(8,128)(2,1)S(1)}, u32[]{:S(2)}, u32[]{:S(2)}) %collective-permute-start.18) | collective-permute-done | bytes 270368 | tf_op jit(solution)/shard_map/ppermute | solution.py:50
  143.6 3.5 %all-to-all-start.1 = ((bf16[8,136,128]{2,1,0:T(8,128)(2,1)}), bf16[8,136,128]{2,1,0:T(8,128)(2,1)S(1)}, u32[]{:S(2)}, u32[]{:S(2)}) async-start(bf16[8,136,128]{2,1,0:T(8,128)(2,1)} %shard_map.163), calls=%async_computation.1 | async-start | bytes 557056 | tf_op jit(solution)/shard_map/all_to_all | solution.py:58
  147.8 1.9 %collective-permute-start.13 = (bf16[2,24,2048]{2,1,0:T(8,128)(2,1)S(1)}, bf16[2,24,2048]{2,1,0:T(8,128)(2,1)S(1)}, u32[]{:S(2)}, u32[]{:S(2)}) collective-permute-start(bf16[2,24,2048]{2,1,0:T(8,128)(2,1)S(1)} %get-tuple-element.49), channel_id=1, source_target_pairs={{0,6},{1,3},{2,4},{3,1},{4,2},{5,7},{6,0},{7,5},{8,14},{9,11},{10,... | collective-permute-start | bytes 589832 | tf_op jit(solution)/shard_map/ppermute | solution.py:41
  149.7 8.0 %all-to-all-done.1.r_ref = bf16[8,136,128]{2,1,0:T(8,128)(2,1)S(1)} async-done(((bf16[8,136,128]{2,1,0:T(8,128)(2,1)}), bf16[8,136,128]{2,1,0:T(8,128)(2,1)S(1)}, u32[]{:S(2)}, u32[]{:S(2)}) %all-to-all-start.1) | async-done | bytes 278560 | tf_op jit(solution)/shard_map/all_to_all | solution.py:58
  (47 shorter events, 12.3 us)
Async XLA Ops:
  1.8 10.6 %collective-permute-start = (bf16[3,24,2048]{2,1,0:T(8,128)(2,1)S(1)}, bf16[3,24,2048]{2,1,0:T(8,128)(2,1)S(1)}, u32[]{:S(2)}, u32[]{:S(2)}) collective-permute-start(bf16[3,24,2048]{2,1,0:T(8,128)(2,1)S(1)} %shard_map.146), channel_id=1, source_target_pairs={{0,8},{8,0},{1,9},{9,1},{2,10},{10,2},{3,11},{11,3},{4,12},{12,4},... | collective-permute-start | bytes 884744 | tf_op jit(solution)/shard_map/ppermute | solution.py:54
  12.5 13.0 %collective-permute-start.1 = (bf16[3,48,2048]{2,1,0:T(8,128)(2,1)S(1)}, bf16[3,48,2048]{2,1,0:T(8,128)(2,1)S(1)}, u32[]{:S(2)}, u32[]{:S(2)}) collective-permute-start(bf16[3,48,2048]{2,1,0:T(8,128)(2,1)S(1)} %pad_maximum_fusion.a_ref), channel_id=1, source_target_pairs={{0,6},{1,3},{2,4},{3,1},{4,2},{5,7},{6,0},{7,5},{8,14},{9,11},{10,... | collective-permute-start | bytes 1769480 | tf_op jit(solution)/shard_map/ppermute | solution.py:41
  25.6 35.6 %collective-permute-start.2 = (bf16[2,3,48,2048]{3,2,1,0:T(8,128)(2,1)S(1)}, bf16[2,3,48,2048]{3,2,1,0:T(8,128)(2,1)}, u32[]{:S(2)}, u32[]{:S(2)}) collective-permute-start(bf16[2,3,48,2048]{3,2,1,0:T(8,128)(2,1)S(1)} %shard_map.147.ta), channel_id=1, source_target_pairs={{0,2},{1,7},{2,0},{3,5},{4,6},{5,3},{6,4},{7,1},{8,10},{9,15},{10,... | collective-permute-start | bytes 3538952 | tf_op jit(solution)/shard_map/ppermute | solution.py:41
  28.7 57.3 %copy-start.7 = (s32[8]{0:T(128)S(1)}, s32[8]{0:T(128)}, u32[]{:S(2)}) copy-start(s32[8]{0:T(128)} %constant.24.clone) | copy-start | bytes 100
  47.3 16.3 %collective-permute-start.4 = (bf16[528,256]{1,0:T(8,128)(2,1)S(1)}, bf16[528,256]{1,0:T(8,128)(2,1)S(1)}, u32[]{:S(2)}, u32[]{:S(2)}) collective-permute-start(bf16[528,256]{1,0:T(8,128)(2,1)S(1)} %shard_map.149.own), channel_id=1, source_target_pairs={{0,448},{1,65},{64,128},{65,1},{128,64},{129,193},{192,256},{193,1... | collective-permute-start | bytes 811016 | tf_op jit(solution)/shard_map/ppermute | solution.py:41
  51.6 13.2 %collective-permute-start.5 = (bf16[528,256]{1,0:T(8,128)(2,1)S(1)}, bf16[528,256]{1,0:T(8,128)(2,1)S(1)}, u32[]{:S(2)}, u32[]{:S(2)}) collective-permute-start(bf16[528,256]{1,0:T(8,128)(2,1)S(1)} %shard_map.149.own), channel_id=1, source_target_pairs={{0,128},{1,385},{64,448},{65,193},{128,256},{129,1},{192,64},{193,... | collective-permute-start | bytes 811016 | tf_op jit(solution)/shard_map/ppermute | solution.py:50
  59.3 33.2 %collective-permute-start.7 = (bf16[2,3,48,2048]{3,2,1,0:T(8,128)(2,1)S(1)}, bf16[2,3,48,2048]{3,2,1,0:T(8,128)(2,1)}, u32[]{:S(2)}, u32[]{:S(2)}) collective-permute-start(bf16[2,3,48,2048]{3,2,1,0:T(8,128)(2,1)S(1)} %shard_map.147.ta), channel_id=1, source_target_pairs={{0,1},{1,0},{2,3},{3,2},{4,5},{5,4},{6,7},{7,6},{8,9},{9,8},{10,11... | collective-permute-start | bytes 3538952 | tf_op jit(solution)/shard_map/ppermute | solution.py:54
  61.2 31.3 %collective-permute-start.8 = (bf16[2,3,48,2048]{3,2,1,0:T(8,128)(2,1)}, bf16[2,3,48,2048]{3,2,1,0:T(8,128)(2,1)}, u32[]{:S(2)}, u32[]{:S(2)}) collective-permute-start(bf16[2,3,48,2048]{3,2,1,0:T(8,128)(2,1)} %collective-permute-done.2.tb), channel_id=1, source_target_pairs={{0,1},{1,0},{2,3},{3,2},{4,5},{5,4},{6,7},{7,6},{8,9},{9,8},{10,11... | collective-permute-start | bytes 3538952 | tf_op jit(solution)/shard_map/ppermute | solution.py:54
  64.8 13.3 %collective-permute-start.6 = (bf16[2,528,256]{2,1,0:T(8,128)(2,1)S(1)}, bf16[2,528,256]{2,1,0:T(8,128)(2,1)S(1)}, u32[]{:S(2)}, u32[]{:S(2)}) collective-permute-start(bf16[2,528,256]{2,1,0:T(8,128)(2,1)S(1)} %shard_map.150.p1), channel_id=1, source_target_pairs={{0,64},{1,449},{64,0},{65,129},{128,192},{129,65},{192,128},{193,2... | collective-permute-start | bytes 1622024 | tf_op jit(solution)/shard_map/ppermute | solution.py:41
  78.1 16.8 %collective-permute-start.9 = (bf16[2,528,256]{2,1,0:T(8,128)(2,1)S(1)}, bf16[2,528,256]{2,1,0:T(8,128)(2,1)S(1)}, u32[]{:S(2)}, u32[]{:S(2)}) collective-permute-start(bf16[2,528,256]{2,1,0:T(8,128)(2,1)S(1)} %collective-permute-done.6.p2), channel_id=1, source_target_pairs={{0,448},{1,65},{64,128},{65,1},{128,64},{129,193},{192,256},{193,1... | collective-permute-start | bytes 1622024 | tf_op jit(solution)/shard_map/ppermute | solution.py:41
  80.1 10.3 %collective-permute-start.3 = (bf16[528,256]{1,0:T(8,128)(2,1)S(1)}, bf16[528,256]{1,0:T(8,128)(2,1)S(1)}, u32[]{:S(2)}, u32[]{:S(2)}) collective-permute-start(bf16[528,256]{1,0:T(8,128)(2,1)S(1)} %shard_map.149.own), channel_id=1, source_target_pairs={{0,64},{1,449},{64,0},{65,129},{128,192},{129,65},{192,128},{193,2... | collective-permute-start | bytes 811016 | tf_op jit(solution)/shard_map/ppermute | solution.py:41
  99.3 5.3 %collective-permute-start.10 = (bf16[2,192,2048]{2,1,0:T(8,128)(2,1)S(1)}, bf16[2,192,2048]{2,1,0:T(8,128)(2,1)S(1)}, u32[]{:S(2)}, u32[]{:S(2)}) collective-permute-start(bf16[2,192,2048]{2,1,0:T(8,128)(2,1)S(1)} %get-tuple-element.43), channel_id=1, source_target_pairs={{0,1},{1,0},{2,3},{3,2},{4,5},{5,4},{6,7},{7,6},{8,9},{9,8},{10,11... | collective-permute-start | bytes 4718600 | tf_op jit(solution)/shard_map/ppermute | solution.py:54
  101.2 11.3 %collective-permute-start.15 = (bf16[2,528,256]{2,1,0:T(8,128)(2,1)S(1)}, bf16[2,528,256]{2,1,0:T(8,128)(2,1)S(1)}, u32[]{:S(2)}, u32[]{:S(2)}) collective-permute-start(bf16[2,528,256]{2,1,0:T(8,128)(2,1)S(1)} %get-tuple-element.53), channel_id=1, source_target_pairs={{0,448},{1,65},{64,128},{65,1},{128,64},{129,193},{192,256},{193,1... | collective-permute-start | bytes 1622024 | tf_op jit(solution)/shard_map/ppermute | solution.py:41
  104.9 29.2 %collective-permute-start.11 = (bf16[2,96,2048]{2,1,0:T(8,128)(2,1)S(1)}, bf16[2,96,2048]{2,1,0:T(8,128)(2,1)S(1)}, u32[]{:S(2)}, u32[]{:S(2)}) collective-permute-start(bf16[2,96,2048]{2,1,0:T(8,128)(2,1)S(1)} %get-tuple-element.45), channel_id=1, source_target_pairs={{0,2},{1,7},{2,0},{3,5},{4,6},{5,3},{6,4},{7,1},{8,10},{9,15},{10,... | collective-permute-start | bytes 2359304 | tf_op jit(solution)/shard_map/ppermute | solution.py:41
  112.9 12.5 %collective-permute-start.16 = (bf16[2,528,256]{2,1,0:T(8,128)(2,1)S(1)}, bf16[2,528,256]{2,1,0:T(8,128)(2,1)S(1)}, u32[]{:S(2)}, u32[]{:S(2)}) collective-permute-start(bf16[2,528,256]{2,1,0:T(8,128)(2,1)S(1)} %shard_map.160), channel_id=1, source_target_pairs={{0,64},{1,449},{64,0},{65,129},{128,192},{129,65},{192,128},{193,2... | collective-permute-start | bytes 1622024 | tf_op jit(solution)/shard_map/ppermute | solution.py:41
  118.4 17.8 %collective-permute-start.14 = (bf16[1,528,256]{2,1,0:T(8,128)(2,1)S(1)}, bf16[1,528,256]{2,1,0:T(8,128)(2,1)S(1)}, u32[]{:S(2)}, u32[]{:S(2)}) collective-permute-start(bf16[1,528,256]{2,1,0:T(8,128)(2,1)S(1)} %shard_map.159), channel_id=1, source_target_pairs={{0,64},{1,449},{64,0},{65,129},{128,192},{129,65},{192,128},{193,2... | collective-permute-start | bytes 811016 | tf_op jit(solution)/shard_map/ppermute | solution.py:41
  125.8 11.3 %collective-permute-start.17 = (bf16[1,528,256]{2,1,0:T(8,128)(2,1)S(1)}, bf16[1,528,256]{2,1,0:T(8,128)(2,1)S(1)}, u32[]{:S(2)}, u32[]{:S(2)}) collective-permute-start(bf16[1,528,256]{2,1,0:T(8,128)(2,1)S(1)} %get-tuple-element.54), channel_id=1, source_target_pairs={{0,448},{1,65},{64,128},{65,1},{128,64},{129,193},{192,256},{193,1... | collective-permute-start | bytes 811016 | tf_op jit(solution)/shard_map/ppermute | solution.py:41
  127.8 14.9 %collective-permute-start.18 = (bf16[1,528,256]{2,1,0:T(8,128)(2,1)S(1)}, bf16[1,528,256]{2,1,0:T(8,128)(2,1)S(1)}, u32[]{:S(2)}, u32[]{:S(2)}) collective-permute-start(bf16[1,528,256]{2,1,0:T(8,128)(2,1)S(1)} %get-tuple-element.55), channel_id=1, source_target_pairs={{0,384},{1,129},{64,192},{65,449},{128,0},{129,257},{192,320},{193... | collective-permute-start | bytes 811016 | tf_op jit(solution)/shard_map/ppermute | solution.py:50
  134.3 13.4 %collective-permute-start.12 = (bf16[2,48,2048]{2,1,0:T(8,128)(2,1)S(1)}, bf16[2,48,2048]{2,1,0:T(8,128)(2,1)S(1)}, u32[]{:S(2)}, u32[]{:S(2)}) collective-permute-start(bf16[2,48,2048]{2,1,0:T(8,128)(2,1)S(1)} %get-tuple-element.47), channel_id=1, source_target_pairs={{0,8},{8,0},{1,9},{9,1},{2,10},{10,2},{3,11},{11,3},{4,12},{12,4},... | collective-permute-start | bytes 1179656 | tf_op jit(solution)/shard_map/ppermute | solution.py:54
  137.6 12.1 %copy-start.6 = (bf16[2048]{0:T(1024)(128)(2,1)S(1)}, bf16[2048]{0:T(1024)(128)(2,1)}, u32[]{:S(2)}) copy-start(bf16[2048]{0:T(1024)(128)(2,1)} %g_hbm.2) | copy-start | bytes 12292
  137.6 20.1 %copy-start.3 = (f32[32,352]{1,0:T(8,128)S(1)}, f32[32,352]{1,0:T(8,128)}, u32[]{:S(2)}) copy-start(f32[32,352]{1,0:T(8,128)} %gs.1) | copy-start | bytes 135172
  137.6 20.1 %copy-start.4 = (f32[32,352]{1,0:T(8,128)S(1)}, f32[32,352]{1,0:T(8,128)}, u32[]{:S(2)}) copy-start(f32[32,352]{1,0:T(8,128)} %us.1) | copy-start | bytes 135172
  137.6 20.1 %copy-start.5 = (f32[32,352]{1,0:T(8,128)S(1)}, f32[32,352]{1,0:T(8,128)}, u32[]{:S(2)}) copy-start(f32[32,352]{1,0:T(8,128)} %ds.1) | copy-start | bytes 135172
  143.6 14.9 %copy-start = (bf16[24,2048]{1,0:T(8,128)(2,1)S(1)}, bf16[24,2048]{1,0:T(8,128)(2,1)}, u32[]{:S(2)}) copy-start(bf16[24,2048]{1,0:T(8,128)(2,1)} %e_ref.1) | copy-start | bytes 294916
  143.6 14.9 %copy-start.1 = (bf16[24,2048]{1,0:T(8,128)(2,1)S(1)}, bf16[24,2048]{1,0:T(8,128)(2,1)}, u32[]{:S(2)}) copy-start(bf16[24,2048]{1,0:T(8,128)(2,1)} %c_ref.1) | copy-start | bytes 294916
  143.6 14.9 %copy-start.2 = (bf16[24,2048]{1,0:T(8,128)(2,1)S(1)}, bf16[24,2048]{1,0:T(8,128)(2,1)}, u32[]{:S(2)}) copy-start(bf16[24,2048]{1,0:T(8,128)(2,1)} %l_ref.1) | copy-start | bytes 294916
  143.6 14.1 %all-to-all-start.1 = ((bf16[8,136,128]{2,1,0:T(8,128)(2,1)}), bf16[8,136,128]{2,1,0:T(8,128)(2,1)S(1)}, u32[]{:S(2)}, u32[]{:S(2)}) async-start(bf16[8,136,128]{2,1,0:T(8,128)(2,1)} %shard_map.163), calls=%async_computation.1 | async-start | bytes 557056 | tf_op jit(solution)/shard_map/all_to_all | solution.py:58
  147.8 10.7 %collective-permute-start.13 = (bf16[2,24,2048]{2,1,0:T(8,128)(2,1)S(1)}, bf16[2,24,2048]{2,1,0:T(8,128)(2,1)S(1)}, u32[]{:S(2)}, u32[]{:S(2)}) collective-permute-start(bf16[2,24,2048]{2,1,0:T(8,128)(2,1)S(1)} %get-tuple-element.49), channel_id=1, source_target_pairs={{0,6},{1,3},{2,4},{3,1},{4,2},{5,7},{6,0},{7,5},{8,14},{9,11},{10,... | collective-permute-start | bytes 589832 | tf_op jit(solution)/shard_map/ppermute | solution.py:41

commit v3 on v2

--- a/solution.py
+++ b/solution.py
@@ -88,22 +88,19 @@
     return jnp.concatenate([shift(x, -16 * j) for j in range(4)], axis=axis)
 
 
-def fetch(pairs, sem):
-    copies = [pltpu.make_async_copy(a, b, sem.at[i]) for i, (a, b) in enumerate(pairs)]
-    for copy in copies:
-        copy.start()
-    for copy in copies:
-        copy.wait()
-
-
 def normalize(x, gain):
     inv = lax.rsqrt(jnp.mean(x * x, axis=-1, keepdims=True) + eps)
     return inv, x * inv * gain
 
 
-def pack_weights(g_hbm, u_hbm, d_hbm, o_ref, g_ref, u_ref, d_ref, sem):
-    fetch(((g_hbm, g_ref), (u_hbm, u_ref), (d_hbm, d_ref)), sem)
-    weights = (g_ref, u_ref, d_ref)
+def prepare(*refs):
+    (w_out, t_out), scratch, sem = refs[7:9], refs[9:16], refs[16]
+    copies = [pltpu.make_async_copy(a, b, sem.at[i]) for i, (a, b) in enumerate(zip(refs[:7], scratch, strict=True))]
+    for copy in copies:
+        copy.start()
+    for copy in copies[:3]:
+        copy.wait()
+    weights, (early, cot, late, gain) = scratch[:3], scratch[3:]
     tails = []
     for r in weights:
         tail = r[:, 256:352].astype(f32)
@@ -115,17 +112,15 @@
         rest = fold_rows(d, at + 32, 0)
         for q in range(4):
             for i, r in enumerate(weights):
-                o_ref[2 * q + h, ROWS * i : ROWS * (i + 1)] = r[:, h * MAIN : (h + 1) * MAIN]
-            o_ref[2 * q + h, 96:128] = tail.astype(bf16)
-            o_ref[2 * q + h, 128:136] = rest.astype(bf16)
-
-
-def prepare_tokens(e_hbm, c_hbm, l_hbm, g_hbm, o_ref, early, cot, late, gain, sem):
-    fetch(((e_hbm, early), (c_hbm, cot), (l_hbm, late), (g_hbm, gain)), sem)
+                w_out[2 * q + h, ROWS * i : ROWS * (i + 1)] = r[:, h * MAIN : (h + 1) * MAIN]
+            w_out[2 * q + h, 96:128] = tail.astype(bf16)
+            w_out[2 * q + h, 128:136] = rest.astype(bf16)
+    for copy in copies[3:]:
+        copy.wait()
     gain = gain[...].astype(f32).reshape(1, 2048)
-    o_ref[0] = normalize(early[...].astype(f32), gain)[1].astype(bf16)
-    o_ref[1] = (0.5 * cot[...].astype(f32)).astype(bf16)
-    o_ref[2] = normalize(late[...].astype(f32), gain)[1].astype(bf16)
+    t_out[0] = normalize(early[...].astype(f32), gain)[1].astype(bf16)
+    t_out[1] = (0.5 * cot[...].astype(f32)).astype(bf16)
+    t_out[2] = normalize(late[...].astype(f32), gain)[1].astype(bf16)
 
 
 def turn_block(r_ref, o_ref):
@@ -217,14 +212,14 @@
     grad_block(at_ref, (te0, te1), (th0, th1), 1, o_ref, 0)
 
 
-def own_block(at_ref, te0, te1, th0, th1, r_ref, q_ref, o_ref, f):
+def own_block(at_ref, te0, te1, th0, th1, q_ref, o_ref, f):
+    grad_block(at_ref, (te0, te1), (th0, th1), 0, f, 0, q_ref[0])
+    o_ref[...] = turned(f[0])
+
+
+def last_block(f_ref, r_ref, q_ref, o_ref):
     both = r_ref[0].astype(f32) + q_ref[0].astype(f32)
-    grad_block(at_ref, (te0, te1), (th0, th1), 0, f, 0, both)
-    o_ref[...] = turned(f[0])
-
-
-def last_block(f_ref, r_ref, o_ref):
-    o_ref[...] = (f_ref[...] + turned(r_ref[0])).astype(bf16)
+    o_ref[...] = (f_ref[...] + turned(both)).astype(bf16)
 
 
 def token_parts(b_ref, dg_ref, du_ref, tl0, tl1, own, got, p1, p2, p3, near, far, w):
@@ -316,19 +311,14 @@
     order = jnp.array([0, 1, -1, -2, 2, 3, -3, -4], jnp.int32)
     blocks = lax.rem(z + order * step + 8, 8).astype(jnp.int32)
 
-    def staged(body, dims, *given):
-        n = len(given)
-        return call(
-            body,
-            shape(dims),
-            *(pltpu.with_memory_space_constraint(a, pltpu.HBM) for a in given),
-            in_specs=[HB] * n,
-            scratch_shapes=[pltpu.VMEM(a.shape, bf16) for a in given]
-            + [pltpu.SemaphoreType.DMA((n,))],
-        )
-
-    sent = staged(pack_weights, (NY, PACK, 128), gate_weight, up_weight, down_weight)
-    tok = staged(prepare_tokens, (3, 24, 2048), x_early, cotangent, x_late, norm_gain)
+    given = (gate_weight, up_weight, down_weight, x_early, cotangent, x_late, norm_gain)
+    sent, tok = call(
+        prepare,
+        (shape((NY, PACK, 128)), shape((3, 24, 2048))),
+        *(pltpu.with_memory_space_constraint(a, pltpu.HBM) for a in given),
+        in_specs=[HB] * 7,
+        scratch_shapes=[pltpu.VMEM(a.shape, bf16) for a in given] + [pltpu.SemaphoreType.DMA((7,))],
+    )
     own = call(turn_block, shape((3 * HALF, 256)), over_y(sent))
     got = exchange(own, "z", NZ, 0)
     far = hop_two(own, 1)
@@ -379,10 +369,10 @@
     block = call(
         own_block,
         shape((NY, PACK, 128), f32),
-        *tokens, mine, r1,
+        *tokens, mine,
         scratch_shapes=[pltpu.VMEM((1, 3 * HALF, 256), f32)],
     )
-    back = call(last_block, shape((NY, PACK, 128)), block, r0)
+    back = call(last_block, shape((NY, PACK, 128)), block, r0, r1)
     sums = call(
         finish_weights,
         (shape((ROWS, 352), f32),) * 3,

time: 160 us -> 160 us (level)
  the two profiles are of different devices: /device:TPU:64 before, /device:TPU:1 now
where the time goes in v3:
time: 160 us
  starting transfers between devices  73.2 us (46%)
  waiting for transfers between devices  53.2 us (33%)
  blocking collectives  16.7 us (10%)
  Pallas kernels  15.2 us (10%)
    ppermute x12, starting transfers between devices, exchange(): return lax.ppermute(x, (axis, 'c'), pairs)  43.2 us
    ppermute x12, waiting for transfers between devices, exchange(): return lax.ppermute(x, (axis, 'c'), pairs)  36.1 us
    all_to_all x1, blocking collectives, over_y(): lax.all_to_all(x, ('yq', 'ys'), split_axis=0, concat_axis=0, tiled=True)  16.7 us
    pallas_call x18, Pallas kernels, call(): pl.pallas_call(body, out_shape=out_shape, compiler_params=pltpu.CompilerP...  15.2 us
    ppermute x5, starting transfers between devices, swapped(): return lax.ppermute(x, axis, [(0, 1), (1, 0)])  14.9 us
    ppermute x2, starting transfers between devices, hop_two(): return lax.ppermute(x, ('z', 'c'), pairs)  11.7 us
    all_to_all x1, waiting for transfers between devices, over_y(): lax.all_to_all(x, ('yq', 'ys'), split_axis=0, concat_axis=0, tiled=True)  9.4 us
    ppermute x5, waiting for transfers between devices, swapped(): return lax.ppermute(x, axis, [(0, 1), (1, 0)])  5.16 us
  transfers between devices with their start and end apart: 20, of which 10 were waited for; matrix products, arithmetic and copies ran while one was open for 0% of the time, Pallas kernels for 5%

profile of v3, /device:TPU:1, one launch (start us, length us, event | category | flops | bytes accessed | tf_op | source)
XLA Modules:
  0.0 159.5 jit_solution(736634530013958522)
XLA Ops:
  1.9 4.0 %collective-permute-start = (bf16[3,24,2048]{2,1,0:T(8,128)(2,1)S(1)}, bf16[3,24,2048]{2,1,0:T(8,128)(2,1)S(1)}, u32[]{:S(2)}, u32[]{:S(2)}) collective-permute-start(bf16[3,24,2048]{2,1,0:T(8,128)(2,1)S(1)} %get-tuple-element.34), channel_id=1, source_target_pairs={{0,8},{8,0},{1,9},{9,1},{2,10},{10,2},{3,11},{11,3},{4,12},{12,4},... | collective-permute-start | bytes 884744 | tf_op jit(solution)/shard_map/ppermute | solution.py:54
  5.9 4.1 %collective-permute-done = bf16[3,24,2048]{2,1,0:T(8,128)(2,1)S(1)} collective-permute-done((bf16[3,24,2048]{2,1,0:T(8,128)(2,1)S(1)}, bf16[3,24,2048]{2,1,0:T(8,128)(2,1)S(1)}, u32[]{:S(2)}, u32[]{:S(2)}) %collective-permute-start) | collective-permute-done | bytes 294944 | tf_op jit(solution)/shard_map/ppermute | solution.py:54
  10.0 5.6 %collective-permute-start.1 = (bf16[3,48,2048]{2,1,0:T(8,128)(2,1)S(1)}, bf16[3,48,2048]{2,1,0:T(8,128)(2,1)S(1)}, u32[]{:S(2)}, u32[]{:S(2)}) collective-permute-start(bf16[3,48,2048]{2,1,0:T(8,128)(2,1)S(1)} %constant_dynamic-update-slice_fusion.a_ref), channel_id=1, source_target_pairs={{0,6},{1,3},{2,4},{3,1},{4,2},{5,7},{6,0},{7,5},{8,14},{9,11},{10,... | collective-permute-start | bytes 1769480 | tf_op jit(solution)/shard_map/ppermute | solution.py:41
  15.6 7.3 %collective-permute-done.1.b_ref = bf16[3,48,2048]{2,1,0:T(8,128)(2,1)S(1)} collective-permute-done((bf16[3,48,2048]{2,1,0:T(8,128)(2,1)S(1)}, bf16[3,48,2048]{2,1,0:T(8,128)(2,1)S(1)}, u32[]{:S(2)}, u32[]{:S(2)}) %collective-permute-start.1) | collective-permute-done | bytes 589856 | tf_op jit(solution)/shard_map/ppermute | solution.py:41
  23.0 4.9 %collective-permute-start.2 = (bf16[2,3,48,2048]{3,2,1,0:T(8,128)(2,1)S(1)}, bf16[2,3,48,2048]{3,2,1,0:T(8,128)(2,1)}, u32[]{:S(2)}, u32[]{:S(2)}) collective-permute-start(bf16[2,3,48,2048]{3,2,1,0:T(8,128)(2,1)S(1)} %shard_map.147.ta), channel_id=1, source_target_pairs={{0,2},{1,7},{2,0},{3,5},{4,6},{5,3},{6,4},{7,1},{8,10},{9,15},{10,... | collective-permute-start | bytes 3538952 | tf_op jit(solution)/shard_map/ppermute | solution.py:41
  27.9 16.7 %all_to_all.10.r_ref = bf16[8,136,128]{2,1,0:T(8,128)(2,1)S(1)} all-to-all(bf16[8,136,128]{2,1,0:T(8,128)(2,1)S(1)} %get-tuple-element.35), channel_id=1, replica_groups=mesh['z'=8,'yq'=4,'ys'=2,'x'=4,'c'=2] {'yq','ys'}, dimensions={0} | all-to-all | bytes 557056 | tf_op jit(solution)/shard_map/all_to_all | solution.py:58
  44.8 4.0 %collective-permute-start.4 = (bf16[528,256]{1,0:T(8,128)(2,1)S(1)}, bf16[528,256]{1,0:T(8,128)(2,1)S(1)}, u32[]{:S(2)}, u32[]{:S(2)}) collective-permute-start(bf16[528,256]{1,0:T(8,128)(2,1)S(1)} %shard_map.148.own), channel_id=1, source_target_pairs={{0,448},{1,65},{64,128},{65,1},{128,64},{129,193},{192,256},{193,1... | collective-permute-start | bytes 811016 | tf_op jit(solution)/shard_map/ppermute | solution.py:41
  48.8 9.8 %collective-permute-start.5 = (bf16[528,256]{1,0:T(8,128)(2,1)S(1)}, bf16[528,256]{1,0:T(8,128)(2,1)S(1)}, u32[]{:S(2)}, u32[]{:S(2)}) collective-permute-start(bf16[528,256]{1,0:T(8,128)(2,1)S(1)} %shard_map.148.own), channel_id=1, source_target_pairs={{0,128},{1,385},{64,448},{65,193},{128,256},{129,1},{192,64},{193,... | collective-permute-start | bytes 811016 | tf_op jit(solution)/shard_map/ppermute | solution.py:50
  58.6 4.2 %collective-permute-start.7 = (bf16[2,3,48,2048]{3,2,1,0:T(8,128)(2,1)S(1)}, bf16[2,3,48,2048]{3,2,1,0:T(8,128)(2,1)}, u32[]{:S(2)}, u32[]{:S(2)}) collective-permute-start(bf16[2,3,48,2048]{3,2,1,0:T(8,128)(2,1)S(1)} %shard_map.147.ta), channel_id=1, source_target_pairs={{0,1},{1,0},{2,3},{3,2},{4,5},{5,4},{6,7},{7,6},{8,9},{9,8},{10,11... | collective-permute-start | bytes 3538952 | tf_op jit(solution)/shard_map/ppermute | solution.py:54
  62.7 1.9 %collective-permute-start.8 = (bf16[2,3,48,2048]{3,2,1,0:T(8,128)(2,1)}, bf16[2,3,48,2048]{3,2,1,0:T(8,128)(2,1)}, u32[]{:S(2)}, u32[]{:S(2)}) collective-permute-start(bf16[2,3,48,2048]{3,2,1,0:T(8,128)(2,1)} %collective-permute-done.2.tb), channel_id=1, source_target_pairs={{0,1},{1,0},{2,3},{3,2},{4,5},{5,4},{6,7},{7,6},{8,9},{9,8},{10,11... | collective-permute-start | bytes 3538952 | tf_op jit(solution)/shard_map/ppermute | solution.py:54
  64.7 2.6 %collective-permute-done.5.b_ref = bf16[528,256]{1,0:T(8,128)(2,1)S(1)} collective-permute-done((bf16[528,256]{1,0:T(8,128)(2,1)S(1)}, bf16[528,256]{1,0:T(8,128)(2,1)S(1)}, u32[]{:S(2)}, u32[]{:S(2)}) %collective-permute-start.5) | collective-permute-done | bytes 270368 | tf_op jit(solution)/shard_map/ppermute | solution.py:50
  67.3 4.1 %collective-permute-start.6 = (bf16[2,528,256]{2,1,0:T(8,128)(2,1)S(1)}, bf16[2,528,256]{2,1,0:T(8,128)(2,1)S(1)}, u32[]{:S(2)}, u32[]{:S(2)}) collective-permute-start(bf16[2,528,256]{2,1,0:T(8,128)(2,1)S(1)} %shard_map.149.p1), channel_id=1, source_target_pairs={{0,64},{1,449},{64,0},{65,129},{128,192},{129,65},{192,128},{193,2... | collective-permute-start | bytes 1622024 | tf_op jit(solution)/shard_map/ppermute | solution.py:41
  71.4 7.2 %collective-permute-done.6.p2 = bf16[2,528,256]{2,1,0:T(8,128)(2,1)S(1)} collective-permute-done((bf16[2,528,256]{2,1,0:T(8,128)(2,1)S(1)}, bf16[2,528,256]{2,1,0:T(8,128)(2,1)S(1)}, u32[]{:S(2)}, u32[]{:S(2)}) %collective-permute-start.6) | collective-permute-done | bytes 540704 | tf_op jit(solution)/shard_map/ppermute | solution.py:41
  80.5 5.3 %collective-permute-start.3 = (bf16[528,256]{1,0:T(8,128)(2,1)S(1)}, bf16[528,256]{1,0:T(8,128)(2,1)S(1)}, u32[]{:S(2)}, u32[]{:S(2)}) collective-permute-start(bf16[528,256]{1,0:T(8,128)(2,1)S(1)} %shard_map.148.own), channel_id=1, source_target_pairs={{0,64},{1,449},{64,0},{65,129},{128,192},{129,65},{192,128},{193,2... | collective-permute-start | bytes 811016 | tf_op jit(solution)/shard_map/ppermute | solution.py:41
  85.8 6.6 %collective-permute-done.3.got = bf16[528,256]{1,0:T(8,128)(2,1)S(1)} collective-permute-done((bf16[528,256]{1,0:T(8,128)(2,1)S(1)}, bf16[528,256]{1,0:T(8,128)(2,1)S(1)}, u32[]{:S(2)}, u32[]{:S(2)}) %collective-permute-start.3) | collective-permute-done | bytes 270368 | tf_op jit(solution)/shard_map/ppermute | solution.py:41
  92.5 2.1 %shard_map.150 = (bf16[192,2048]{1,0:T(8,128)(2,1)S(1)}, bf16[192,2048]{1,0:T(8,128)(2,1)S(1)}, bf16[192,2048]{1,0:T(8,128)(2,1)S(1)}, f32[3,192,176]{2,1,0:T(8,128)S(1)}) custom-call(s32[8]{0:T(128)S(1)} %compare_select_fusion.b_ref, bf16[2,3,48,2048]{3,2,1,0:T(8,128)(2,1)S(1)} %shard_map.147.ta, bf16[2,3,48,2048]{3,2,1,0:T(8,128)(2,1)} %collective-permute-done.2.tb, ...), custom_call_target="tpu_custom_call" | custom-call | tf_op jit(solution)/shard_map/pallas_call | solution.py:27
  94.5 2.4 %shard_map.151 = (bf16[192,2048]{1,0:T(8,128)(2,1)S(1)}, bf16[192,2048]{1,0:T(8,128)(2,1)S(1)}, bf16[192,2048]{1,0:T(8,128)(2,1)S(1)}, f32[3,192,176]{2,1,0:T(8,128)S(1)}) custom-call(s32[8]{0:T(128)S(1)} %compare_select_fusion.b_ref, bf16[2,3,48,2048]{3,2,1,0:T(8,128)(2,1)} %collective-permute-done.7.ta, ...), custom_call_target="tpu_custom_call" | custom-call | tf_op jit(solution)/shard_map/pallas_call | solution.py:27
  98.1 3.2 %shard_map.153 = (f32[2,192,2048]{2,1,0:T(8,128)S(1)}, bf16[2,192,2048]{2,1,0:T(8,128)(2,1)S(1)}) custom-call(s32[8]{0:T(128)S(1)} %compare_select_fusion.b_ref, bf16[2,192,176]{2,1,0:T(8,128)(2,1)S(1)} %get-tuple-element.42.dg_ref, bf16[2,192,176]{2,1,0:T(8,128)(2,1)S(1)} %get-tuple-element.43.du_ref, bf16[192,2048]{1,0:T(8,128)(2,1)S(1)} %get-tuple-element.44.tl0, ...), custom_call_target="tpu_custom_call" | custom-call | tf_op jit(solution)/shard_map/pallas_call | solution.py:27
  101.4 2.9 %collective-permute-start.10 = (bf16[2,192,2048]{2,1,0:T(8,128)(2,1)S(1)}, bf16[2,192,2048]{2,1,0:T(8,128)(2,1)S(1)}, u32[]{:S(2)}, u32[]{:S(2)}) collective-permute-start(bf16[2,192,2048]{2,1,0:T(8,128)(2,1)S(1)} %get-tuple-element.47), channel_id=1, source_target_pairs={{0,1},{1,0},{2,3},{3,2},{4,5},{5,4},{6,7},{7,6},{8,9},{9,8},{10,11... | collective-permute-start | bytes 4718600 | tf_op jit(solution)/shard_map/ppermute | solution.py:54
  104.2 1.9 %collective-permute-start.15 = (bf16[2,528,256]{2,1,0:T(8,128)(2,1)S(1)}, bf16[2,528,256]{2,1,0:T(8,128)(2,1)S(1)}, u32[]{:S(2)}, u32[]{:S(2)}) collective-permute-start(bf16[2,528,256]{2,1,0:T(8,128)(2,1)S(1)} %get-tuple-element.57), channel_id=1, source_target_pairs={{0,448},{1,65},{64,128},{65,1},{128,64},{129,193},{192,256},{193,1... | collective-permute-start | bytes 1622024 | tf_op jit(solution)/shard_map/ppermute | solution.py:41
  107.6 1.9 %collective-permute-start.11 = (bf16[2,96,2048]{2,1,0:T(8,128)(2,1)S(1)}, bf16[2,96,2048]{2,1,0:T(8,128)(2,1)S(1)}, u32[]{:S(2)}, u32[]{:S(2)}) collective-permute-start(bf16[2,96,2048]{2,1,0:T(8,128)(2,1)S(1)} %get-tuple-element.49), channel_id=1, source_target_pairs={{0,2},{1,7},{2,0},{3,5},{4,6},{5,3},{6,4},{7,1},{8,10},{9,15},{10,... | collective-permute-start | bytes 2359304 | tf_op jit(solution)/shard_map/ppermute | solution.py:41
  109.5 5.1 %collective-permute-done.15.r_ref = bf16[2,528,256]{2,1,0:T(8,128)(2,1)S(1)} collective-permute-done((bf16[2,528,256]{2,1,0:T(8,128)(2,1)S(1)}, bf16[2,528,256]{2,1,0:T(8,128)(2,1)S(1)}, u32[]{:S(2)}, u32[]{:S(2)}) %collective-permute-start.15) | collective-permute-done | bytes 540704 | tf_op jit(solution)/shard_map/ppermute | solution.py:41
  115.1 4.0 %collective-permute-start.16 = (bf16[2,528,256]{2,1,0:T(8,128)(2,1)S(1)}, bf16[2,528,256]{2,1,0:T(8,128)(2,1)S(1)}, u32[]{:S(2)}, u32[]{:S(2)}) collective-permute-start(bf16[2,528,256]{2,1,0:T(8,128)(2,1)S(1)} %shard_map.160), channel_id=1, source_target_pairs={{0,64},{1,449},{64,0},{65,129},{128,192},{129,65},{192,128},{193,2... | collective-permute-start | bytes 1622024 | tf_op jit(solution)/shard_map/ppermute | solution.py:41
  119.4 2.5 %collective-permute-start.14 = (bf16[1,528,256]{2,1,0:T(8,128)(2,1)S(1)}, bf16[1,528,256]{2,1,0:T(8,128)(2,1)S(1)}, u32[]{:S(2)}, u32[]{:S(2)}) collective-permute-start(bf16[1,528,256]{2,1,0:T(8,128)(2,1)S(1)} %shard_map.158), channel_id=1, source_target_pairs={{0,64},{1,449},{64,0},{65,129},{128,192},{129,65},{192,128},{193,2... | collective-permute-start | bytes 811016 | tf_op jit(solution)/shard_map/ppermute | solution.py:41
  121.9 4.5 %collective-permute-done.16.r_ref = bf16[2,528,256]{2,1,0:T(8,128)(2,1)S(1)} collective-permute-done((bf16[2,528,256]{2,1,0:T(8,128)(2,1)S(1)}, bf16[2,528,256]{2,1,0:T(8,128)(2,1)S(1)}, u32[]{:S(2)}, u32[]{:S(2)}) %collective-permute-start.16) | collective-permute-done | bytes 540704 | tf_op jit(solution)/shard_map/ppermute | solution.py:41
  126.8 1.9 %collective-permute-start.17 = (bf16[1,528,256]{2,1,0:T(8,128)(2,1)S(1)}, bf16[1,528,256]{2,1,0:T(8,128)(2,1)S(1)}, u32[]{:S(2)}, u32[]{:S(2)}) collective-permute-start(bf16[1,528,256]{2,1,0:T(8,128)(2,1)S(1)} %get-tuple-element.58), channel_id=1, source_target_pairs={{0,384},{1,129},{64,192},{65,449},{128,0},{129,257},{192,320},{193... | collective-permute-start | bytes 811016 | tf_op jit(solution)/shard_map/ppermute | solution.py:50
  128.8 5.2 %collective-permute-start.18 = (bf16[1,528,256]{2,1,0:T(8,128)(2,1)S(1)}, bf16[1,528,256]{2,1,0:T(8,128)(2,1)S(1)}, u32[]{:S(2)}, u32[]{:S(2)}) collective-permute-start(bf16[1,528,256]{2,1,0:T(8,128)(2,1)S(1)} %get-tuple-element.59), channel_id=1, source_target_pairs={{0,448},{1,65},{64,128},{65,1},{128,64},{129,193},{192,256},{193,1... | collective-permute-start | bytes 811016 | tf_op jit(solution)/shard_map/ppermute | solution.py:41
  134.1 1.9 %collective-permute-start.12 = (bf16[2,48,2048]{2,1,0:T(8,128)(2,1)S(1)}, bf16[2,48,2048]{2,1,0:T(8,128)(2,1)S(1)}, u32[]{:S(2)}, u32[]{:S(2)}) collective-permute-start(bf16[2,48,2048]{2,1,0:T(8,128)(2,1)S(1)} %get-tuple-element.51), channel_id=1, source_target_pairs={{0,8},{8,0},{1,9},{9,1},{2,10},{10,2},{3,11},{11,3},{4,12},{12,4},... | collective-permute-start | bytes 1179656 | tf_op jit(solution)/shard_map/ppermute | solution.py:54
  136.6 5.4 %collective-permute-done.18.q_ref = bf16[1,528,256]{2,1,0:T(8,128)(2,1)S(1)} collective-permute-done((bf16[1,528,256]{2,1,0:T(8,128)(2,1)S(1)}, bf16[1,528,256]{2,1,0:T(8,128)(2,1)S(1)}, u32[]{:S(2)}, u32[]{:S(2)}) %collective-permute-start.18) | collective-permute-done | bytes 270368 | tf_op jit(solution)/shard_map/ppermute | solution.py:41
  143.0 3.4 %all-to-all-start.1 = ((bf16[8,136,128]{2,1,0:T(8,128)(2,1)}), bf16[8,136,128]{2,1,0:T(8,128)(2,1)S(1)}, u32[]{:S(2)}, u32[]{:S(2)}) async-start(bf16[8,136,128]{2,1,0:T(8,128)(2,1)} %shard_map.162), calls=%async_computation.1 | async-start | bytes 557056 | tf_op jit(solution)/shard_map/all_to_all | solution.py:58
  146.5 1.9 %collective-permute-start.13 = (bf16[2,24,2048]{2,1,0:T(8,128)(2,1)S(1)}, bf16[2,24,2048]{2,1,0:T(8,128)(2,1)S(1)}, u32[]{:S(2)}, u32[]{:S(2)}) collective-permute-start(bf16[2,24,2048]{2,1,0:T(8,128)(2,1)S(1)} %get-tuple-element.53), channel_id=1, source_target_pairs={{0,6},{1,3},{2,4},{3,1},{4,2},{5,7},{6,0},{7,5},{8,14},{9,11},{10,... | collective-permute-start | bytes 589832 | tf_op jit(solution)/shard_map/ppermute | solution.py:41
  148.5 9.4 %all-to-all-done.1.r_ref = bf16[8,136,128]{2,1,0:T(8,128)(2,1)S(1)} async-done(((bf16[8,136,128]{2,1,0:T(8,128)(2,1)}), bf16[8,136,128]{2,1,0:T(8,128)(2,1)S(1)}, u32[]{:S(2)}, u32[]{:S(2)}) %all-to-all-start.1) | async-done | bytes 278560 | tf_op jit(solution)/shard_map/all_to_all | solution.py:58
  (47 shorter events, 10.7 us)
Async XLA Ops:
  1.9 8.1 %collective-permute-start = (bf16[3,24,2048]{2,1,0:T(8,128)(2,1)S(1)}, bf16[3,24,2048]{2,1,0:T(8,128)(2,1)S(1)}, u32[]{:S(2)}, u32[]{:S(2)}) collective-permute-start(bf16[3,24,2048]{2,1,0:T(8,128)(2,1)S(1)} %get-tuple-element.34), channel_id=1, source_target_pairs={{0,8},{8,0},{1,9},{9,1},{2,10},{10,2},{3,11},{11,3},{4,12},{12,4},... | collective-permute-start | bytes 884744 | tf_op jit(solution)/shard_map/ppermute | solution.py:54
  10.0 12.9 %collective-permute-start.1 = (bf16[3,48,2048]{2,1,0:T(8,128)(2,1)S(1)}, bf16[3,48,2048]{2,1,0:T(8,128)(2,1)S(1)}, u32[]{:S(2)}, u32[]{:S(2)}) collective-permute-start(bf16[3,48,2048]{2,1,0:T(8,128)(2,1)S(1)} %constant_dynamic-update-slice_fusion.a_ref), channel_id=1, source_target_pairs={{0,6},{1,3},{2,4},{3,1},{4,2},{5,7},{6,0},{7,5},{8,14},{9,11},{10,... | collective-permute-start | bytes 1769480 | tf_op jit(solution)/shard_map/ppermute | solution.py:41
  23.0 62.8 %copy-start.7 = (s32[8]{0:T(128)S(1)}, s32[8]{0:T(128)}, u32[]{:S(2)}) copy-start(s32[8]{0:T(128)} %constant.24.clone) | copy-start | bytes 100
  23.0 39.7 %collective-permute-start.2 = (bf16[2,3,48,2048]{3,2,1,0:T(8,128)(2,1)S(1)}, bf16[2,3,48,2048]{3,2,1,0:T(8,128)(2,1)}, u32[]{:S(2)}, u32[]{:S(2)}) collective-permute-start(bf16[2,3,48,2048]{3,2,1,0:T(8,128)(2,1)S(1)} %shard_map.147.ta), channel_id=1, source_target_pairs={{0,2},{1,7},{2,0},{3,5},{4,6},{5,3},{6,4},{7,1},{8,10},{9,15},{10,... | collective-permute-start | bytes 3538952 | tf_op jit(solution)/shard_map/ppermute | solution.py:41
  44.8 19.9 %collective-permute-start.4 = (bf16[528,256]{1,0:T(8,128)(2,1)S(1)}, bf16[528,256]{1,0:T(8,128)(2,1)S(1)}, u32[]{:S(2)}, u32[]{:S(2)}) collective-permute-start(bf16[528,256]{1,0:T(8,128)(2,1)S(1)} %shard_map.148.own), channel_id=1, source_target_pairs={{0,448},{1,65},{64,128},{65,1},{128,64},{129,193},{192,256},{193,1... | collective-permute-start | bytes 811016 | tf_op jit(solution)/shard_map/ppermute | solution.py:41
  48.8 18.4 %collective-permute-start.5 = (bf16[528,256]{1,0:T(8,128)(2,1)S(1)}, bf16[528,256]{1,0:T(8,128)(2,1)S(1)}, u32[]{:S(2)}, u32[]{:S(2)}) collective-permute-start(bf16[528,256]{1,0:T(8,128)(2,1)S(1)} %shard_map.148.own), channel_id=1, source_target_pairs={{0,128},{1,385},{64,448},{65,193},{128,256},{129,1},{192,64},{193,... | collective-permute-start | bytes 811016 | tf_op jit(solution)/shard_map/ppermute | solution.py:50
  58.6 36.0 %collective-permute-start.7 = (bf16[2,3,48,2048]{3,2,1,0:T(8,128)(2,1)S(1)}, bf16[2,3,48,2048]{3,2,1,0:T(8,128)(2,1)}, u32[]{:S(2)}, u32[]{:S(2)}) collective-permute-start(bf16[2,3,48,2048]{3,2,1,0:T(8,128)(2,1)S(1)} %shard_map.147.ta), channel_id=1, source_target_pairs={{0,1},{1,0},{2,3},{3,2},{4,5},{5,4},{6,7},{7,6},{8,9},{9,8},{10,11... | collective-permute-start | bytes 3538952 | tf_op jit(solution)/shard_map/ppermute | solution.py:54
  62.7 31.8 %collective-permute-start.8 = (bf16[2,3,48,2048]{3,2,1,0:T(8,128)(2,1)}, bf16[2,3,48,2048]{3,2,1,0:T(8,128)(2,1)}, u32[]{:S(2)}, u32[]{:S(2)}) collective-permute-start(bf16[2,3,48,2048]{3,2,1,0:T(8,128)(2,1)} %collective-permute-done.2.tb), channel_id=1, source_target_pairs={{0,1},{1,0},{2,3},{3,2},{4,5},{5,4},{6,7},{7,6},{8,9},{9,8},{10,11... | collective-permute-start | bytes 3538952 | tf_op jit(solution)/shard_map/ppermute | solution.py:54
  67.3 11.3 %collective-permute-start.6 = (bf16[2,528,256]{2,1,0:T(8,128)(2,1)S(1)}, bf16[2,528,256]{2,1,0:T(8,128)(2,1)S(1)}, u32[]{:S(2)}, u32[]{:S(2)}) collective-permute-start(bf16[2,528,256]{2,1,0:T(8,128)(2,1)S(1)} %shard_map.149.p1), channel_id=1, source_target_pairs={{0,64},{1,449},{64,0},{65,129},{128,192},{129,65},{192,128},{193,2... | collective-permute-start | bytes 1622024 | tf_op jit(solution)/shard_map/ppermute | solution.py:41
  78.6 18.4 %collective-permute-start.9 = (bf16[2,528,256]{2,1,0:T(8,128)(2,1)S(1)}, bf16[2,528,256]{2,1,0:T(8,128)(2,1)S(1)}, u32[]{:S(2)}, u32[]{:S(2)}) collective-permute-start(bf16[2,528,256]{2,1,0:T(8,128)(2,1)S(1)} %collective-permute-done.6.p2), channel_id=1, source_target_pairs={{0,448},{1,65},{64,128},{65,1},{128,64},{129,193},{192,256},{193,1... | collective-permute-start | bytes 1622024 | tf_op jit(solution)/shard_map/ppermute | solution.py:41
  80.5 11.9 %collective-permute-start.3 = (bf16[528,256]{1,0:T(8,128)(2,1)S(1)}, bf16[528,256]{1,0:T(8,128)(2,1)S(1)}, u32[]{:S(2)}, u32[]{:S(2)}) collective-permute-start(bf16[528,256]{1,0:T(8,128)(2,1)S(1)} %shard_map.148.own), channel_id=1, source_target_pairs={{0,64},{1,449},{64,0},{65,129},{128,192},{129,65},{192,128},{193,2... | collective-permute-start | bytes 811016 | tf_op jit(solution)/shard_map/ppermute | solution.py:41
  101.4 5.9 %collective-permute-start.10 = (bf16[2,192,2048]{2,1,0:T(8,128)(2,1)S(1)}, bf16[2,192,2048]{2,1,0:T(8,128)(2,1)S(1)}, u32[]{:S(2)}, u32[]{:S(2)}) collective-permute-start(bf16[2,192,2048]{2,1,0:T(8,128)(2,1)S(1)} %get-tuple-element.47), channel_id=1, source_target_pairs={{0,1},{1,0},{2,3},{3,2},{4,5},{5,4},{6,7},{7,6},{8,9},{9,8},{10,11... | collective-permute-start | bytes 4718600 | tf_op jit(solution)/shard_map/ppermute | solution.py:54
  104.2 10.4 %collective-permute-start.15 = (bf16[2,528,256]{2,1,0:T(8,128)(2,1)S(1)}, bf16[2,528,256]{2,1,0:T(8,128)(2,1)S(1)}, u32[]{:S(2)}, u32[]{:S(2)}) collective-permute-start(bf16[2,528,256]{2,1,0:T(8,128)(2,1)S(1)} %get-tuple-element.57), channel_id=1, source_target_pairs={{0,448},{1,65},{64,128},{65,1},{128,64},{129,193},{192,256},{193,1... | collective-permute-start | bytes 1622024 | tf_op jit(solution)/shard_map/ppermute | solution.py:41
  107.6 26.4 %collective-permute-start.11 = (bf16[2,96,2048]{2,1,0:T(8,128)(2,1)S(1)}, bf16[2,96,2048]{2,1,0:T(8,128)(2,1)S(1)}, u32[]{:S(2)}, u32[]{:S(2)}) collective-permute-start(bf16[2,96,2048]{2,1,0:T(8,128)(2,1)S(1)} %get-tuple-element.49), channel_id=1, source_target_pairs={{0,2},{1,7},{2,0},{3,5},{4,6},{5,3},{6,4},{7,1},{8,10},{9,15},{10,... | collective-permute-start | bytes 2359304 | tf_op jit(solution)/shard_map/ppermute | solution.py:41
  115.1 11.3 %collective-permute-start.16 = (bf16[2,528,256]{2,1,0:T(8,128)(2,1)S(1)}, bf16[2,528,256]{2,1,0:T(8,128)(2,1)S(1)}, u32[]{:S(2)}, u32[]{:S(2)}) collective-permute-start(bf16[2,528,256]{2,1,0:T(8,128)(2,1)S(1)} %shard_map.160), channel_id=1, source_target_pairs={{0,64},{1,449},{64,0},{65,129},{128,192},{129,65},{192,128},{193,2... | collective-permute-start | bytes 1622024 | tf_op jit(solution)/shard_map/ppermute | solution.py:41
  119.4 16.6 %collective-permute-start.14 = (bf16[1,528,256]{2,1,0:T(8,128)(2,1)S(1)}, bf16[1,528,256]{2,1,0:T(8,128)(2,1)S(1)}, u32[]{:S(2)}, u32[]{:S(2)}) collective-permute-start(bf16[1,528,256]{2,1,0:T(8,128)(2,1)S(1)} %shard_map.158), channel_id=1, source_target_pairs={{0,64},{1,449},{64,0},{65,129},{128,192},{129,65},{192,128},{193,2... | collective-permute-start | bytes 811016 | tf_op jit(solution)/shard_map/ppermute | solution.py:41
  126.8 9.8 %collective-permute-start.17 = (bf16[1,528,256]{2,1,0:T(8,128)(2,1)S(1)}, bf16[1,528,256]{2,1,0:T(8,128)(2,1)S(1)}, u32[]{:S(2)}, u32[]{:S(2)}) collective-permute-start(bf16[1,528,256]{2,1,0:T(8,128)(2,1)S(1)} %get-tuple-element.58), channel_id=1, source_target_pairs={{0,384},{1,129},{64,192},{65,449},{128,0},{129,257},{192,320},{193... | collective-permute-start | bytes 811016 | tf_op jit(solution)/shard_map/ppermute | solution.py:50
  128.8 13.2 %collective-permute-start.18 = (bf16[1,528,256]{2,1,0:T(8,128)(2,1)S(1)}, bf16[1,528,256]{2,1,0:T(8,128)(2,1)S(1)}, u32[]{:S(2)}, u32[]{:S(2)}) collective-permute-start(bf16[1,528,256]{2,1,0:T(8,128)(2,1)S(1)} %get-tuple-element.59), channel_id=1, source_target_pairs={{0,448},{1,65},{64,128},{65,1},{128,64},{129,193},{192,256},{193,1... | collective-permute-start | bytes 811016 | tf_op jit(solution)/shard_map/ppermute | solution.py:41
  134.1 12.4 %collective-permute-start.12 = (bf16[2,48,2048]{2,1,0:T(8,128)(2,1)S(1)}, bf16[2,48,2048]{2,1,0:T(8,128)(2,1)S(1)}, u32[]{:S(2)}, u32[]{:S(2)}) collective-permute-start(bf16[2,48,2048]{2,1,0:T(8,128)(2,1)S(1)} %get-tuple-element.51), channel_id=1, source_target_pairs={{0,8},{8,0},{1,9},{9,1},{2,10},{10,2},{3,11},{11,3},{4,12},{12,4},... | collective-permute-start | bytes 1179656 | tf_op jit(solution)/shard_map/ppermute | solution.py:54
  136.5 11.9 %copy-start.6 = (bf16[2048]{0:T(1024)(128)(2,1)S(1)}, bf16[2048]{0:T(1024)(128)(2,1)}, u32[]{:S(2)}) copy-start(bf16[2048]{0:T(1024)(128)(2,1)} %refs_6_.1) | copy-start | bytes 12292
  136.5 21.3 %copy-start.3 = (f32[32,352]{1,0:T(8,128)S(1)}, f32[32,352]{1,0:T(8,128)}, u32[]{:S(2)}) copy-start(f32[32,352]{1,0:T(8,128)} %gs.1) | copy-start | bytes 135172
  136.6 21.3 %copy-start.4 = (f32[32,352]{1,0:T(8,128)S(1)}, f32[32,352]{1,0:T(8,128)}, u32[]{:S(2)}) copy-start(f32[32,352]{1,0:T(8,128)} %us.1) | copy-start | bytes 135172
  136.6 21.3 %copy-start.5 = (f32[32,352]{1,0:T(8,128)S(1)}, f32[32,352]{1,0:T(8,128)}, u32[]{:S(2)}) copy-start(f32[32,352]{1,0:T(8,128)} %ds.1) | copy-start | bytes 135172
  136.6 22.1 %copy-start = (bf16[24,2048]{1,0:T(8,128)(2,1)S(1)}, bf16[24,2048]{1,0:T(8,128)(2,1)}, u32[]{:S(2)}) copy-start(bf16[24,2048]{1,0:T(8,128)(2,1)} %e_ref.1) | copy-start | bytes 294916
  136.6 22.1 %copy-start.1 = (bf16[24,2048]{1,0:T(8,128)(2,1)S(1)}, bf16[24,2048]{1,0:T(8,128)(2,1)}, u32[]{:S(2)}) copy-start(bf16[24,2048]{1,0:T(8,128)(2,1)} %c_ref.1) | copy-start | bytes 294916
  136.6 22.1 %copy-start.2 = (bf16[24,2048]{1,0:T(8,128)(2,1)S(1)}, bf16[24,2048]{1,0:T(8,128)(2,1)}, u32[]{:S(2)}) copy-start(bf16[24,2048]{1,0:T(8,128)(2,1)} %l_ref.1) | copy-start | bytes 294916
  143.0 14.9 %all-to-all-start.1 = ((bf16[8,136,128]{2,1,0:T(8,128)(2,1)}), bf16[8,136,128]{2,1,0:T(8,128)(2,1)S(1)}, u32[]{:S(2)}, u32[]{:S(2)}) async-start(bf16[8,136,128]{2,1,0:T(8,128)(2,1)} %shard_map.162), calls=%async_computation.1 | async-start | bytes 557056 | tf_op jit(solution)/shard_map/all_to_all | solution.py:58
  146.5 12.1 %collective-permute-start.13 = (bf16[2,24,2048]{2,1,0:T(8,128)(2,1)S(1)}, bf16[2,24,2048]{2,1,0:T(8,128)(2,1)S(1)}, u32[]{:S(2)}, u32[]{:S(2)}) collective-permute-start(bf16[2,24,2048]{2,1,0:T(8,128)(2,1)S(1)} %get-tuple-element.53), channel_id=1, source_target_pairs={{0,6},{1,3},{2,4},{3,1},{4,2},{5,7},{6,0},{7,5},{8,14},{9,11},{10,... | collective-permute-start | bytes 589832 | tf_op jit(solution)/shard_map/ppermute | solution.py:41

commit v4 on v3

--- a/solution.py
+++ b/solution.py
@@ -198,14 +198,18 @@
         grad_block(at_ref, (te0, te1), (th0, th1), 6 + n, s_ref, n)
 
 
-def add_pair(k, at_ref, te0, te1, th0, th1, r_ref, o_ref):
+def shares(k, at_ref, te0, te1, th0, th1, o_ref):
     for n in range(2):
-        grad_block(at_ref, (te0, te1), (th0, th1), k + n, o_ref, n, r_ref[n])
-
-
-def add_each(at_ref, te0, te1, th0, th1, r_ref, o_ref, p_ref):
+        grad_block(at_ref, (te0, te1), (th0, th1), k + n, o_ref, n)
+
+
+def add_pair(f_ref, r_ref, o_ref):
+    o_ref[...] = (f_ref[...] + r_ref[...].astype(f32)).astype(bf16)
+
+
+def add_each(f_ref, r_ref, o_ref, p_ref):
     for n, o in enumerate((o_ref, p_ref)):
-        grad_block(at_ref, (te0, te1), (th0, th1), 2 + n, o, 0, r_ref[n])
+        o[0] = (f_ref[n] + r_ref[n].astype(f32)).astype(bf16)
 
 
 def neighbour_share(at_ref, te0, te1, th0, th1, o_ref):
@@ -217,9 +221,8 @@
     o_ref[...] = turned(f[0])
 
 
-def last_block(f_ref, r_ref, q_ref, o_ref):
-    both = r_ref[0].astype(f32) + q_ref[0].astype(f32)
-    o_ref[...] = (f_ref[...] + turned(both)).astype(bf16)
+def last_block(f_ref, r_ref, o_ref):
+    o_ref[...] = (f_ref[...] + turned(r_ref[0])).astype(o_ref.dtype)
 
 
 def token_parts(b_ref, dg_ref, du_ref, tl0, tl1, own, got, p1, p2, p3, near, far, w):
@@ -359,11 +362,13 @@
         in_specs=[SM] + [VM] * 9,
         scratch_shapes=[pltpu.VMEM((2 * HALF, 2048), bf16)],
     )
-    s2 = call(functools.partial(add_pair, 4), pair, *tokens, r3)
+    both = shape((2, 3 * HALF, 256), f32)
+    s2 = call(add_pair, pair, call(functools.partial(shares, 4), both, *tokens), r3)
     r2 = exchange(s2, "z", NZ, 0)
     one = shape((1, 3 * HALF, 256))
     mine = exchange(call(neighbour_share, one, *tokens), "z", NZ, 0)
-    s1, s0 = call(add_each, (one, one), *tokens, r2)
+    pre = call(functools.partial(shares, 2), both, *tokens)
+    s1, s0 = call(add_each, (one, one), pre, r2)
     r0 = hop_two(s0, -1)
     r1 = exchange(s1, "z", NZ, 1)
     block = call(
@@ -372,7 +377,8 @@
         *tokens, mine,
         scratch_shapes=[pltpu.VMEM((1, 3 * HALF, 256), f32)],
     )
-    back = call(last_block, shape((NY, PACK, 128)), block, r0, r1)
+    block = call(last_block, shape((NY, PACK, 128), f32), block, r0)
+    back = call(last_block, shape((NY, PACK, 128)), block, r1)
     sums = call(
         finish_weights,
         (shape((ROWS, 352), f32),) * 3,

time: 160 us -> 160 us (level)
    pallas_call x18 -> x21, Pallas kernels: 15.2 us -> 15.6 us  [call(): pl.pallas_call(body, out_shape=out_shape, compiler_params=pltpu.CompilerP...]
  transfers between devices with their start and end apart: 20 -> 20, of which waited for: 10 -> 10; matrix products, arithmetic and copies ran while one was open for 0% -> 0% of each run, Pallas kernels for 5% -> 6%
where the time goes in v4:
time: 160 us; the launch traced here: 159 us
  starting transfers between devices  73.3 us (46%)
  waiting for transfers between devices  52 us (32%)
  blocking collectives  16.7 us (10%)
  Pallas kernels  15.6 us (10%)
    ppermute x12, starting transfers between devices, exchange(): return lax.ppermute(x, (axis, 'c'), pairs)  43.2 us
    ppermute x12, waiting for transfers between devices, exchange(): return lax.ppermute(x, (axis, 'c'), pairs)  35 us
    all_to_all x1, blocking collectives, over_y(): lax.all_to_all(x, ('yq', 'ys'), split_axis=0, concat_axis=0, tiled=True)  16.7 us
    pallas_call x21, Pallas kernels, call(): pl.pallas_call(body, out_shape=out_shape, compiler_params=pltpu.CompilerP...  15.6 us
    ppermute x5, starting transfers between devices, swapped(): return lax.ppermute(x, axis, [(0, 1), (1, 0)])  14.9 us
    ppermute x2, starting transfers between devices, hop_two(): return lax.ppermute(x, ('z', 'c'), pairs)  11.7 us
    all_to_all x1, waiting for transfers between devices, over_y(): lax.all_to_all(x, ('yq', 'ys'), split_axis=0, concat_axis=0, tiled=True)  9.33 us
    ppermute x5, waiting for transfers between devices, swapped(): return lax.ppermute(x, axis, [(0, 1), (1, 0)])  5.16 us
  transfers between devices with their start and end apart: 20, of which 10 were waited for; matrix products, arithmetic and copies ran while one was open for 0% of the time, Pallas kernels for 6%

profile of v4, /device:TPU:1, one launch (start us, length us, event | category | flops | bytes accessed | tf_op | source)
XLA Modules:
  0.0 158.8 jit_solution(8358119779314013587)
XLA Ops:
  1.9 4.0 %collective-permute-start = (bf16[3,24,2048]{2,1,0:T(8,128)(2,1)S(1)}, bf16[3,24,2048]{2,1,0:T(8,128)(2,1)S(1)}, u32[]{:S(2)}, u32[]{:S(2)}) collective-permute-start(bf16[3,24,2048]{2,1,0:T(8,128)(2,1)S(1)} %get-tuple-element.34), channel_id=1, source_target_pairs={{0,8},{8,0},{1,9},{9,1},{2,10},{10,2},{3,11},{11,3},{4,12},{12,4},... | collective-permute-start | bytes 884744 | tf_op jit(solution)/shard_map/ppermute | solution.py:54
  5.9 4.1 %collective-permute-done = bf16[3,24,2048]{2,1,0:T(8,128)(2,1)S(1)} collective-permute-done((bf16[3,24,2048]{2,1,0:T(8,128)(2,1)S(1)}, bf16[3,24,2048]{2,1,0:T(8,128)(2,1)S(1)}, u32[]{:S(2)}, u32[]{:S(2)}) %collective-permute-start) | collective-permute-done | bytes 294944 | tf_op jit(solution)/shard_map/ppermute | solution.py:54
  10.0 5.6 %collective-permute-start.1 = (bf16[3,48,2048]{2,1,0:T(8,128)(2,1)S(1)}, bf16[3,48,2048]{2,1,0:T(8,128)(2,1)S(1)}, u32[]{:S(2)}, u32[]{:S(2)}) collective-permute-start(bf16[3,48,2048]{2,1,0:T(8,128)(2,1)S(1)} %constant_dynamic-update-slice_fusion.a_ref), channel_id=1, source_target_pairs={{0,6},{1,3},{2,4},{3,1},{4,2},{5,7},{6,0},{7,5},{8,14},{9,11},{10,... | collective-permute-start | bytes 1769480 | tf_op jit(solution)/shard_map/ppermute | solution.py:41
  15.6 7.3 %collective-permute-done.1.b_ref = bf16[3,48,2048]{2,1,0:T(8,128)(2,1)S(1)} collective-permute-done((bf16[3,48,2048]{2,1,0:T(8,128)(2,1)S(1)}, bf16[3,48,2048]{2,1,0:T(8,128)(2,1)S(1)}, u32[]{:S(2)}, u32[]{:S(2)}) %collective-permute-start.1) | collective-permute-done | bytes 589856 | tf_op jit(solution)/shard_map/ppermute | solution.py:41
  23.0 4.9 %collective-permute-start.2 = (bf16[2,3,48,2048]{3,2,1,0:T(8,128)(2,1)S(1)}, bf16[2,3,48,2048]{3,2,1,0:T(8,128)(2,1)}, u32[]{:S(2)}, u32[]{:S(2)}) collective-permute-start(bf16[2,3,48,2048]{3,2,1,0:T(8,128)(2,1)S(1)} %shard_map.147.ta), channel_id=1, source_target_pairs={{0,2},{1,7},{2,0},{3,5},{4,6},{5,3},{6,4},{7,1},{8,10},{9,15},{10,... | collective-permute-start | bytes 3538952 | tf_op jit(solution)/shard_map/ppermute | solution.py:41
  27.9 16.7 %all_to_all.10.r_ref = bf16[8,136,128]{2,1,0:T(8,128)(2,1)S(1)} all-to-all(bf16[8,136,128]{2,1,0:T(8,128)(2,1)S(1)} %get-tuple-element.35), channel_id=1, replica_groups=mesh['z'=8,'yq'=4,'ys'=2,'x'=4,'c'=2] {'yq','ys'}, dimensions={0} | all-to-all | bytes 557056 | tf_op jit(solution)/shard_map/all_to_all | solution.py:58
  44.8 4.0 %collective-permute-start.4 = (bf16[528,256]{1,0:T(8,128)(2,1)S(1)}, bf16[528,256]{1,0:T(8,128)(2,1)S(1)}, u32[]{:S(2)}, u32[]{:S(2)}) collective-permute-start(bf16[528,256]{1,0:T(8,128)(2,1)S(1)} %shard_map.148.own), channel_id=1, source_target_pairs={{0,448},{1,65},{64,128},{65,1},{128,64},{129,193},{192,256},{193,1... | collective-permute-start | bytes 811016 | tf_op jit(solution)/shard_map/ppermute | solution.py:41
  48.8 9.8 %collective-permute-start.5 = (bf16[528,256]{1,0:T(8,128)(2,1)S(1)}, bf16[528,256]{1,0:T(8,128)(2,1)S(1)}, u32[]{:S(2)}, u32[]{:S(2)}) collective-permute-start(bf16[528,256]{1,0:T(8,128)(2,1)S(1)} %shard_map.148.own), channel_id=1, source_target_pairs={{0,128},{1,385},{64,448},{65,193},{128,256},{129,1},{192,64},{193,... | collective-permute-start | bytes 811016 | tf_op jit(solution)/shard_map/ppermute | solution.py:50
  58.6 4.2 %collective-permute-start.7 = (bf16[2,3,48,2048]{3,2,1,0:T(8,128)(2,1)S(1)}, bf16[2,3,48,2048]{3,2,1,0:T(8,128)(2,1)}, u32[]{:S(2)}, u32[]{:S(2)}) collective-permute-start(bf16[2,3,48,2048]{3,2,1,0:T(8,128)(2,1)S(1)} %shard_map.147.ta), channel_id=1, source_target_pairs={{0,1},{1,0},{2,3},{3,2},{4,5},{5,4},{6,7},{7,6},{8,9},{9,8},{10,11... | collective-permute-start | bytes 3538952 | tf_op jit(solution)/shard_map/ppermute | solution.py:54
  62.7 1.9 %collective-permute-start.8 = (bf16[2,3,48,2048]{3,2,1,0:T(8,128)(2,1)}, bf16[2,3,48,2048]{3,2,1,0:T(8,128)(2,1)}, u32[]{:S(2)}, u32[]{:S(2)}) collective-permute-start(bf16[2,3,48,2048]{3,2,1,0:T(8,128)(2,1)} %collective-permute-done.2.tb), channel_id=1, source_target_pairs={{0,1},{1,0},{2,3},{3,2},{4,5},{5,4},{6,7},{7,6},{8,9},{9,8},{10,11... | collective-permute-start | bytes 3538952 | tf_op jit(solution)/shard_map/ppermute | solution.py:54
  64.7 2.6 %collective-permute-done.5.b_ref = bf16[528,256]{1,0:T(8,128)(2,1)S(1)} collective-permute-done((bf16[528,256]{1,0:T(8,128)(2,1)S(1)}, bf16[528,256]{1,0:T(8,128)(2,1)S(1)}, u32[]{:S(2)}, u32[]{:S(2)}) %collective-permute-start.5) | collective-permute-done | bytes 270368 | tf_op jit(solution)/shard_map/ppermute | solution.py:50
  67.3 4.1 %collective-permute-start.6 = (bf16[2,528,256]{2,1,0:T(8,128)(2,1)S(1)}, bf16[2,528,256]{2,1,0:T(8,128)(2,1)S(1)}, u32[]{:S(2)}, u32[]{:S(2)}) collective-permute-start(bf16[2,528,256]{2,1,0:T(8,128)(2,1)S(1)} %shard_map.149.p1), channel_id=1, source_target_pairs={{0,64},{1,449},{64,0},{65,129},{128,192},{129,65},{192,128},{193,2... | collective-permute-start | bytes 1622024 | tf_op jit(solution)/shard_map/ppermute | solution.py:41
  71.4 7.2 %collective-permute-done.6.p2 = bf16[2,528,256]{2,1,0:T(8,128)(2,1)S(1)} collective-permute-done((bf16[2,528,256]{2,1,0:T(8,128)(2,1)S(1)}, bf16[2,528,256]{2,1,0:T(8,128)(2,1)S(1)}, u32[]{:S(2)}, u32[]{:S(2)}) %collective-permute-start.6) | collective-permute-done | bytes 540704 | tf_op jit(solution)/shard_map/ppermute | solution.py:41
  80.5 5.3 %collective-permute-start.3 = (bf16[528,256]{1,0:T(8,128)(2,1)S(1)}, bf16[528,256]{1,0:T(8,128)(2,1)S(1)}, u32[]{:S(2)}, u32[]{:S(2)}) collective-permute-start(bf16[528,256]{1,0:T(8,128)(2,1)S(1)} %shard_map.148.own), channel_id=1, source_target_pairs={{0,64},{1,449},{64,0},{65,129},{128,192},{129,65},{192,128},{193,2... | collective-permute-start | bytes 811016 | tf_op jit(solution)/shard_map/ppermute | solution.py:41
  85.8 6.6 %collective-permute-done.3.got = bf16[528,256]{1,0:T(8,128)(2,1)S(1)} collective-permute-done((bf16[528,256]{1,0:T(8,128)(2,1)S(1)}, bf16[528,256]{1,0:T(8,128)(2,1)S(1)}, u32[]{:S(2)}, u32[]{:S(2)}) %collective-permute-start.3) | collective-permute-done | bytes 270368 | tf_op jit(solution)/shard_map/ppermute | solution.py:41
  92.5 2.1 %shard_map.150 = (bf16[192,2048]{1,0:T(8,128)(2,1)S(1)}, bf16[192,2048]{1,0:T(8,128)(2,1)S(1)}, bf16[192,2048]{1,0:T(8,128)(2,1)S(1)}, f32[3,192,176]{2,1,0:T(8,128)S(1)}) custom-call(s32[8]{0:T(128)S(1)} %compare_select_fusion.b_ref, bf16[2,3,48,2048]{3,2,1,0:T(8,128)(2,1)S(1)} %shard_map.147.ta, bf16[2,3,48,2048]{3,2,1,0:T(8,128)(2,1)} %collective-permute-done.2.tb, ...), custom_call_target="tpu_custom_call" | custom-call | tf_op jit(solution)/shard_map/pallas_call | solution.py:27
  94.5 2.4 %shard_map.151 = (bf16[192,2048]{1,0:T(8,128)(2,1)S(1)}, bf16[192,2048]{1,0:T(8,128)(2,1)S(1)}, bf16[192,2048]{1,0:T(8,128)(2,1)S(1)}, f32[3,192,176]{2,1,0:T(8,128)S(1)}) custom-call(s32[8]{0:T(128)S(1)} %compare_select_fusion.b_ref, bf16[2,3,48,2048]{3,2,1,0:T(8,128)(2,1)} %collective-permute-done.7.ta, ...), custom_call_target="tpu_custom_call" | custom-call | tf_op jit(solution)/shard_map/pallas_call | solution.py:27
  98.1 3.2 %shard_map.153 = (f32[2,192,2048]{2,1,0:T(8,128)S(1)}, bf16[2,192,2048]{2,1,0:T(8,128)(2,1)S(1)}) custom-call(s32[8]{0:T(128)S(1)} %compare_select_fusion.b_ref, bf16[2,192,176]{2,1,0:T(8,128)(2,1)S(1)} %get-tuple-element.42.dg_ref, bf16[2,192,176]{2,1,0:T(8,128)(2,1)S(1)} %get-tuple-element.43.du_ref, bf16[192,2048]{1,0:T(8,128)(2,1)S(1)} %get-tuple-element.44.tl0, ...), custom_call_target="tpu_custom_call" | custom-call | tf_op jit(solution)/shard_map/pallas_call | solution.py:27
  101.4 2.9 %collective-permute-start.10 = (bf16[2,192,2048]{2,1,0:T(8,128)(2,1)S(1)}, bf16[2,192,2048]{2,1,0:T(8,128)(2,1)S(1)}, u32[]{:S(2)}, u32[]{:S(2)}) collective-permute-start(bf16[2,192,2048]{2,1,0:T(8,128)(2,1)S(1)} %get-tuple-element.47), channel_id=1, source_target_pairs={{0,1},{1,0},{2,3},{3,2},{4,5},{5,4},{6,7},{7,6},{8,9},{9,8},{10,11... | collective-permute-start | bytes 4718600 | tf_op jit(solution)/shard_map/ppermute | solution.py:54
  104.2 1.9 %collective-permute-start.15 = (bf16[2,528,256]{2,1,0:T(8,128)(2,1)S(1)}, bf16[2,528,256]{2,1,0:T(8,128)(2,1)S(1)}, u32[]{:S(2)}, u32[]{:S(2)}) collective-permute-start(bf16[2,528,256]{2,1,0:T(8,128)(2,1)S(1)} %get-tuple-element.57), channel_id=1, source_target_pairs={{0,448},{1,65},{64,128},{65,1},{128,64},{129,193},{192,256},{193,1... | collective-permute-start | bytes 1622024 | tf_op jit(solution)/shard_map/ppermute | solution.py:41
  107.6 1.9 %collective-permute-start.11 = (bf16[2,96,2048]{2,1,0:T(8,128)(2,1)S(1)}, bf16[2,96,2048]{2,1,0:T(8,128)(2,1)S(1)}, u32[]{:S(2)}, u32[]{:S(2)}) collective-permute-start(bf16[2,96,2048]{2,1,0:T(8,128)(2,1)S(1)} %get-tuple-element.49), channel_id=1, source_target_pairs={{0,2},{1,7},{2,0},{3,5},{4,6},{5,3},{6,4},{7,1},{8,10},{9,15},{10,... | collective-permute-start | bytes 2359304 | tf_op jit(solution)/shard_map/ppermute | solution.py:41
  110.0 4.7 %collective-permute-done.15.r_ref = bf16[2,528,256]{2,1,0:T(8,128)(2,1)S(1)} collective-permute-done((bf16[2,528,256]{2,1,0:T(8,128)(2,1)S(1)}, bf16[2,528,256]{2,1,0:T(8,128)(2,1)S(1)}, u32[]{:S(2)}, u32[]{:S(2)}) %collective-permute-start.15) | collective-permute-done | bytes 540704 | tf_op jit(solution)/shard_map/ppermute | solution.py:41
  114.7 4.0 %collective-permute-start.16 = (bf16[2,528,256]{2,1,0:T(8,128)(2,1)S(1)}, bf16[2,528,256]{2,1,0:T(8,128)(2,1)S(1)}, u32[]{:S(2)}, u32[]{:S(2)}) collective-permute-start(bf16[2,528,256]{2,1,0:T(8,128)(2,1)S(1)} %shard_map.162), channel_id=1, source_target_pairs={{0,64},{1,449},{64,0},{65,129},{128,192},{129,65},{192,128},{193,2... | collective-permute-start | bytes 1622024 | tf_op jit(solution)/shard_map/ppermute | solution.py:41
  119.5 2.5 %collective-permute-start.14 = (bf16[1,528,256]{2,1,0:T(8,128)(2,1)S(1)}, bf16[1,528,256]{2,1,0:T(8,128)(2,1)S(1)}, u32[]{:S(2)}, u32[]{:S(2)}) collective-permute-start(bf16[1,528,256]{2,1,0:T(8,128)(2,1)S(1)} %shard_map.158), channel_id=1, source_target_pairs={{0,64},{1,449},{64,0},{65,129},{128,192},{129,65},{192,128},{193,2... | collective-permute-start | bytes 811016 | tf_op jit(solution)/shard_map/ppermute | solution.py:41
  122.0 4.1 %collective-permute-done.16.r_ref = bf16[2,528,256]{2,1,0:T(8,128)(2,1)S(1)} collective-permute-done((bf16[2,528,256]{2,1,0:T(8,128)(2,1)S(1)}, bf16[2,528,256]{2,1,0:T(8,128)(2,1)S(1)}, u32[]{:S(2)}, u32[]{:S(2)}) %collective-permute-start.16) | collective-permute-done | bytes 540704 | tf_op jit(solution)/shard_map/ppermute | solution.py:41
  126.1 1.9 %collective-permute-start.17 = (bf16[1,528,256]{2,1,0:T(8,128)(2,1)S(1)}, bf16[1,528,256]{2,1,0:T(8,128)(2,1)S(1)}, u32[]{:S(2)}, u32[]{:S(2)}) collective-permute-start(bf16[1,528,256]{2,1,0:T(8,128)(2,1)S(1)} %get-tuple-element.58), channel_id=1, source_target_pairs={{0,384},{1,129},{64,192},{65,449},{128,0},{129,257},{192,320},{193... | collective-permute-start | bytes 811016 | tf_op jit(solution)/shard_map/ppermute | solution.py:50
  128.0 5.2 %collective-permute-start.18 = (bf16[1,528,256]{2,1,0:T(8,128)(2,1)S(1)}, bf16[1,528,256]{2,1,0:T(8,128)(2,1)S(1)}, u32[]{:S(2)}, u32[]{:S(2)}) collective-permute-start(bf16[1,528,256]{2,1,0:T(8,128)(2,1)S(1)} %get-tuple-element.59), channel_id=1, source_target_pairs={{0,448},{1,65},{64,128},{65,1},{128,64},{129,193},{192,256},{193,1... | collective-permute-start | bytes 811016 | tf_op jit(solution)/shard_map/ppermute | solution.py:41
  133.4 1.9 %collective-permute-start.12 = (bf16[2,48,2048]{2,1,0:T(8,128)(2,1)S(1)}, bf16[2,48,2048]{2,1,0:T(8,128)(2,1)S(1)}, u32[]{:S(2)}, u32[]{:S(2)}) collective-permute-start(bf16[2,48,2048]{2,1,0:T(8,128)(2,1)S(1)} %get-tuple-element.51), channel_id=1, source_target_pairs={{0,8},{8,0},{1,9},{9,1},{2,10},{10,2},{3,11},{11,3},{4,12},{12,4},... | collective-permute-start | bytes 1179656 | tf_op jit(solution)/shard_map/ppermute | solution.py:54
  136.1 5.2 %collective-permute-done.18.r_ref = bf16[1,528,256]{2,1,0:T(8,128)(2,1)S(1)} collective-permute-done((bf16[1,528,256]{2,1,0:T(8,128)(2,1)S(1)}, bf16[1,528,256]{2,1,0:T(8,128)(2,1)S(1)}, u32[]{:S(2)}, u32[]{:S(2)}) %collective-permute-start.18) | collective-permute-done | bytes 270368 | tf_op jit(solution)/shard_map/ppermute | solution.py:41
  142.2 3.5 %all-to-all-start.1 = ((bf16[8,136,128]{2,1,0:T(8,128)(2,1)}), bf16[8,136,128]{2,1,0:T(8,128)(2,1)S(1)}, u32[]{:S(2)}, u32[]{:S(2)}) async-start(bf16[8,136,128]{2,1,0:T(8,128)(2,1)} %shard_map.165), calls=%async_computation.1 | async-start | bytes 557056 | tf_op jit(solution)/shard_map/all_to_all | solution.py:58
  145.9 1.9 %collective-permute-start.13 = (bf16[2,24,2048]{2,1,0:T(8,128)(2,1)S(1)}, bf16[2,24,2048]{2,1,0:T(8,128)(2,1)S(1)}, u32[]{:S(2)}, u32[]{:S(2)}) collective-permute-start(bf16[2,24,2048]{2,1,0:T(8,128)(2,1)S(1)} %get-tuple-element.53), channel_id=1, source_target_pairs={{0,6},{1,3},{2,4},{3,1},{4,2},{5,7},{6,0},{7,5},{8,14},{9,11},{10,... | collective-permute-start | bytes 589832 | tf_op jit(solution)/shard_map/ppermute | solution.py:41
  147.8 9.3 %all-to-all-done.1.r_ref = bf16[8,136,128]{2,1,0:T(8,128)(2,1)S(1)} async-done(((bf16[8,136,128]{2,1,0:T(8,128)(2,1)}), bf16[8,136,128]{2,1,0:T(8,128)(2,1)S(1)}, u32[]{:S(2)}, u32[]{:S(2)}) %all-to-all-start.1) | async-done | bytes 278560 | tf_op jit(solution)/shard_map/all_to_all | solution.py:58
  (50 shorter events, 11.0 us)
Async XLA Ops:
  1.9 8.1 %collective-permute-start = (bf16[3,24,2048]{2,1,0:T(8,128)(2,1)S(1)}, bf16[3,24,2048]{2,1,0:T(8,128)(2,1)S(1)}, u32[]{:S(2)}, u32[]{:S(2)}) collective-permute-start(bf16[3,24,2048]{2,1,0:T(8,128)(2,1)S(1)} %get-tuple-element.34), channel_id=1, source_target_pairs={{0,8},{8,0},{1,9},{9,1},{2,10},{10,2},{3,11},{11,3},{4,12},{12,4},... | collective-permute-start | bytes 884744 | tf_op jit(solution)/shard_map/ppermute | solution.py:54
  10.0 12.9 %collective-permute-start.1 = (bf16[3,48,2048]{2,1,0:T(8,128)(2,1)S(1)}, bf16[3,48,2048]{2,1,0:T(8,128)(2,1)S(1)}, u32[]{:S(2)}, u32[]{:S(2)}) collective-permute-start(bf16[3,48,2048]{2,1,0:T(8,128)(2,1)S(1)} %constant_dynamic-update-slice_fusion.a_ref), channel_id=1, source_target_pairs={{0,6},{1,3},{2,4},{3,1},{4,2},{5,7},{6,0},{7,5},{8,14},{9,11},{10,... | collective-permute-start | bytes 1769480 | tf_op jit(solution)/shard_map/ppermute | solution.py:41
  23.0 62.8 %copy-start.7 = (s32[8]{0:T(128)S(1)}, s32[8]{0:T(128)}, u32[]{:S(2)}) copy-start(s32[8]{0:T(128)} %constant.24.clone) | copy-start | bytes 100
  23.0 39.7 %collective-permute-start.2 = (bf16[2,3,48,2048]{3,2,1,0:T(8,128)(2,1)S(1)}, bf16[2,3,48,2048]{3,2,1,0:T(8,128)(2,1)}, u32[]{:S(2)}, u32[]{:S(2)}) collective-permute-start(bf16[2,3,48,2048]{3,2,1,0:T(8,128)(2,1)S(1)} %shard_map.147.ta), channel_id=1, source_target_pairs={{0,2},{1,7},{2,0},{3,5},{4,6},{5,3},{6,4},{7,1},{8,10},{9,15},{10,... | collective-permute-start | bytes 3538952 | tf_op jit(solution)/shard_map/ppermute | solution.py:41
  44.8 19.9 %collective-permute-start.4 = (bf16[528,256]{1,0:T(8,128)(2,1)S(1)}, bf16[528,256]{1,0:T(8,128)(2,1)S(1)}, u32[]{:S(2)}, u32[]{:S(2)}) collective-permute-start(bf16[528,256]{1,0:T(8,128)(2,1)S(1)} %shard_map.148.own), channel_id=1, source_target_pairs={{0,448},{1,65},{64,128},{65,1},{128,64},{129,193},{192,256},{193,1... | collective-permute-start | bytes 811016 | tf_op jit(solution)/shard_map/ppermute | solution.py:41
  48.8 18.4 %collective-permute-start.5 = (bf16[528,256]{1,0:T(8,128)(2,1)S(1)}, bf16[528,256]{1,0:T(8,128)(2,1)S(1)}, u32[]{:S(2)}, u32[]{:S(2)}) collective-permute-start(bf16[528,256]{1,0:T(8,128)(2,1)S(1)} %shard_map.148.own), channel_id=1, source_target_pairs={{0,128},{1,385},{64,448},{65,193},{128,256},{129,1},{192,64},{193,... | collective-permute-start | bytes 811016 | tf_op jit(solution)/shard_map/ppermute | solution.py:50
  58.6 36.0 %collective-permute-start.7 = (bf16[2,3,48,2048]{3,2,1,0:T(8,128)(2,1)S(1)}, bf16[2,3,48,2048]{3,2,1,0:T(8,128)(2,1)}, u32[]{:S(2)}, u32[]{:S(2)}) collective-permute-start(bf16[2,3,48,2048]{3,2,1,0:T(8,128)(2,1)S(1)} %shard_map.147.ta), channel_id=1, source_target_pairs={{0,1},{1,0},{2,3},{3,2},{4,5},{5,4},{6,7},{7,6},{8,9},{9,8},{10,11... | collective-permute-start | bytes 3538952 | tf_op jit(solution)/shard_map/ppermute | solution.py:54
  62.7 31.8 %collective-permute-start.8 = (bf16[2,3,48,2048]{3,2,1,0:T(8,128)(2,1)}, bf16[2,3,48,2048]{3,2,1,0:T(8,128)(2,1)}, u32[]{:S(2)}, u32[]{:S(2)}) collective-permute-start(bf16[2,3,48,2048]{3,2,1,0:T(8,128)(2,1)} %collective-permute-done.2.tb), channel_id=1, source_target_pairs={{0,1},{1,0},{2,3},{3,2},{4,5},{5,4},{6,7},{7,6},{8,9},{9,8},{10,11... | collective-permute-start | bytes 3538952 | tf_op jit(solution)/shard_map/ppermute | solution.py:54
  67.3 11.3 %collective-permute-start.6 = (bf16[2,528,256]{2,1,0:T(8,128)(2,1)S(1)}, bf16[2,528,256]{2,1,0:T(8,128)(2,1)S(1)}, u32[]{:S(2)}, u32[]{:S(2)}) collective-permute-start(bf16[2,528,256]{2,1,0:T(8,128)(2,1)S(1)} %shard_map.149.p1), channel_id=1, source_target_pairs={{0,64},{1,449},{64,0},{65,129},{128,192},{129,65},{192,128},{193,2... | collective-permute-start | bytes 1622024 | tf_op jit(solution)/shard_map/ppermute | solution.py:41
  78.6 18.4 %collective-permute-start.9 = (bf16[2,528,256]{2,1,0:T(8,128)(2,1)S(1)}, bf16[2,528,256]{2,1,0:T(8,128)(2,1)S(1)}, u32[]{:S(2)}, u32[]{:S(2)}) collective-permute-start(bf16[2,528,256]{2,1,0:T(8,128)(2,1)S(1)} %collective-permute-done.6.p2), channel_id=1, source_target_pairs={{0,448},{1,65},{64,128},{65,1},{128,64},{129,193},{192,256},{193,1... | collective-permute-start | bytes 1622024 | tf_op jit(solution)/shard_map/ppermute | solution.py:41
  80.5 11.9 %collective-permute-start.3 = (bf16[528,256]{1,0:T(8,128)(2,1)S(1)}, bf16[528,256]{1,0:T(8,128)(2,1)S(1)}, u32[]{:S(2)}, u32[]{:S(2)}) collective-permute-start(bf16[528,256]{1,0:T(8,128)(2,1)S(1)} %shard_map.148.own), channel_id=1, source_target_pairs={{0,64},{1,449},{64,0},{65,129},{128,192},{129,65},{192,128},{193,2... | collective-permute-start | bytes 811016 | tf_op jit(solution)/shard_map/ppermute | solution.py:41
  101.4 5.9 %collective-permute-start.10 = (bf16[2,192,2048]{2,1,0:T(8,128)(2,1)S(1)}, bf16[2,192,2048]{2,1,0:T(8,128)(2,1)S(1)}, u32[]{:S(2)}, u32[]{:S(2)}) collective-permute-start(bf16[2,192,2048]{2,1,0:T(8,128)(2,1)S(1)} %get-tuple-element.47), channel_id=1, source_target_pairs={{0,1},{1,0},{2,3},{3,2},{4,5},{5,4},{6,7},{7,6},{8,9},{9,8},{10,11... | collective-permute-start | bytes 4718600 | tf_op jit(solution)/shard_map/ppermute | solution.py:54
  104.2 10.4 %collective-permute-start.15 = (bf16[2,528,256]{2,1,0:T(8,128)(2,1)S(1)}, bf16[2,528,256]{2,1,0:T(8,128)(2,1)S(1)}, u32[]{:S(2)}, u32[]{:S(2)}) collective-permute-start(bf16[2,528,256]{2,1,0:T(8,128)(2,1)S(1)} %get-tuple-element.57), channel_id=1, source_target_pairs={{0,448},{1,65},{64,128},{65,1},{128,64},{129,193},{192,256},{193,1... | collective-permute-start | bytes 1622024 | tf_op jit(solution)/shard_map/ppermute | solution.py:41
  107.6 25.7 %collective-permute-start.11 = (bf16[2,96,2048]{2,1,0:T(8,128)(2,1)S(1)}, bf16[2,96,2048]{2,1,0:T(8,128)(2,1)S(1)}, u32[]{:S(2)}, u32[]{:S(2)}) collective-permute-start(bf16[2,96,2048]{2,1,0:T(8,128)(2,1)S(1)} %get-tuple-element.49), channel_id=1, source_target_pairs={{0,2},{1,7},{2,0},{3,5},{4,6},{5,3},{6,4},{7,1},{8,10},{9,15},{10,... | collective-permute-start | bytes 2359304 | tf_op jit(solution)/shard_map/ppermute | solution.py:41
  114.7 11.3 %collective-permute-start.16 = (bf16[2,528,256]{2,1,0:T(8,128)(2,1)S(1)}, bf16[2,528,256]{2,1,0:T(8,128)(2,1)S(1)}, u32[]{:S(2)}, u32[]{:S(2)}) collective-permute-start(bf16[2,528,256]{2,1,0:T(8,128)(2,1)S(1)} %shard_map.162), channel_id=1, source_target_pairs={{0,64},{1,449},{64,0},{65,129},{128,192},{129,65},{192,128},{193,2... | collective-permute-start | bytes 1622024 | tf_op jit(solution)/shard_map/ppermute | solution.py:41
  119.5 15.8 %collective-permute-start.14 = (bf16[1,528,256]{2,1,0:T(8,128)(2,1)S(1)}, bf16[1,528,256]{2,1,0:T(8,128)(2,1)S(1)}, u32[]{:S(2)}, u32[]{:S(2)}) collective-permute-start(bf16[1,528,256]{2,1,0:T(8,128)(2,1)S(1)} %shard_map.158), channel_id=1, source_target_pairs={{0,64},{1,449},{64,0},{65,129},{128,192},{129,65},{192,128},{193,2... | collective-permute-start | bytes 811016 | tf_op jit(solution)/shard_map/ppermute | solution.py:41
  126.1 9.7 %collective-permute-start.17 = (bf16[1,528,256]{2,1,0:T(8,128)(2,1)S(1)}, bf16[1,528,256]{2,1,0:T(8,128)(2,1)S(1)}, u32[]{:S(2)}, u32[]{:S(2)}) collective-permute-start(bf16[1,528,256]{2,1,0:T(8,128)(2,1)S(1)} %get-tuple-element.58), channel_id=1, source_target_pairs={{0,384},{1,129},{64,192},{65,449},{128,0},{129,257},{192,320},{193... | collective-permute-start | bytes 811016 | tf_op jit(solution)/shard_map/ppermute | solution.py:50
  128.0 13.2 %collective-permute-start.18 = (bf16[1,528,256]{2,1,0:T(8,128)(2,1)S(1)}, bf16[1,528,256]{2,1,0:T(8,128)(2,1)S(1)}, u32[]{:S(2)}, u32[]{:S(2)}) collective-permute-start(bf16[1,528,256]{2,1,0:T(8,128)(2,1)S(1)} %get-tuple-element.59), channel_id=1, source_target_pairs={{0,448},{1,65},{64,128},{65,1},{128,64},{129,193},{192,256},{193,1... | collective-permute-start | bytes 811016 | tf_op jit(solution)/shard_map/ppermute | solution.py:41
  133.4 12.4 %collective-permute-start.12 = (bf16[2,48,2048]{2,1,0:T(8,128)(2,1)S(1)}, bf16[2,48,2048]{2,1,0:T(8,128)(2,1)S(1)}, u32[]{:S(2)}, u32[]{:S(2)}) collective-permute-start(bf16[2,48,2048]{2,1,0:T(8,128)(2,1)S(1)} %get-tuple-element.51), channel_id=1, source_target_pairs={{0,8},{8,0},{1,9},{9,1},{2,10},{10,2},{3,11},{11,3},{4,12},{12,4},... | collective-permute-start | bytes 1179656 | tf_op jit(solution)/shard_map/ppermute | solution.py:54
  136.1 11.7 %copy-start.6 = (bf16[2048]{0:T(1024)(128)(2,1)S(1)}, bf16[2048]{0:T(1024)(128)(2,1)}, u32[]{:S(2)}) copy-start(bf16[2048]{0:T(1024)(128)(2,1)} %refs_6_.1) | copy-start | bytes 12292
  136.1 21.1 %copy-start.3 = (f32[32,352]{1,0:T(8,128)S(1)}, f32[32,352]{1,0:T(8,128)}, u32[]{:S(2)}) copy-start(f32[32,352]{1,0:T(8,128)} %gs.1) | copy-start | bytes 135172
  136.1 21.1 %copy-start.4 = (f32[32,352]{1,0:T(8,128)S(1)}, f32[32,352]{1,0:T(8,128)}, u32[]{:S(2)}) copy-start(f32[32,352]{1,0:T(8,128)} %us.1) | copy-start | bytes 135172
  136.1 21.1 %copy-start.5 = (f32[32,352]{1,0:T(8,128)S(1)}, f32[32,352]{1,0:T(8,128)}, u32[]{:S(2)}) copy-start(f32[32,352]{1,0:T(8,128)} %ds.1) | copy-start | bytes 135172
  142.2 15.7 %copy-start = (bf16[24,2048]{1,0:T(8,128)(2,1)S(1)}, bf16[24,2048]{1,0:T(8,128)(2,1)}, u32[]{:S(2)}) copy-start(bf16[24,2048]{1,0:T(8,128)(2,1)} %e_ref.1) | copy-start | bytes 294916
  142.2 15.7 %copy-start.1 = (bf16[24,2048]{1,0:T(8,128)(2,1)S(1)}, bf16[24,2048]{1,0:T(8,128)(2,1)}, u32[]{:S(2)}) copy-start(bf16[24,2048]{1,0:T(8,128)(2,1)} %c_ref.1) | copy-start | bytes 294916
  142.2 15.7 %copy-start.2 = (bf16[24,2048]{1,0:T(8,128)(2,1)S(1)}, bf16[24,2048]{1,0:T(8,128)(2,1)}, u32[]{:S(2)}) copy-start(bf16[24,2048]{1,0:T(8,128)(2,1)} %l_ref.1) | copy-start | bytes 294916
  142.2 14.9 %all-to-all-start.1 = ((bf16[8,136,128]{2,1,0:T(8,128)(2,1)}), bf16[8,136,128]{2,1,0:T(8,128)(2,1)S(1)}, u32[]{:S(2)}, u32[]{:S(2)}) async-start(bf16[8,136,128]{2,1,0:T(8,128)(2,1)} %shard_map.165), calls=%async_computation.1 | async-start | bytes 557056 | tf_op jit(solution)/shard_map/all_to_all | solution.py:58
  145.9 12.1 %collective-permute-start.13 = (bf16[2,24,2048]{2,1,0:T(8,128)(2,1)S(1)}, bf16[2,24,2048]{2,1,0:T(8,128)(2,1)S(1)}, u32[]{:S(2)}, u32[]{:S(2)}) collective-permute-start(bf16[2,24,2048]{2,1,0:T(8,128)(2,1)S(1)} %get-tuple-element.53), channel_id=1, source_target_pairs={{0,6},{1,3},{2,4},{3,1},{4,2},{5,7},{6,0},{7,5},{8,14},{9,11},{10,... | collective-permute-start | bytes 589832 | tf_op jit(solution)/shard_map/ppermute | solution.py:41

commit v5 on v4

--- a/solution.py
+++ b/solution.py
@@ -125,14 +125,14 @@
 
 def turn_block(r_ref, o_ref):
     tiles = [r_ref[:, 32 * i : 32 * (i + 1)].reshape(NY * ROWS, 128).T for i in range(4)]
-    rest = unfold_rows(r_ref[:, 128:136].astype(f32), 1).reshape(NY * ROWS, 128).T
+    rest = unfold_rows(r_ref[:, 128:136].astype(f32), 1).astype(bf16).reshape(NY * ROWS, 128).T
     for i in range(3):
         o_ref[HALF * i : HALF * i + MAIN] = tiles[i]
     tail = tiles[3]
     o_ref[128:176] = tail[0:48]
     o_ref[304:352] = tail[48:96]
     o_ref[480:512] = tail[96:128]
-    o_ref[512:528] = rest[0:16].astype(bf16)
+    o_ref[512:528] = rest[0:16]
 
 
 def join(a_ref, b_ref, o_ref):
@@ -143,8 +143,10 @@
 def turned(f):
     parts = [f[HALF * i : HALF * i + MAIN] for i in range(3)]
     parts.append(jnp.concatenate([f[128:176], f[304:352], f[480:512]], axis=0))
-    parts.append(jnp.concatenate([f[512:528], jnp.zeros((112, 256), f.dtype)], axis=0))
+    few = f[512:528].T.astype(f32)
     parts = [p.T.reshape(NY, ROWS, 128).astype(f32) for p in parts]
+    few = jnp.concatenate([few, jnp.zeros((256, 112), f32)], axis=1)
+    parts.append(few.reshape(NY, ROWS, 128))
     return jnp.concatenate([*parts[:4], fold_rows(parts[4], 0, 1)], axis=1)
 
 

time: 160 us -> 160 us (level)
  no operation moved by 1% of the time
where the time goes in v5:
time: 160 us; the launch traced here: 159 us
  starting transfers between devices  73.3 us (46%)
  waiting for transfers between devices  52.1 us (33%)
  blocking collectives  16.7 us (10%)
  Pallas kernels  15.5 us (10%)
    ppermute x12, starting transfers between devices, exchange(): return lax.ppermute(x, (axis, 'c'), pairs)  43.2 us
    ppermute x12, waiting for transfers between devices, exchange(): return lax.ppermute(x, (axis, 'c'), pairs)  35 us
    all_to_all x1, blocking collectives, over_y(): lax.all_to_all(x, ('yq', 'ys'), split_axis=0, concat_axis=0, tiled=True)  16.7 us
    pallas_call x21, Pallas kernels, call(): pl.pallas_call(body, out_shape=out_shape, compiler_params=pltpu.CompilerP...  15.5 us
    ppermute x5, starting transfers between devices, swapped(): return lax.ppermute(x, axis, [(0, 1), (1, 0)])  14.9 us
    ppermute x2, starting transfers between devices, hop_two(): return lax.ppermute(x, ('z', 'c'), pairs)  11.7 us
    all_to_all x1, waiting for transfers between devices, over_y(): lax.all_to_all(x, ('yq', 'ys'), split_axis=0, concat_axis=0, tiled=True)  9.33 us
    ppermute x5, waiting for transfers between devices, swapped(): return lax.ppermute(x, axis, [(0, 1), (1, 0)])  5.16 us
  transfers between devices with their start and end apart: 20, of which 10 were waited for; matrix products, arithmetic and copies ran while one was open for 0% of the time, Pallas kernels for 6%

profile of v5, /device:TPU:1, one launch (start us, length us, event | category | flops | bytes accessed | tf_op | source)
XLA Modules:
  0.0 158.7 jit_solution(16385150222238604014)
XLA Ops:
  1.9 4.0 %collective-permute-start = (bf16[3,24,2048]{2,1,0:T(8,128)(2,1)S(1)}, bf16[3,24,2048]{2,1,0:T(8,128)(2,1)S(1)}, u32[]{:S(2)}, u32[]{:S(2)}) collective-permute-start(bf16[3,24,2048]{2,1,0:T(8,128)(2,1)S(1)} %get-tuple-element.34), channel_id=1, source_target_pairs={{0,8},{8,0},{1,9},{9,1},{2,10},{10,2},{3,11},{11,3},{4,12},{12,4},... | collective-permute-start | bytes 884744 | tf_op jit(solution)/shard_map/ppermute | solution.py:54
  5.9 4.1 %collective-permute-done = bf16[3,24,2048]{2,1,0:T(8,128)(2,1)S(1)} collective-permute-done((bf16[3,24,2048]{2,1,0:T(8,128)(2,1)S(1)}, bf16[3,24,2048]{2,1,0:T(8,128)(2,1)S(1)}, u32[]{:S(2)}, u32[]{:S(2)}) %collective-permute-start) | collective-permute-done | bytes 294944 | tf_op jit(solution)/shard_map/ppermute | solution.py:54
  10.0 5.6 %collective-permute-start.1 = (bf16[3,48,2048]{2,1,0:T(8,128)(2,1)S(1)}, bf16[3,48,2048]{2,1,0:T(8,128)(2,1)S(1)}, u32[]{:S(2)}, u32[]{:S(2)}) collective-permute-start(bf16[3,48,2048]{2,1,0:T(8,128)(2,1)S(1)} %constant_dynamic-update-slice_fusion.a_ref), channel_id=1, source_target_pairs={{0,6},{1,3},{2,4},{3,1},{4,2},{5,7},{6,0},{7,5},{8,14},{9,11},{10,... | collective-permute-start | bytes 1769480 | tf_op jit(solution)/shard_map/ppermute | solution.py:41
  15.6 7.3 %collective-permute-done.1.b_ref = bf16[3,48,2048]{2,1,0:T(8,128)(2,1)S(1)} collective-permute-done((bf16[3,48,2048]{2,1,0:T(8,128)(2,1)S(1)}, bf16[3,48,2048]{2,1,0:T(8,128)(2,1)S(1)}, u32[]{:S(2)}, u32[]{:S(2)}) %collective-permute-start.1) | collective-permute-done | bytes 589856 | tf_op jit(solution)/shard_map/ppermute | solution.py:41
  23.0 4.9 %collective-permute-start.2 = (bf16[2,3,48,2048]{3,2,1,0:T(8,128)(2,1)S(1)}, bf16[2,3,48,2048]{3,2,1,0:T(8,128)(2,1)}, u32[]{:S(2)}, u32[]{:S(2)}) collective-permute-start(bf16[2,3,48,2048]{3,2,1,0:T(8,128)(2,1)S(1)} %shard_map.147.ta), channel_id=1, source_target_pairs={{0,2},{1,7},{2,0},{3,5},{4,6},{5,3},{6,4},{7,1},{8,10},{9,15},{10,... | collective-permute-start | bytes 3538952 | tf_op jit(solution)/shard_map/ppermute | solution.py:41
  27.9 16.7 %all_to_all.10.r_ref = bf16[8,136,128]{2,1,0:T(8,128)(2,1)S(1)} all-to-all(bf16[8,136,128]{2,1,0:T(8,128)(2,1)S(1)} %get-tuple-element.35), channel_id=1, replica_groups=mesh['z'=8,'yq'=4,'ys'=2,'x'=4,'c'=2] {'yq','ys'}, dimensions={0} | all-to-all | bytes 557056 | tf_op jit(solution)/shard_map/all_to_all | solution.py:58
  44.8 4.0 %collective-permute-start.4 = (bf16[528,256]{1,0:T(8,128)(2,1)S(1)}, bf16[528,256]{1,0:T(8,128)(2,1)S(1)}, u32[]{:S(2)}, u32[]{:S(2)}) collective-permute-start(bf16[528,256]{1,0:T(8,128)(2,1)S(1)} %shard_map.148.own), channel_id=1, source_target_pairs={{0,448},{1,65},{64,128},{65,1},{128,64},{129,193},{192,256},{193,1... | collective-permute-start | bytes 811016 | tf_op jit(solution)/shard_map/ppermute | solution.py:41
  48.8 9.8 %collective-permute-start.5 = (bf16[528,256]{1,0:T(8,128)(2,1)S(1)}, bf16[528,256]{1,0:T(8,128)(2,1)S(1)}, u32[]{:S(2)}, u32[]{:S(2)}) collective-permute-start(bf16[528,256]{1,0:T(8,128)(2,1)S(1)} %shard_map.148.own), channel_id=1, source_target_pairs={{0,128},{1,385},{64,448},{65,193},{128,256},{129,1},{192,64},{193,... | collective-permute-start | bytes 811016 | tf_op jit(solution)/shard_map/ppermute | solution.py:50
  58.5 4.2 %collective-permute-start.7 = (bf16[2,3,48,2048]{3,2,1,0:T(8,128)(2,1)S(1)}, bf16[2,3,48,2048]{3,2,1,0:T(8,128)(2,1)}, u32[]{:S(2)}, u32[]{:S(2)}) collective-permute-start(bf16[2,3,48,2048]{3,2,1,0:T(8,128)(2,1)S(1)} %shard_map.147.ta), channel_id=1, source_target_pairs={{0,1},{1,0},{2,3},{3,2},{4,5},{5,4},{6,7},{7,6},{8,9},{9,8},{10,11... | collective-permute-start | bytes 3538952 | tf_op jit(solution)/shard_map/ppermute | solution.py:54
  62.7 1.9 %collective-permute-start.8 = (bf16[2,3,48,2048]{3,2,1,0:T(8,128)(2,1)}, bf16[2,3,48,2048]{3,2,1,0:T(8,128)(2,1)}, u32[]{:S(2)}, u32[]{:S(2)}) collective-permute-start(bf16[2,3,48,2048]{3,2,1,0:T(8,128)(2,1)} %collective-permute-done.2.tb), channel_id=1, source_target_pairs={{0,1},{1,0},{2,3},{3,2},{4,5},{5,4},{6,7},{7,6},{8,9},{9,8},{10,11... | collective-permute-start | bytes 3538952 | tf_op jit(solution)/shard_map/ppermute | solution.py:54
  64.7 2.6 %collective-permute-done.5.b_ref = bf16[528,256]{1,0:T(8,128)(2,1)S(1)} collective-permute-done((bf16[528,256]{1,0:T(8,128)(2,1)S(1)}, bf16[528,256]{1,0:T(8,128)(2,1)S(1)}, u32[]{:S(2)}, u32[]{:S(2)}) %collective-permute-start.5) | collective-permute-done | bytes 270368 | tf_op jit(solution)/shard_map/ppermute | solution.py:50
  67.3 4.1 %collective-permute-start.6 = (bf16[2,528,256]{2,1,0:T(8,128)(2,1)S(1)}, bf16[2,528,256]{2,1,0:T(8,128)(2,1)S(1)}, u32[]{:S(2)}, u32[]{:S(2)}) collective-permute-start(bf16[2,528,256]{2,1,0:T(8,128)(2,1)S(1)} %shard_map.149.p1), channel_id=1, source_target_pairs={{0,64},{1,449},{64,0},{65,129},{128,192},{129,65},{192,128},{193,2... | collective-permute-start | bytes 1622024 | tf_op jit(solution)/shard_map/ppermute | solution.py:41
  71.4 7.2 %collective-permute-done.6.p2 = bf16[2,528,256]{2,1,0:T(8,128)(2,1)S(1)} collective-permute-done((bf16[2,528,256]{2,1,0:T(8,128)(2,1)S(1)}, bf16[2,528,256]{2,1,0:T(8,128)(2,1)S(1)}, u32[]{:S(2)}, u32[]{:S(2)}) %collective-permute-start.6) | collective-permute-done | bytes 540704 | tf_op jit(solution)/shard_map/ppermute | solution.py:41
  80.5 5.3 %collective-permute-start.3 = (bf16[528,256]{1,0:T(8,128)(2,1)S(1)}, bf16[528,256]{1,0:T(8,128)(2,1)S(1)}, u32[]{:S(2)}, u32[]{:S(2)}) collective-permute-start(bf16[528,256]{1,0:T(8,128)(2,1)S(1)} %shard_map.148.own), channel_id=1, source_target_pairs={{0,64},{1,449},{64,0},{65,129},{128,192},{129,65},{192,128},{193,2... | collective-permute-start | bytes 811016 | tf_op jit(solution)/shard_map/ppermute | solution.py:41
  85.8 6.6 %collective-permute-done.3.got = bf16[528,256]{1,0:T(8,128)(2,1)S(1)} collective-permute-done((bf16[528,256]{1,0:T(8,128)(2,1)S(1)}, bf16[528,256]{1,0:T(8,128)(2,1)S(1)}, u32[]{:S(2)}, u32[]{:S(2)}) %collective-permute-start.3) | collective-permute-done | bytes 270368 | tf_op jit(solution)/shard_map/ppermute | solution.py:41
  92.4 2.1 %shard_map.150 = (bf16[192,2048]{1,0:T(8,128)(2,1)S(1)}, bf16[192,2048]{1,0:T(8,128)(2,1)S(1)}, bf16[192,2048]{1,0:T(8,128)(2,1)S(1)}, f32[3,192,176]{2,1,0:T(8,128)S(1)}) custom-call(s32[8]{0:T(128)S(1)} %compare_select_fusion.b_ref, bf16[2,3,48,2048]{3,2,1,0:T(8,128)(2,1)S(1)} %shard_map.147.ta, bf16[2,3,48,2048]{3,2,1,0:T(8,128)(2,1)} %collective-permute-done.2.tb, ...), custom_call_target="tpu_custom_call" | custom-call | tf_op jit(solution)/shard_map/pallas_call | solution.py:27
  94.5 2.4 %shard_map.151 = (bf16[192,2048]{1,0:T(8,128)(2,1)S(1)}, bf16[192,2048]{1,0:T(8,128)(2,1)S(1)}, bf16[192,2048]{1,0:T(8,128)(2,1)S(1)}, f32[3,192,176]{2,1,0:T(8,128)S(1)}) custom-call(s32[8]{0:T(128)S(1)} %compare_select_fusion.b_ref, bf16[2,3,48,2048]{3,2,1,0:T(8,128)(2,1)} %collective-permute-done.7.ta, ...), custom_call_target="tpu_custom_call" | custom-call | tf_op jit(solution)/shard_map/pallas_call | solution.py:27
  98.1 3.2 %shard_map.153 = (f32[2,192,2048]{2,1,0:T(8,128)S(1)}, bf16[2,192,2048]{2,1,0:T(8,128)(2,1)S(1)}) custom-call(s32[8]{0:T(128)S(1)} %compare_select_fusion.b_ref, bf16[2,192,176]{2,1,0:T(8,128)(2,1)S(1)} %get-tuple-element.42.dg_ref, bf16[2,192,176]{2,1,0:T(8,128)(2,1)S(1)} %get-tuple-element.43.du_ref, bf16[192,2048]{1,0:T(8,128)(2,1)S(1)} %get-tuple-element.44.tl0, ...), custom_call_target="tpu_custom_call" | custom-call | tf_op jit(solution)/shard_map/pallas_call | solution.py:27
  101.3 2.9 %collective-permute-start.10 = (bf16[2,192,2048]{2,1,0:T(8,128)(2,1)S(1)}, bf16[2,192,2048]{2,1,0:T(8,128)(2,1)S(1)}, u32[]{:S(2)}, u32[]{:S(2)}) collective-permute-start(bf16[2,192,2048]{2,1,0:T(8,128)(2,1)S(1)} %get-tuple-element.47), channel_id=1, source_target_pairs={{0,1},{1,0},{2,3},{3,2},{4,5},{5,4},{6,7},{7,6},{8,9},{9,8},{10,11... | collective-permute-start | bytes 4718600 | tf_op jit(solution)/shard_map/ppermute | solution.py:54
  104.2 1.9 %collective-permute-start.15 = (bf16[2,528,256]{2,1,0:T(8,128)(2,1)S(1)}, bf16[2,528,256]{2,1,0:T(8,128)(2,1)S(1)}, u32[]{:S(2)}, u32[]{:S(2)}) collective-permute-start(bf16[2,528,256]{2,1,0:T(8,128)(2,1)S(1)} %get-tuple-element.57), channel_id=1, source_target_pairs={{0,448},{1,65},{64,128},{65,1},{128,64},{129,193},{192,256},{193,1... | collective-permute-start | bytes 1622024 | tf_op jit(solution)/shard_map/ppermute | solution.py:41
  107.5 1.9 %collective-permute-start.11 = (bf16[2,96,2048]{2,1,0:T(8,128)(2,1)S(1)}, bf16[2,96,2048]{2,1,0:T(8,128)(2,1)S(1)}, u32[]{:S(2)}, u32[]{:S(2)}) collective-permute-start(bf16[2,96,2048]{2,1,0:T(8,128)(2,1)S(1)} %get-tuple-element.49), channel_id=1, source_target_pairs={{0,2},{1,7},{2,0},{3,5},{4,6},{5,3},{6,4},{7,1},{8,10},{9,15},{10,... | collective-permute-start | bytes 2359304 | tf_op jit(solution)/shard_map/ppermute | solution.py:41
  109.9 4.7 %collective-permute-done.15.r_ref = bf16[2,528,256]{2,1,0:T(8,128)(2,1)S(1)} collective-permute-done((bf16[2,528,256]{2,1,0:T(8,128)(2,1)S(1)}, bf16[2,528,256]{2,1,0:T(8,128)(2,1)S(1)}, u32[]{:S(2)}, u32[]{:S(2)}) %collective-permute-start.15) | collective-permute-done | bytes 540704 | tf_op jit(solution)/shard_map/ppermute | solution.py:41
  114.7 4.0 %collective-permute-start.16 = (bf16[2,528,256]{2,1,0:T(8,128)(2,1)S(1)}, bf16[2,528,256]{2,1,0:T(8,128)(2,1)S(1)}, u32[]{:S(2)}, u32[]{:S(2)}) collective-permute-start(bf16[2,528,256]{2,1,0:T(8,128)(2,1)S(1)} %shard_map.162), channel_id=1, source_target_pairs={{0,64},{1,449},{64,0},{65,129},{128,192},{129,65},{192,128},{193,2... | collective-permute-start | bytes 1622024 | tf_op jit(solution)/shard_map/ppermute | solution.py:41
  119.5 2.5 %collective-permute-start.14 = (bf16[1,528,256]{2,1,0:T(8,128)(2,1)S(1)}, bf16[1,528,256]{2,1,0:T(8,128)(2,1)S(1)}, u32[]{:S(2)}, u32[]{:S(2)}) collective-permute-start(bf16[1,528,256]{2,1,0:T(8,128)(2,1)S(1)} %shard_map.158), channel_id=1, source_target_pairs={{0,64},{1,449},{64,0},{65,129},{128,192},{129,65},{192,128},{193,2... | collective-permute-start | bytes 811016 | tf_op jit(solution)/shard_map/ppermute | solution.py:41
  121.9 4.1 %collective-permute-done.16.r_ref = bf16[2,528,256]{2,1,0:T(8,128)(2,1)S(1)} collective-permute-done((bf16[2,528,256]{2,1,0:T(8,128)(2,1)S(1)}, bf16[2,528,256]{2,1,0:T(8,128)(2,1)S(1)}, u32[]{:S(2)}, u32[]{:S(2)}) %collective-permute-start.16) | collective-permute-done | bytes 540704 | tf_op jit(solution)/shard_map/ppermute | solution.py:41
  126.1 1.9 %collective-permute-start.17 = (bf16[1,528,256]{2,1,0:T(8,128)(2,1)S(1)}, bf16[1,528,256]{2,1,0:T(8,128)(2,1)S(1)}, u32[]{:S(2)}, u32[]{:S(2)}) collective-permute-start(bf16[1,528,256]{2,1,0:T(8,128)(2,1)S(1)} %get-tuple-element.58), channel_id=1, source_target_pairs={{0,384},{1,129},{64,192},{65,449},{128,0},{129,257},{192,320},{193... | collective-permute-start | bytes 811016 | tf_op jit(solution)/shard_map/ppermute | solution.py:50
  128.0 5.2 %collective-permute-start.18 = (bf16[1,528,256]{2,1,0:T(8,128)(2,1)S(1)}, bf16[1,528,256]{2,1,0:T(8,128)(2,1)S(1)}, u32[]{:S(2)}, u32[]{:S(2)}) collective-permute-start(bf16[1,528,256]{2,1,0:T(8,128)(2,1)S(1)} %get-tuple-element.59), channel_id=1, source_target_pairs={{0,448},{1,65},{64,128},{65,1},{128,64},{129,193},{192,256},{193,1... | collective-permute-start | bytes 811016 | tf_op jit(solution)/shard_map/ppermute | solution.py:41
  133.4 1.9 %collective-permute-start.12 = (bf16[2,48,2048]{2,1,0:T(8,128)(2,1)S(1)}, bf16[2,48,2048]{2,1,0:T(8,128)(2,1)S(1)}, u32[]{:S(2)}, u32[]{:S(2)}) collective-permute-start(bf16[2,48,2048]{2,1,0:T(8,128)(2,1)S(1)} %get-tuple-element.51), channel_id=1, source_target_pairs={{0,8},{8,0},{1,9},{9,1},{2,10},{10,2},{3,11},{11,3},{4,12},{12,4},... | collective-permute-start | bytes 1179656 | tf_op jit(solution)/shard_map/ppermute | solution.py:54
  136.1 5.2 %collective-permute-done.18.r_ref = bf16[1,528,256]{2,1,0:T(8,128)(2,1)S(1)} collective-permute-done((bf16[1,528,256]{2,1,0:T(8,128)(2,1)S(1)}, bf16[1,528,256]{2,1,0:T(8,128)(2,1)S(1)}, u32[]{:S(2)}, u32[]{:S(2)}) %collective-permute-start.18) | collective-permute-done | bytes 270368 | tf_op jit(solution)/shard_map/ppermute | solution.py:41
  142.2 3.5 %all-to-all-start.1 = ((bf16[8,136,128]{2,1,0:T(8,128)(2,1)}), bf16[8,136,128]{2,1,0:T(8,128)(2,1)S(1)}, u32[]{:S(2)}, u32[]{:S(2)}) async-start(bf16[8,136,128]{2,1,0:T(8,128)(2,1)} %shard_map.165), calls=%async_computation.1 | async-start | bytes 557056 | tf_op jit(solution)/shard_map/all_to_all | solution.py:58
  145.8 1.9 %collective-permute-start.13 = (bf16[2,24,2048]{2,1,0:T(8,128)(2,1)S(1)}, bf16[2,24,2048]{2,1,0:T(8,128)(2,1)S(1)}, u32[]{:S(2)}, u32[]{:S(2)}) collective-permute-start(bf16[2,24,2048]{2,1,0:T(8,128)(2,1)S(1)} %get-tuple-element.53), channel_id=1, source_target_pairs={{0,6},{1,3},{2,4},{3,1},{4,2},{5,7},{6,0},{7,5},{8,14},{9,11},{10,... | collective-permute-start | bytes 589832 | tf_op jit(solution)/shard_map/ppermute | solution.py:41
  147.8 9.3 %all-to-all-done.1.r_ref = bf16[8,136,128]{2,1,0:T(8,128)(2,1)S(1)} async-done(((bf16[8,136,128]{2,1,0:T(8,128)(2,1)}), bf16[8,136,128]{2,1,0:T(8,128)(2,1)S(1)}, u32[]{:S(2)}, u32[]{:S(2)}) %all-to-all-start.1) | async-done | bytes 278560 | tf_op jit(solution)/shard_map/all_to_all | solution.py:58
  (50 shorter events, 10.9 us)
Async XLA Ops:
  1.9 8.1 %collective-permute-start = (bf16[3,24,2048]{2,1,0:T(8,128)(2,1)S(1)}, bf16[3,24,2048]{2,1,0:T(8,128)(2,1)S(1)}, u32[]{:S(2)}, u32[]{:S(2)}) collective-permute-start(bf16[3,24,2048]{2,1,0:T(8,128)(2,1)S(1)} %get-tuple-element.34), channel_id=1, source_target_pairs={{0,8},{8,0},{1,9},{9,1},{2,10},{10,2},{3,11},{11,3},{4,12},{12,4},... | collective-permute-start | bytes 884744 | tf_op jit(solution)/shard_map/ppermute | solution.py:54
  10.0 12.9 %collective-permute-start.1 = (bf16[3,48,2048]{2,1,0:T(8,128)(2,1)S(1)}, bf16[3,48,2048]{2,1,0:T(8,128)(2,1)S(1)}, u32[]{:S(2)}, u32[]{:S(2)}) collective-permute-start(bf16[3,48,2048]{2,1,0:T(8,128)(2,1)S(1)} %constant_dynamic-update-slice_fusion.a_ref), channel_id=1, source_target_pairs={{0,6},{1,3},{2,4},{3,1},{4,2},{5,7},{6,0},{7,5},{8,14},{9,11},{10,... | collective-permute-start | bytes 1769480 | tf_op jit(solution)/shard_map/ppermute | solution.py:41
  23.0 62.8 %copy-start.7 = (s32[8]{0:T(128)S(1)}, s32[8]{0:T(128)}, u32[]{:S(2)}) copy-start(s32[8]{0:T(128)} %constant.24.clone) | copy-start | bytes 100
  23.0 39.7 %collective-permute-start.2 = (bf16[2,3,48,2048]{3,2,1,0:T(8,128)(2,1)S(1)}, bf16[2,3,48,2048]{3,2,1,0:T(8,128)(2,1)}, u32[]{:S(2)}, u32[]{:S(2)}) collective-permute-start(bf16[2,3,48,2048]{3,2,1,0:T(8,128)(2,1)S(1)} %shard_map.147.ta), channel_id=1, source_target_pairs={{0,2},{1,7},{2,0},{3,5},{4,6},{5,3},{6,4},{7,1},{8,10},{9,15},{10,... | collective-permute-start | bytes 3538952 | tf_op jit(solution)/shard_map/ppermute | solution.py:41
  44.8 19.9 %collective-permute-start.4 = (bf16[528,256]{1,0:T(8,128)(2,1)S(1)}, bf16[528,256]{1,0:T(8,128)(2,1)S(1)}, u32[]{:S(2)}, u32[]{:S(2)}) collective-permute-start(bf16[528,256]{1,0:T(8,128)(2,1)S(1)} %shard_map.148.own), channel_id=1, source_target_pairs={{0,448},{1,65},{64,128},{65,1},{128,64},{129,193},{192,256},{193,1... | collective-permute-start | bytes 811016 | tf_op jit(solution)/shard_map/ppermute | solution.py:41
  48.8 18.4 %collective-permute-start.5 = (bf16[528,256]{1,0:T(8,128)(2,1)S(1)}, bf16[528,256]{1,0:T(8,128)(2,1)S(1)}, u32[]{:S(2)}, u32[]{:S(2)}) collective-permute-start(bf16[528,256]{1,0:T(8,128)(2,1)S(1)} %shard_map.148.own), channel_id=1, source_target_pairs={{0,128},{1,385},{64,448},{65,193},{128,256},{129,1},{192,64},{193,... | collective-permute-start | bytes 811016 | tf_op jit(solution)/shard_map/ppermute | solution.py:50
  58.5 36.0 %collective-permute-start.7 = (bf16[2,3,48,2048]{3,2,1,0:T(8,128)(2,1)S(1)}, bf16[2,3,48,2048]{3,2,1,0:T(8,128)(2,1)}, u32[]{:S(2)}, u32[]{:S(2)}) collective-permute-start(bf16[2,3,48,2048]{3,2,1,0:T(8,128)(2,1)S(1)} %shard_map.147.ta), channel_id=1, source_target_pairs={{0,1},{1,0},{2,3},{3,2},{4,5},{5,4},{6,7},{7,6},{8,9},{9,8},{10,11... | collective-permute-start | bytes 3538952 | tf_op jit(solution)/shard_map/ppermute | solution.py:54
  62.7 31.8 %collective-permute-start.8 = (bf16[2,3,48,2048]{3,2,1,0:T(8,128)(2,1)}, bf16[2,3,48,2048]{3,2,1,0:T(8,128)(2,1)}, u32[]{:S(2)}, u32[]{:S(2)}) collective-permute-start(bf16[2,3,48,2048]{3,2,1,0:T(8,128)(2,1)} %collective-permute-done.2.tb), channel_id=1, source_target_pairs={{0,1},{1,0},{2,3},{3,2},{4,5},{5,4},{6,7},{7,6},{8,9},{9,8},{10,11... | collective-permute-start | bytes 3538952 | tf_op jit(solution)/shard_map/ppermute | solution.py:54
  67.3 11.3 %collective-permute-start.6 = (bf16[2,528,256]{2,1,0:T(8,128)(2,1)S(1)}, bf16[2,528,256]{2,1,0:T(8,128)(2,1)S(1)}, u32[]{:S(2)}, u32[]{:S(2)}) collective-permute-start(bf16[2,528,256]{2,1,0:T(8,128)(2,1)S(1)} %shard_map.149.p1), channel_id=1, source_target_pairs={{0,64},{1,449},{64,0},{65,129},{128,192},{129,65},{192,128},{193,2... | collective-permute-start | bytes 1622024 | tf_op jit(solution)/shard_map/ppermute | solution.py:41
  78.6 18.4 %collective-permute-start.9 = (bf16[2,528,256]{2,1,0:T(8,128)(2,1)S(1)}, bf16[2,528,256]{2,1,0:T(8,128)(2,1)S(1)}, u32[]{:S(2)}, u32[]{:S(2)}) collective-permute-start(bf16[2,528,256]{2,1,0:T(8,128)(2,1)S(1)} %collective-permute-done.6.p2), channel_id=1, source_target_pairs={{0,448},{1,65},{64,128},{65,1},{128,64},{129,193},{192,256},{193,1... | collective-permute-start | bytes 1622024 | tf_op jit(solution)/shard_map/ppermute | solution.py:41
  80.5 11.9 %collective-permute-start.3 = (bf16[528,256]{1,0:T(8,128)(2,1)S(1)}, bf16[528,256]{1,0:T(8,128)(2,1)S(1)}, u32[]{:S(2)}, u32[]{:S(2)}) collective-permute-start(bf16[528,256]{1,0:T(8,128)(2,1)S(1)} %shard_map.148.own), channel_id=1, source_target_pairs={{0,64},{1,449},{64,0},{65,129},{128,192},{129,65},{192,128},{193,2... | collective-permute-start | bytes 811016 | tf_op jit(solution)/shard_map/ppermute | solution.py:41
  101.3 5.9 %collective-permute-start.10 = (bf16[2,192,2048]{2,1,0:T(8,128)(2,1)S(1)}, bf16[2,192,2048]{2,1,0:T(8,128)(2,1)S(1)}, u32[]{:S(2)}, u32[]{:S(2)}) collective-permute-start(bf16[2,192,2048]{2,1,0:T(8,128)(2,1)S(1)} %get-tuple-element.47), channel_id=1, source_target_pairs={{0,1},{1,0},{2,3},{3,2},{4,5},{5,4},{6,7},{7,6},{8,9},{9,8},{10,11... | collective-permute-start | bytes 4718600 | tf_op jit(solution)/shard_map/ppermute | solution.py:54
  104.2 10.4 %collective-permute-start.15 = (bf16[2,528,256]{2,1,0:T(8,128)(2,1)S(1)}, bf16[2,528,256]{2,1,0:T(8,128)(2,1)S(1)}, u32[]{:S(2)}, u32[]{:S(2)}) collective-permute-start(bf16[2,528,256]{2,1,0:T(8,128)(2,1)S(1)} %get-tuple-element.57), channel_id=1, source_target_pairs={{0,448},{1,65},{64,128},{65,1},{128,64},{129,193},{192,256},{193,1... | collective-permute-start | bytes 1622024 | tf_op jit(solution)/shard_map/ppermute | solution.py:41
  107.5 25.7 %collective-permute-start.11 = (bf16[2,96,2048]{2,1,0:T(8,128)(2,1)S(1)}, bf16[2,96,2048]{2,1,0:T(8,128)(2,1)S(1)}, u32[]{:S(2)}, u32[]{:S(2)}) collective-permute-start(bf16[2,96,2048]{2,1,0:T(8,128)(2,1)S(1)} %get-tuple-element.49), channel_id=1, source_target_pairs={{0,2},{1,7},{2,0},{3,5},{4,6},{5,3},{6,4},{7,1},{8,10},{9,15},{10,... | collective-permute-start | bytes 2359304 | tf_op jit(solution)/shard_map/ppermute | solution.py:41
  114.7 11.3 %collective-permute-start.16 = (bf16[2,528,256]{2,1,0:T(8,128)(2,1)S(1)}, bf16[2,528,256]{2,1,0:T(8,128)(2,1)S(1)}, u32[]{:S(2)}, u32[]{:S(2)}) collective-permute-start(bf16[2,528,256]{2,1,0:T(8,128)(2,1)S(1)} %shard_map.162), channel_id=1, source_target_pairs={{0,64},{1,449},{64,0},{65,129},{128,192},{129,65},{192,128},{193,2... | collective-permute-start | bytes 1622024 | tf_op jit(solution)/shard_map/ppermute | solution.py:41
  119.5 15.8 %collective-permute-start.14 = (bf16[1,528,256]{2,1,0:T(8,128)(2,1)S(1)}, bf16[1,528,256]{2,1,0:T(8,128)(2,1)S(1)}, u32[]{:S(2)}, u32[]{:S(2)}) collective-permute-start(bf16[1,528,256]{2,1,0:T(8,128)(2,1)S(1)} %shard_map.158), channel_id=1, source_target_pairs={{0,64},{1,449},{64,0},{65,129},{128,192},{129,65},{192,128},{193,2... | collective-permute-start | bytes 811016 | tf_op jit(solution)/shard_map/ppermute | solution.py:41
  126.1 9.7 %collective-permute-start.17 = (bf16[1,528,256]{2,1,0:T(8,128)(2,1)S(1)}, bf16[1,528,256]{2,1,0:T(8,128)(2,1)S(1)}, u32[]{:S(2)}, u32[]{:S(2)}) collective-permute-start(bf16[1,528,256]{2,1,0:T(8,128)(2,1)S(1)} %get-tuple-element.58), channel_id=1, source_target_pairs={{0,384},{1,129},{64,192},{65,449},{128,0},{129,257},{192,320},{193... | collective-permute-start | bytes 811016 | tf_op jit(solution)/shard_map/ppermute | solution.py:50
  128.0 13.2 %collective-permute-start.18 = (bf16[1,528,256]{2,1,0:T(8,128)(2,1)S(1)}, bf16[1,528,256]{2,1,0:T(8,128)(2,1)S(1)}, u32[]{:S(2)}, u32[]{:S(2)}) collective-permute-start(bf16[1,528,256]{2,1,0:T(8,128)(2,1)S(1)} %get-tuple-element.59), channel_id=1, source_target_pairs={{0,448},{1,65},{64,128},{65,1},{128,64},{129,193},{192,256},{193,1... | collective-permute-start | bytes 811016 | tf_op jit(solution)/shard_map/ppermute | solution.py:41
  133.4 12.4 %collective-permute-start.12 = (bf16[2,48,2048]{2,1,0:T(8,128)(2,1)S(1)}, bf16[2,48,2048]{2,1,0:T(8,128)(2,1)S(1)}, u32[]{:S(2)}, u32[]{:S(2)}) collective-permute-start(bf16[2,48,2048]{2,1,0:T(8,128)(2,1)S(1)} %get-tuple-element.51), channel_id=1, source_target_pairs={{0,8},{8,0},{1,9},{9,1},{2,10},{10,2},{3,11},{11,3},{4,12},{12,4},... | collective-permute-start | bytes 1179656 | tf_op jit(solution)/shard_map/ppermute | solution.py:54
  136.0 11.7 %copy-start.6 = (bf16[2048]{0:T(1024)(128)(2,1)S(1)}, bf16[2048]{0:T(1024)(128)(2,1)}, u32[]{:S(2)}) copy-start(bf16[2048]{0:T(1024)(128)(2,1)} %refs_6_.1) | copy-start | bytes 12292
  136.0 21.1 %copy-start.3 = (f32[32,352]{1,0:T(8,128)S(1)}, f32[32,352]{1,0:T(8,128)}, u32[]{:S(2)}) copy-start(f32[32,352]{1,0:T(8,128)} %gs.1) | copy-start | bytes 135172
  136.1 21.1 %copy-start.4 = (f32[32,352]{1,0:T(8,128)S(1)}, f32[32,352]{1,0:T(8,128)}, u32[]{:S(2)}) copy-start(f32[32,352]{1,0:T(8,128)} %us.1) | copy-start | bytes 135172
  136.1 21.1 %copy-start.5 = (f32[32,352]{1,0:T(8,128)S(1)}, f32[32,352]{1,0:T(8,128)}, u32[]{:S(2)}) copy-start(f32[32,352]{1,0:T(8,128)} %ds.1) | copy-start | bytes 135172
  142.2 15.7 %copy-start = (bf16[24,2048]{1,0:T(8,128)(2,1)S(1)}, bf16[24,2048]{1,0:T(8,128)(2,1)}, u32[]{:S(2)}) copy-start(bf16[24,2048]{1,0:T(8,128)(2,1)} %e_ref.1) | copy-start | bytes 294916
  142.2 15.7 %copy-start.1 = (bf16[24,2048]{1,0:T(8,128)(2,1)S(1)}, bf16[24,2048]{1,0:T(8,128)(2,1)}, u32[]{:S(2)}) copy-start(bf16[24,2048]{1,0:T(8,128)(2,1)} %c_ref.1) | copy-start | bytes 294916
  142.2 15.7 %copy-start.2 = (bf16[24,2048]{1,0:T(8,128)(2,1)S(1)}, bf16[24,2048]{1,0:T(8,128)(2,1)}, u32[]{:S(2)}) copy-start(bf16[24,2048]{1,0:T(8,128)(2,1)} %l_ref.1) | copy-start | bytes 294916
  142.2 14.9 %all-to-all-start.1 = ((bf16[8,136,128]{2,1,0:T(8,128)(2,1)}), bf16[8,136,128]{2,1,0:T(8,128)(2,1)S(1)}, u32[]{:S(2)}, u32[]{:S(2)}) async-start(bf16[8,136,128]{2,1,0:T(8,128)(2,1)} %shard_map.165), calls=%async_computation.1 | async-start | bytes 557056 | tf_op jit(solution)/shard_map/all_to_all | solution.py:58
  145.8 12.1 %collective-permute-start.13 = (bf16[2,24,2048]{2,1,0:T(8,128)(2,1)S(1)}, bf16[2,24,2048]{2,1,0:T(8,128)(2,1)S(1)}, u32[]{:S(2)}, u32[]{:S(2)}) collective-permute-start(bf16[2,24,2048]{2,1,0:T(8,128)(2,1)S(1)} %get-tuple-element.53), channel_id=1, source_target_pairs={{0,6},{1,3},{2,4},{3,1},{4,2},{5,7},{6,0},{7,5},{8,14},{9,11},{10,... | collective-permute-start | bytes 589832 | tf_op jit(solution)/shard_map/ppermute | solution.py:41
